TPU v7x, 512 devices: a whole 4x8x8 slice. The times are simulated.
512 devices in a mesh: sp: 128 (over z, y, core), tp: 4 (over x).
Axes of the slice: x: 4, y: 8, z: 8, core: 2. Of those that a mesh axis runs over, the one named last changes fastest.
Arguments:
- features: bfloat16 [16384, 2048], P('sp', 'tp'), may hold values from -16 to 16
- norm_gain: float32 [2048], replicated, may hold values from 0.1 to 1.9
- att_query: bfloat16 [2048, 1024], P('sp', 'tp'), may hold values from -1 to 1
- att_key: bfloat16 [2048, 512], P('sp', 'tp'), may hold values from -1 to 1
- att_value: bfloat16 [2048, 512], P('sp', 'tp'), may hold values from -0.125 to 0.125
- att_lambda: float32 [8], P('tp'), may hold values from 0.3 to 0.8
- att_gain: float32 [128], replicated, may hold values from 0.1 to 1.9
- ret_query: bfloat16 [2048, 512], P('sp', 'tp'), may hold values from -0.125 to 0.125
- ret_key: bfloat16 [2048, 512], P('sp', 'tp'), may hold values from -0.125 to 0.125
- ret_value: bfloat16 [2048, 1024], P('sp', 'tp'), may hold values from -0.125 to 0.125
- ret_gain: float32 [128], replicated, may hold values from 0.1 to 1.9
- out_weight: bfloat16 [2, 1024, 2048], P(None, 'tp'), may hold values from -0.125 to 0.125
Outputs:
- mixed: float32 [16384, 2048], P(('sp', 'tp'))
All inputs are finite; a program needn't handle non-finite values.
Results may differ from a plain program's by a relative error of at most 0.0092.
Values may be sent and summed in bfloat16 or wider, within the bound.
No kernel may reach another device: no remote copies, remote signals or barrier semaphores. Data moves between devices by JAX's collectives and lax.ppermute only.
A program may use at most 64 MiB of HBM per device.

v0:
```python
import functools

import jax
import jax.numpy as jnp
from jax import lax
from jax.experimental import pallas as pl
from jax.experimental.pallas import tpu as pltpu
from jax.sharding import Mesh
from jax.sharding import PartitionSpec as P

DH = 64
DV = 128
SEG = 64
Z = ("zh", "zl")
SP = ("zh", "zl", "y", "c")
SP_TP = ("zh", "zl", "y", "c", "tp")
EPSILON = 1e-06
NEG = -1e30
KEYS = 512
ROWS = 144
INTERPRET = False


def to_all(value, axes):
    count = lax.axis_size(axes)
    return lax.all_to_all(
        jnp.broadcast_to(value[None], (count, *value.shape)), axes, 0, 0, tiled=True
    )


def swapped(value):
    return lax.ppermute(value, "c", [(0, 1), (1, 0)])


def attend_kernel(where_ref, q_ref, k_ref, v_ref, out_ref, vt_ref, qt_ref, m_ref, l_ref, o_ref):
    step = pl.program_id(0)
    z = where_ref[0]
    y = where_ref[1]
    keys = k_ref.shape[0]
    tokens = q_ref.shape[1]

    @pl.when(step == 0)
    def _():
        vt_ref[...] = v_ref[...].T

    def visit(start, count, masked):
        s = jnp.dot(k_ref[pl.ds(start, count)], qt_ref[...], preferred_element_type=jnp.float32)
        if masked:
            rows = lax.broadcasted_iota(jnp.int32, s.shape, 0) + start
            cols = lax.broadcasted_iota(jnp.int32, s.shape, 1) % tokens + y * tokens
            allowed = (rows // SEG) <= (cols // SEG)
            s = jnp.where(allowed, s, NEG)
        old = m_ref[...]
        top = jnp.maximum(old, jnp.max(s, axis=0, keepdims=True))
        w = jnp.exp(s - top)
        factor = jnp.exp(old - top)
        m_ref[...] = top
        l_ref[...] = l_ref[...] * factor + jnp.sum(w, axis=0, keepdims=True)
        o_ref[...] = o_ref[...] * factor + jnp.dot(
            vt_ref[:, pl.ds(start, count)],
            w.astype(jnp.bfloat16),
            preferred_element_type=jnp.float32,
        )

    @pl.when(step >= z)
    def _():
        q = q_ref[0]
        lane = lax.broadcasted_iota(jnp.int32, q.shape, 1)
        zero = jnp.zeros_like(q)
        q = jnp.concatenate([jnp.where(lane < DH, q, zero), jnp.where(lane < DH, zero, q)], axis=0)
        qt_ref[...] = q.T
        m_ref[...] = jnp.full(m_ref.shape, NEG, jnp.float32)
        l_ref[...] = jnp.zeros(l_ref.shape, jnp.float32)
        o_ref[...] = jnp.zeros(o_ref.shape, jnp.float32)

    @pl.when(step == z)
    def _():
        def body(i, _):
            visit(pl.multiple_of(i * KEYS, KEYS), KEYS, True)
            return 0

        lax.fori_loop(0, (y * tokens) // KEYS + 1, body, 0)

    @pl.when(step > z)
    def _():
        for start in range(0, keys, KEYS):
            visit(start, KEYS, False)

    @pl.when(step >= z)
    def _():
        total = l_ref[...]
        out_ref[0, :DV] = (o_ref[...] / total).astype(jnp.bfloat16)
        weight = m_ref[...] + jnp.log(total)
        high = weight.astype(jnp.bfloat16)
        rest = weight - high.astype(jnp.float32)
        middle = rest.astype(jnp.bfloat16)
        low = (rest - middle.astype(jnp.float32)).astype(jnp.bfloat16)
        pad = jnp.zeros((ROWS - DV - 3, weight.shape[1]), jnp.bfloat16)
        out_ref[0, DV:] = jnp.concatenate([high, middle, low, pad], axis=0)

    @pl.when(step < z)
    def _():
        out_ref[0, :DV] = jnp.zeros((DV, 2 * tokens), jnp.bfloat16)
        row = lax.broadcasted_iota(jnp.int32, (ROWS - DV, 2 * tokens), 0)
        out_ref[0, DV:] = jnp.where(row == 0, NEG, 0.0).astype(jnp.bfloat16)


def attend(where, queries, keys, values):
    blocks, tokens, _ = queries.shape
    count = keys.shape[0]

    def whole(shape):
        return pl.BlockSpec(shape, lambda g, w: (0, 0))

    return pl.pallas_call(
        attend_kernel,
        grid_spec=pltpu.PrefetchScalarGridSpec(
            num_scalar_prefetch=1,
            grid=(blocks,),
            in_specs=[
                pl.BlockSpec((1, tokens, 2 * DH), lambda g, w: (g, 0, 0)),
                whole(keys.shape),
                whole(values.shape),
            ],
            out_specs=pl.BlockSpec((1, ROWS, 2 * tokens), lambda g, w: (g, 0, 0)),
            scratch_shapes=[
                pltpu.VMEM((DV, count), jnp.bfloat16),
                pltpu.VMEM((2 * DH, 2 * tokens), jnp.bfloat16),
                pltpu.VMEM((1, 2 * tokens), jnp.float32),
                pltpu.VMEM((1, 2 * tokens), jnp.float32),
                pltpu.VMEM((DV, 2 * tokens), jnp.float32),
            ],
        ),
        out_shape=jax.ShapeDtypeStruct((blocks, ROWS, 2 * tokens), jnp.bfloat16),
        compiler_params=pltpu.CompilerParams(dimension_semantics=("arbitrary",)),
        cost_estimate=pl.CostEstimate(
            flops=blocks * count * tokens * 4 * 256,
            bytes_accessed=blocks * tokens * 1024 + count * 512,
            transcendentals=blocks * count * tokens * 2,
        ),
        name="attend",
        interpret=INTERPRET,
    )(where, queries, keys, values)


def finish_kernel(parts_ref, mix_ref, gain_ref, out_ref):
    blocks = parts_ref.shape[0]
    tokens = out_ref.shape[0]
    logs = []
    for i in range(blocks):
        rows = parts_ref[i, DV:].astype(jnp.float32)
        logs.append(rows[0:1] + rows[1:2] + rows[2:3])
    top = functools.reduce(jnp.maximum, logs)
    shares = [jnp.exp(log - top) for log in logs]
    total = functools.reduce(jnp.add, shares)
    acc = jnp.zeros((DV, 2 * tokens), jnp.float32)
    for i in range(blocks):
        acc = acc + parts_ref[i, :DV].astype(jnp.float32) * (shares[i] / total)
    att = acc[:, :tokens] - mix_ref[...] * acc[:, tokens:]
    att = att * lax.rsqrt(jnp.mean(att * att, axis=0, keepdims=True) + EPSILON)
    out_ref[...] = (att.T * gain_ref[...]).astype(jnp.bfloat16)


def finish(parts, mixing, gain):
    tokens = parts.shape[2] // 2
    return pl.pallas_call(
        finish_kernel,
        out_shape=jax.ShapeDtypeStruct((tokens, DV), jnp.bfloat16),
        name="finish",
        interpret=INTERPRET,
    )(parts, jnp.broadcast_to(mixing.reshape(1, 1), (1, tokens)), gain.reshape(1, DV))


def rotate(vectors, cosine, sine):
    half = vectors.shape[-1] // 2
    a = vectors[..., :half]
    b = vectors[..., half:]
    return jnp.concatenate([a * cosine - b * sine, a * sine + b * cosine], axis=-1)


def decay_log(head, length):
    pair = (head // 2).astype(jnp.float32)
    quick = jnp.log1p(-jnp.exp2(-5.0 - pair / 4.0))
    slow = jnp.log1p(-1.0 / (length * (1.0 + pair)))
    return jnp.where(head % 2 == 0, quick, slow)


def layer(
    features,
    norm_gain,
    att_query,
    att_key,
    att_value,
    att_lambda,
    att_gain,
    ret_query,
    ret_key,
    ret_value,
    ret_gain,
    out_weight,
):
    z = lax.axis_index(Z)
    y = lax.axis_index("y")
    c = lax.axis_index("c")
    ny = lax.axis_size("y")
    nz = lax.axis_size(Z)
    chip = z * ny + y

    def half(array, h):
        width = array.shape[1] // 2
        return array[:, h * width : (h + 1) * width]

    per_head = (ret_query, ret_key, ret_value)
    halves = jnp.stack(
        [
            jnp.concatenate([half(att_query, h), whole] + [half(a, h) for a in per_head], axis=1)
            for h, whole in enumerate((att_key, att_value))
        ]
    )
    rows, width = halves.shape[1:]
    sent = jnp.broadcast_to(halves[None], (ny, 2, rows, width)).reshape(2 * ny, rows, width)
    w_z = lax.all_to_all(sent, ("y", "c"), 0, 0, tiled=True).reshape(2 * ny * rows, width)
    w_z, features = lax.optimization_barrier((w_z, features))
    w_all = to_all(w_z, Z).reshape(-1, width)

    groups = lax.axis_size("tp")
    x = lax.axis_index("tp")
    pieces = [features] + [
        lax.ppermute(features, "tp", [(i, (i + k) % groups) for i in range(groups)])
        for k in range(1, groups)
    ]
    tokens = features.shape[0]
    gathered = jnp.zeros((groups, *features.shape), features.dtype)
    for k, piece in enumerate(pieces):
        gathered = lax.dynamic_update_index_in_dim(gathered, piece, (x - k) % groups, 0)
    floats = gathered.astype(jnp.float32)
    mean_sq = jnp.sum(floats * floats, axis=(0, 2)) / norm_gain.shape[0]
    gain = norm_gain.reshape(groups, 1, -1)
    scaled = floats * lax.rsqrt(mean_sq + EPSILON)[None, :, None] * gain
    normed = jnp.concatenate(list(scaled.astype(jnp.bfloat16)), axis=1)
    across = swapped(normed)
    both = jnp.concatenate(
        [jnp.where(c == 0, normed, across), jnp.where(c == 0, across, normed)], axis=0
    )
    tokens = 2 * tokens
    made = jnp.dot(both, w_all, preferred_element_type=jnp.float32).astype(jnp.bfloat16)
    q_att = made[:, :128]
    kv = made[:, 128:256]
    q_ret = made[:, 256:320].astype(jnp.float32)
    k_ret = made[:, 320:384].astype(jnp.float32)
    v_ret = made[:, 384:512].astype(jnp.float32)

    highest = lax.Precision.HIGHEST
    length = nz * ny * tokens
    log_decay = decay_log(lax.axis_index("tp") * 2 + c, float(length))
    offsets = jnp.arange(tokens).astype(jnp.float32)
    positions = (chip * tokens + jnp.arange(tokens)).astype(jnp.float32)
    inverse = 10000.0 ** (-jnp.arange(0, DH, 2).astype(jnp.float32) / DH)
    angles = positions[:, None] * inverse[None, :]
    cosine, sine = jnp.cos(angles), jnp.sin(angles)
    q_rot = rotate(q_ret, cosine, sine)
    k_rot = rotate(k_ret, cosine, sine) * DH ** (-0.5)
    key_weight = jnp.exp(log_decay * (tokens - 1.0 - offsets))
    own_state = jnp.einsum("jd,je->de", k_rot * key_weight[:, None], v_ret, precision=highest)

    spread = to_all(jnp.concatenate([kv, own_state.astype(jnp.bfloat16)], axis=0), "y")
    kv_mine = spread[:, :tokens].reshape(ny * tokens, 2 * DH)
    kv_other = swapped(kv_mine)
    keys = jnp.where(c == 0, kv_mine, kv_other)
    values = jnp.where(c == 0, kv_other, kv_mine)
    states = spread[:, tokens:].astype(jnp.float32)
    ys = jnp.arange(ny)
    zs = jnp.arange(nz)
    span = log_decay * tokens
    to_end = jnp.exp(span * (ny - 1 - ys).astype(jnp.float32))
    sums = jnp.sum(states * to_end[:, None, None], axis=0)
    scaled_q = q_att * jnp.bfloat16(DH ** (-0.5))
    along = to_all(jnp.concatenate([scaled_q, sums.astype(jnp.bfloat16)], axis=0), Z)
    parts = attend(jnp.stack([z, y]).astype(jnp.int32), along[:, :tokens], keys, values)
    parts = lax.all_to_all(parts, Z, 0, 0, tiled=True)

    others = along[:, tokens:].astype(jnp.float32)
    y_weight = jnp.where(ys < y, jnp.exp(span * jnp.maximum(y - 1 - ys, 0).astype(jnp.float32)), 0.0)
    steps = jnp.maximum(ny * (z - 1 - zs) + y, 0).astype(jnp.float32)
    z_weight = jnp.where(zs < z, jnp.exp(span * steps), 0.0)
    carried = jnp.sum(states * y_weight[:, None, None], axis=0)
    carried = carried + jnp.sum(others * z_weight[:, None, None], axis=0)

    distance = offsets[:, None] - offsets[None, :]
    inside = jnp.where(distance >= 0, jnp.exp(log_decay * jnp.maximum(distance, 0.0)), 0.0)
    scores = jnp.einsum("id,jd->ij", q_rot, k_rot, precision=highest) * inside
    within = jnp.dot(scores, v_ret, precision=highest)
    query_weight = jnp.exp(log_decay * (offsets + 1.0))
    ret = within + jnp.dot(q_rot, carried, precision=highest) * query_weight[:, None]
    ret = ret * lax.rsqrt(jnp.mean(ret * ret, axis=-1, keepdims=True) + EPSILON) * ret_gain
    ret = ret.astype(jnp.bfloat16)

    mixing = lax.dynamic_index_in_dim(att_lambda, c, 0, keepdims=False)
    att = finish(parts, mixing, att_gain)

    heads = jnp.concatenate([att, ret], axis=1).reshape(2, tokens // 2, 2 * DV)
    heads = lax.all_to_all(heads, "c", 0, 0, tiled=True)
    joined = jnp.concatenate(
        [heads[0, :, :DV], heads[1, :, :DV], heads[0, :, DV:], heads[1, :, DV:]], axis=1
    )
    partial = jnp.dot(
        joined, out_weight.reshape(-1, out_weight.shape[2]), preferred_element_type=jnp.float32
    ).astype(jnp.bfloat16)
    partial = lax.all_to_all(
        partial.reshape(groups, -1, partial.shape[1]), "tp", 0, 0, tiled=True
    )
    return jnp.sum(partial.astype(jnp.float32), axis=0)


def solution(mesh):
    devices = mesh.devices
    torus = Mesh(devices.reshape(2, 4, -1, 2, devices.shape[-1]), SP_TP)
    return jax.shard_map(
        layer,
        mesh=torus,
        in_specs=(
            P(SP, "tp"),
            P(),
            P(SP, "tp"),
            P(SP, "tp"),
            P(SP, "tp"),
            P("tp"),
            P(),
            P(SP, "tp"),
            P(SP, "tp"),
            P(SP, "tp"),
            P(),
            P(None, "tp", None),
        ),
        out_specs=P(SP_TP, None),
        check_vma=False,
    )
```

profile of v0, /device:TPU:1, one launch (start us, length us, event | category | flops | bytes accessed | tf_op | source)
XLA Modules:
  0.0 220.6 jit_solution(17047331772982891598)
XLA Ops:
  3.3 21.0 %all_to_all.35 = bf16[16,16,512]{2,1,0:T(8,128)(2,1)S(1)} all-to-all(bf16[16,16,512]{2,1,0:T(8,128)(2,1)S(1)} %bitcast.46), channel_id=1, replica_groups=mesh['zh'=2,'zl'=4,'y'=8,'c'=2,'tp'=4] {'y','c'}, dimensions={0} | all-to-all | bytes 524288 | tf_op jit(solution)/shard_map/all_to_all | solution.py:222
  24.3 1.5 broadcast_in_dim.72
  25.8 9.1 %all-to-all-start.1 = ((bf16[8,256,512]{2,1,0:T(8,128)(2,1)}), bf16[8,256,512]{2,1,0:T(8,128)(2,1)}, u32[]{:S(2)}, u32[]{:S(2)}) async-start(bf16[8,256,512]{2,1,0:T(8,128)(2,1)} %broadcast_in_dim.72), calls=%async_computation.1 | async-start | bytes 4194304 | tf_op jit(solution)/shard_map/all_to_all | solution.py:26
  35.0 3.1 %collective-permute-start = (bf16[128,512]{1,0:T(8,128)(2,1)S(1)}, bf16[128,512]{1,0:T(8,128)(2,1)S(1)}, u32[]{:S(2)}, u32[]{:S(2)}) collective-permute-start(bf16[128,512]{1,0:T(8,128)(2,1)S(1)} %copy-done.4), channel_id=1, source_target_pairs={{0,1},{1,2},{2,3},{3,0},{4,5},{5,6},{6,7},{7,4},{8,9},{9,10},{10,1... | collective-permute-start | bytes 393224 | tf_op jit(solution)/shard_map/ppermute | solution.py:229
  38.1 4.4 %collective-permute-start.1 = (bf16[128,512]{1,0:T(8,128)(2,1)S(1)}, bf16[128,512]{1,0:T(8,128)(2,1)S(1)}, u32[]{:S(2)}, u32[]{:S(2)}) collective-permute-start(bf16[128,512]{1,0:T(8,128)(2,1)S(1)} %copy-done.4), channel_id=1, source_target_pairs={{0,2},{1,3},{2,0},{3,1},{4,6},{5,7},{6,4},{7,5},{8,10},{9,11},{10,... | collective-permute-start | bytes 393224 | tf_op jit(solution)/shard_map/ppermute | solution.py:229
  42.5 3.1 %collective-permute-start.2 = (bf16[128,512]{1,0:T(8,128)(2,1)S(1)}, bf16[128,512]{1,0:T(8,128)(2,1)S(1)}, u32[]{:S(2)}, u32[]{:S(2)}) collective-permute-start(bf16[128,512]{1,0:T(8,128)(2,1)S(1)} %copy-done.4), channel_id=1, source_target_pairs={{0,3},{1,0},{2,1},{3,2},{4,7},{5,4},{6,5},{7,6},{8,11},{9,8},{10,9... | collective-permute-start | bytes 393224 | tf_op jit(solution)/shard_map/ppermute | solution.py:229
  45.7 1.5 collective-permute-done.1
  47.2 1.9 collective-permute-done.2
  50.4 3.1 %collective-permute-start.3 = (bf16[128,2048]{1,0:T(8,128)(2,1)}, bf16[128,2048]{1,0:T(8,128)(2,1)S(1)}, u32[]{:S(2)}, u32[]{:S(2)}) collective-permute-start(bf16[128,2048]{1,0:T(8,128)(2,1)} %pad_maximum_fusion), channel_id=1, source_target_pairs={{0,4},{4,0},{1,5},{5,1},{2,6},{6,2},{3,7},{7,3},{8,12},{12,8},{9,1... | collective-permute-start | bytes 1572872 | tf_op jit(solution)/shard_map/ppermute | solution.py:32
  53.8 1.5 collective-permute-done.3
  56.4 30.4 %all-to-all-done.1 = bf16[8,256,512]{2,1,0:T(8,128)(2,1)} async-done(((bf16[8,256,512]{2,1,0:T(8,128)(2,1)}), bf16[8,256,512]{2,1,0:T(8,128)(2,1)}, u32[]{:S(2)}, u32[]{:S(2)}) %all-to-all-start.1) | async-done | bytes 2097184 | tf_op jit(solution)/shard_map/all_to_all | solution.py:26
  86.9 2.9 %convolution_convert_fusion.1 = bf16[256,512]{0,1:T(8,128)(2,1)S(1)} fusion(bf16[2048,512]{1,0:T(8,128)(2,1)} %bitcast.14, bf16[128,2048]{1,0:T(8,128)(2,1)} %get-tuple-element.14, bf16[128,2048]{1,0:T(8,128)(2,1)} %get-tuple-element.13), kind=kOutput, calls=%fused_computation.3 | convolution fusion | flops 539099136 | bytes 3407872 | tf_op jit(solution)/shard_map/dot_general | solution.py:246
  91.9 3.5 %all-to-all-start.2 = ((bf16[8,320,128]{2,1,0:T(8,128)(2,1)}), bf16[8,320,128]{2,1,0:T(8,128)(2,1)S(1)}, u32[]{:S(2)}, u32[]{:S(2)}) async-start(bf16[8,320,128]{2,1,0:T(8,128)(2,1)} %broadcast_in_dim.73), calls=%async_computation.2 | async-start | bytes 1310720 | tf_op jit(solution)/shard_map/all_to_all | solution.py:26
  95.5 20.7 %all-to-all-done.2 = bf16[8,320,128]{2,1,0:T(8,128)(2,1)S(1)} async-done(((bf16[8,320,128]{2,1,0:T(8,128)(2,1)}), bf16[8,320,128]{2,1,0:T(8,128)(2,1)S(1)}, u32[]{:S(2)}, u32[]{:S(2)}) %all-to-all-start.2) | async-done | bytes 655392 | tf_op jit(solution)/shard_map/all_to_all | solution.py:26
  117.4 3.5 %all-to-all-start.3 = ((bf16[8,320,128]{2,1,0:T(8,128)(2,1)}), bf16[8,320,128]{2,1,0:T(8,128)(2,1)S(1)}, u32[]{:S(2)}, u32[]{:S(2)}) async-start(bf16[8,320,128]{2,1,0:T(8,128)(2,1)} %broadcast_in_dim.74), calls=%async_computation.3 | async-start | bytes 1310720 | tf_op jit(solution)/shard_map/all_to_all | solution.py:26
  121.0 2.4 %collective-permute-start.4 = (bf16[2048,128]{1,0:T(8,128)(2,1)S(1)}, bf16[2048,128]{1,0:T(8,128)(2,1)S(1)}, u32[]{:S(2)}, u32[]{:S(2)}) collective-permute-start(bf16[2048,128]{1,0:T(8,128)(2,1)S(1)} %bitcast.43), channel_id=1, source_target_pairs={{0,4},{4,0},{1,5},{5,1},{2,6},{6,2},{3,7},{7,3},{8,12},{12,8},{9,1... | collective-permute-start | bytes 1572872 | tf_op jit(solution)/shard_map/ppermute | solution.py:32
  126.0 15.6 %all-to-all-done.3 = bf16[8,320,128]{2,1,0:T(8,128)(2,1)S(1)} async-done(((bf16[8,320,128]{2,1,0:T(8,128)(2,1)}), bf16[8,320,128]{2,1,0:T(8,128)(2,1)S(1)}, u32[]{:S(2)}, u32[]{:S(2)}) %all-to-all-start.3) | async-done | bytes 655392 | tf_op jit(solution)/shard_map/all_to_all | solution.py:26
  142.6 20.2 %attend.1 = bf16[8,144,512]{2,1,0:T(8,128)(2,1)} custom-call(s32[2]{0:T(128)} %pad_add_fusion.where_ref, bf16[8,256,128]{2,1,0:T(8,128)(2,1)} %slice.107.q_ref, bf16[2048,128]{1,0:T(8,128)(2,1)} %get-tuple-element.12.k_ref, bf16[2048,128]{1,0:T(8,128)(2,1)} %get-tuple-element.11.v_ref), custom_call_target="tpu_custom_call" | custom-call | flops 4294967296 | bytes 3145728 | tf_op jit(solution)/shard_map/attend/pallas_call | solution.py:115
  162.8 3.7 %all-to-all-start.4 = ((bf16[8,144,512]{2,1,0:T(8,128)(2,1)}), bf16[8,144,512]{2,1,0:T(8,128)(2,1)S(1)}, u32[]{:S(2)}, u32[]{:S(2)}) async-start(bf16[8,144,512]{2,1,0:T(8,128)(2,1)} %attend.1), calls=%async_computation.4 | async-start | bytes 2359296 | tf_op jit(solution)/shard_map/all_to_all | solution.py:280
  170.5 1.2 multiply_reduce_fusion.1
  171.8 26.6 %all-to-all-done.4.parts_ref = bf16[8,144,512]{2,1,0:T(8,128)(2,1)S(1)} async-done(((bf16[8,144,512]{2,1,0:T(8,128)(2,1)}), bf16[8,144,512]{2,1,0:T(8,128)(2,1)S(1)}, u32[]{:S(2)}, u32[]{:S(2)}) %all-to-all-start.4) | async-done | bytes 1179680 | tf_op jit(solution)/shard_map/all_to_all | solution.py:280
  199.7 2.4 %finish.1 = bf16[256,128]{1,0:T(8,128)(2,1)} custom-call(bf16[8,144,512]{2,1,0:T(8,128)(2,1)} %copy-done.1, f32[1,256]{1,0:T(1,128)} %broadcast_in_dim.76.mix_ref, f32[1,128]{1,0:T(1,128)} %bitcast.50), custom_call_target="tpu_custom_call" | custom-call | tf_op jit(solution)/shard_map/finish/pallas_call | solution.py:166
  202.9 4.0 %all_to_all.36 = bf16[2,128,256]{2,1,0:T(8,128)(2,1)S(1)} all-to-all(bf16[2,128,256]{2,1,0:T(8,128)(2,1)S(1)} %bitcast.47), channel_id=1, replica_groups=mesh['zh'=2,'zl'=4,'y'=8,'c'=2,'tp'=4] {'c'}, dimensions={0} | all-to-all | bytes 262144 | tf_op jit(solution)/shard_map/all_to_all | solution.py:302
  207.4 12.5 %all_to_all.37 = bf16[4,32,2048]{2,1,0:T(8,128)(2,1)S(1)} all-to-all(bf16[4,32,2048]{2,1,0:T(8,128)(2,1)S(1)} %bitcast.44), channel_id=1, replica_groups=mesh['zh'=2,'zl'=4,'y'=8,'c'=2,'tp'=4] {'tp'}, dimensions={0} | all-to-all | bytes 1048576 | tf_op jit(solution)/shard_map/all_to_all | solution.py:309
  (70 shorter events, 20.2 us)
Async XLA Ops:
  0.0 206.9 %copy-start = (bf16[2,256,2048]{2,1,0:T(8,128)(2,1)S(1)}, bf16[2,256,2048]{2,1,0:T(8,128)(2,1)}, u32[]{:S(2)}) copy-start(bf16[2,256,2048]{2,1,0:T(8,128)(2,1)} %param.23) | copy-start | bytes 6291460
  25.8 9.2 %copy-start.5 = (f32[2048]{0:T(1024)S(1)}, f32[2048]{0:T(1024)}, u32[]{:S(2)}) copy-start(f32[2048]{0:T(1024)} %param.13) | copy-start | bytes 24580
  25.8 9.2 %copy-start.4 = (bf16[128,512]{1,0:T(8,128)(2,1)S(1)}, bf16[128,512]{1,0:T(8,128)(2,1)}, u32[]{:S(2)}) copy-start(bf16[128,512]{1,0:T(8,128)(2,1)} %param.12) | copy-start | bytes 393220
  25.8 61.1 %all-to-all-start.1 = ((bf16[8,256,512]{2,1,0:T(8,128)(2,1)}), bf16[8,256,512]{2,1,0:T(8,128)(2,1)}, u32[]{:S(2)}, u32[]{:S(2)}) async-start(bf16[8,256,512]{2,1,0:T(8,128)(2,1)} %broadcast_in_dim.72), calls=%async_computation.1 | async-start | bytes 4194304 | tf_op jit(solution)/shard_map/all_to_all | solution.py:26
  35.0 10.6 %collective-permute-start = (bf16[128,512]{1,0:T(8,128)(2,1)S(1)}, bf16[128,512]{1,0:T(8,128)(2,1)S(1)}, u32[]{:S(2)}, u32[]{:S(2)}) collective-permute-start(bf16[128,512]{1,0:T(8,128)(2,1)S(1)} %copy-done.4), channel_id=1, source_target_pairs={{0,1},{1,2},{2,3},{3,0},{4,5},{5,6},{6,7},{7,4},{8,9},{9,10},{10,1... | collective-permute-start | bytes 393224 | tf_op jit(solution)/shard_map/ppermute | solution.py:229
  38.1 9.0 %collective-permute-start.1 = (bf16[128,512]{1,0:T(8,128)(2,1)S(1)}, bf16[128,512]{1,0:T(8,128)(2,1)S(1)}, u32[]{:S(2)}, u32[]{:S(2)}) collective-permute-start(bf16[128,512]{1,0:T(8,128)(2,1)S(1)} %copy-done.4), channel_id=1, source_target_pairs={{0,2},{1,3},{2,0},{3,1},{4,6},{5,7},{6,4},{7,5},{8,10},{9,11},{10,... | collective-permute-start | bytes 393224 | tf_op jit(solution)/shard_map/ppermute | solution.py:229
  42.5 6.6 %collective-permute-start.2 = (bf16[128,512]{1,0:T(8,128)(2,1)S(1)}, bf16[128,512]{1,0:T(8,128)(2,1)S(1)}, u32[]{:S(2)}, u32[]{:S(2)}) collective-permute-start(bf16[128,512]{1,0:T(8,128)(2,1)S(1)} %copy-done.4), channel_id=1, source_target_pairs={{0,3},{1,0},{2,1},{3,2},{4,7},{5,4},{6,5},{7,6},{8,11},{9,8},{10,9... | collective-permute-start | bytes 393224 | tf_op jit(solution)/shard_map/ppermute | solution.py:229
  50.4 4.9 %collective-permute-start.3 = (bf16[128,2048]{1,0:T(8,128)(2,1)}, bf16[128,2048]{1,0:T(8,128)(2,1)S(1)}, u32[]{:S(2)}, u32[]{:S(2)}) collective-permute-start(bf16[128,2048]{1,0:T(8,128)(2,1)} %pad_maximum_fusion), channel_id=1, source_target_pairs={{0,4},{4,0},{1,5},{5,1},{2,6},{6,2},{3,7},{7,3},{8,12},{12,8},{9,1... | collective-permute-start | bytes 1572872 | tf_op jit(solution)/shard_map/ppermute | solution.py:32
  89.7 0.9 copy-start.3
  91.9 24.2 %all-to-all-start.2 = ((bf16[8,320,128]{2,1,0:T(8,128)(2,1)}), bf16[8,320,128]{2,1,0:T(8,128)(2,1)S(1)}, u32[]{:S(2)}, u32[]{:S(2)}) async-start(bf16[8,320,128]{2,1,0:T(8,128)(2,1)} %broadcast_in_dim.73), calls=%async_computation.2 | async-start | bytes 1310720 | tf_op jit(solution)/shard_map/all_to_all | solution.py:26
  117.4 24.2 %all-to-all-start.3 = ((bf16[8,320,128]{2,1,0:T(8,128)(2,1)}), bf16[8,320,128]{2,1,0:T(8,128)(2,1)S(1)}, u32[]{:S(2)}, u32[]{:S(2)}) async-start(bf16[8,320,128]{2,1,0:T(8,128)(2,1)} %broadcast_in_dim.74), calls=%async_computation.3 | async-start | bytes 1310720 | tf_op jit(solution)/shard_map/all_to_all | solution.py:26
  121.0 3.9 %collective-permute-start.4 = (bf16[2048,128]{1,0:T(8,128)(2,1)S(1)}, bf16[2048,128]{1,0:T(8,128)(2,1)S(1)}, u32[]{:S(2)}, u32[]{:S(2)}) collective-permute-start(bf16[2048,128]{1,0:T(8,128)(2,1)S(1)} %bitcast.43), channel_id=1, source_target_pairs={{0,4},{4,0},{1,5},{5,1},{2,6},{6,2},{3,7},{7,3},{8,12},{12,8},{9,1... | collective-permute-start | bytes 1572872 | tf_op jit(solution)/shard_map/ppermute | solution.py:32
  141.7 21.1 %copy-start.2 = (bf16[8,320,128]{2,1,0:T(8,128)(2,1)}, bf16[8,320,128]{2,1,0:T(8,128)(2,1)S(1)}, u32[]{:S(2)}) copy-start(bf16[8,320,128]{2,1,0:T(8,128)(2,1)S(1)} %all-to-all-done.3) | copy-start | bytes 1966084
  162.8 3.7 %copy-start.7 = (f32[2]{0:T(128)S(1)}, f32[2]{0:T(128)}, u32[]{:S(2)}) copy-start(f32[2]{0:T(128)} %param.17) | copy-start | bytes 28
  162.8 8.9 %copy-start.6 = (f32[128]{0:T(128)S(1)}, f32[128]{0:T(128)}, u32[]{:S(2)}) copy-start(f32[128]{0:T(128)} %param.22) | copy-start | bytes 1540
  162.8 35.7 %all-to-all-start.4 = ((bf16[8,144,512]{2,1,0:T(8,128)(2,1)}), bf16[8,144,512]{2,1,0:T(8,128)(2,1)S(1)}, u32[]{:S(2)}, u32[]{:S(2)}) async-start(bf16[8,144,512]{2,1,0:T(8,128)(2,1)} %attend.1), calls=%async_computation.4 | async-start | bytes 2359296 | tf_op jit(solution)/shard_map/all_to_all | solution.py:280
  198.5 1.2 copy-start.1
where the time goes:
time: 222 us; the launch traced here: 221 us
  waiting for transfers between devices  99.1 us (45%)
  blocking collectives  37.4 us (17%)
  starting transfers between devices  36 us (16%)
  Pallas kernels  22.6 us (10%)
  local copies, waits for them, and re-layouts  9.92 us (4%)
  other arithmetic  7.97 us (4%)
  matrix products  7.03 us (3%)
    all_to_all x3, waiting for transfers between devices, to_all(): lax.all_to_all(jnp.broadcast_to(value[None], (count, *value.shape)), axes...  66.7 us
    all_to_all x1, waiting for transfers between devices, layer(): parts = lax.all_to_all(parts, Z, 0, 0, tiled=True)  26.6 us
    all_to_all x1, blocking collectives, layer(): lax.all_to_all(sent, ('y', 'c'), 0, 0, tiled=True)  21 us
    pallas_call x1, Pallas kernels, attend(): pl.pallas_call(attend_kernel, grid_spec=pltpu.PrefetchScalarGridSpec(num_...  20.2 us
    all_to_all x3, starting transfers between devices, to_all(): lax.all_to_all(jnp.broadcast_to(value[None], (count, *value.shape)), axes...  16.2 us
    all_to_all x1, blocking collectives, layer(): lax.all_to_all(partial.reshape(groups, -1, partial.shape[1]), 'tp', 0, 0,...  12.5 us
    ppermute x3, starting transfers between devices, layer(): lax.ppermute(features, 'tp', [(i, (i + k) % groups) for i in range(groups)])  10.5 us
    ppermute x2, starting transfers between devices, swapped(): return lax.ppermute(value, 'c', [(0, 1), (1, 0)])  5.54 us
  transfers between devices with their start and end apart: 9, of which 8 were waited for; matrix products, arithmetic and copies ran while one was open for 4% of the time, Pallas kernels for 0%

commit v1 on v0

v1 whole, which is shorter than its diff:
```python
import functools

import jax
import jax.numpy as jnp
from jax import lax
from jax.experimental import pallas as pl
from jax.experimental.pallas import tpu as pltpu
from jax.sharding import Mesh
from jax.sharding import PartitionSpec as P

DH = 64
DV = 128
SEG = 64
Z = ("zh", "zl")
SP = ("zh", "zl", "y", "c")
SP_TP = ("zh", "zl", "y", "c", "tp")
EPSILON = 1e-06
NEG = -1e30
KEYS = 512
ROWS = 144
VMEM = pl.BlockSpec(memory_space=pltpu.VMEM)
SMEM = pl.BlockSpec(memory_space=pltpu.SMEM)
INTERPRET = False


def swapped(value):
    return lax.ppermute(value, "c", [(0, 1), (1, 0)])


def shifted(value, step):
    count = lax.axis_size(Z)
    return lax.ppermute(value, Z, [(i, (i + step) % count) for i in range(count)])


def two_steps(own, half):
    before = shifted(own, 1)
    after = shifted(own, -1)
    low = shifted(before[:half], 1)
    high = shifted(after[half:], -1)
    return before, after, low, high


def pack_kernel(query_ref, key_ref, value_ref, rq_ref, rk_ref, rv_ref, out_ref):
    for h, whole in enumerate((key_ref, value_ref)):
        parts = []
        for ref in (query_ref, None, rq_ref, rk_ref, rv_ref):
            if ref is None:
                parts.append(whole[...])
            else:
                width = ref.shape[1] // 2
                parts.append(ref[:, h * width : (h + 1) * width])
        row = jnp.concatenate(parts, axis=1)
        for i in range(out_ref.shape[0]):
            out_ref[i, h] = row


def pack(count, *matrices):
    rows = matrices[0].shape[0]
    return pl.pallas_call(
        pack_kernel,
        out_shape=jax.ShapeDtypeStruct((count, 2, rows, 512), jnp.bfloat16),
        name="pack",
        interpret=INTERPRET,
    )(*matrices)


def exact(a, b, dims):
    return lax.dot_general(
        a, b, (dims, ((), ())), precision=lax.Precision.HIGHEST, preferred_element_type=jnp.float32
    )


def retain_kernel(made_ref, turn_ref, decay_ref, send_ref, query_ref, within_ref):
    tokens = made_ref.shape[0]
    pair = made_ref[:, 256:384].astype(jnp.float32)
    lane = lax.broadcasted_iota(jnp.int32, pair.shape, 1)
    quarter = DH // 2
    ahead = pltpu.roll(pair, 2 * DH - quarter, 1)
    behind = pltpu.roll(pair, quarter, 1)
    crossed = jnp.where((lane & quarter) == 0, -ahead, behind)
    turned = pair * turn_ref[0] + crossed * turn_ref[1]
    query = turned[:, :DH]
    key = turned[:, DH:] * DH ** (-0.5)
    value = made_ref[:, 384:512].astype(jnp.float32)
    log_decay = decay_ref[0]
    offset = lax.broadcasted_iota(jnp.int32, (tokens, 1), 0).astype(jnp.float32)
    i = lax.broadcasted_iota(jnp.int32, (tokens, tokens), 0)
    j = lax.broadcasted_iota(jnp.int32, (tokens, tokens), 1)
    distance = (i - j).astype(jnp.float32)
    inside = jnp.where(i >= j, jnp.exp(log_decay * jnp.maximum(distance, 0.0)), 0.0)
    scores = exact(query, key, ((1,), (1,))) * inside
    within_ref[...] = exact(scores, value, ((1,), (0,)))
    query_ref[...] = query * jnp.exp(log_decay * (offset + 1.0))
    state = exact(key * jnp.exp(log_decay * (tokens - 1.0 - offset)), value, ((0,), (0,)))
    kv = made_ref[:, 128:256]
    for k in range(send_ref.shape[0]):
        send_ref[k, :tokens] = kv
        send_ref[k, tokens:] = state.astype(jnp.bfloat16)


def retain(made, turn, log_decay, count):
    tokens = made.shape[0]
    return pl.pallas_call(
        retain_kernel,
        in_specs=[VMEM, VMEM, SMEM],
        out_shape=[
            jax.ShapeDtypeStruct((count, tokens + DH, DV), jnp.bfloat16),
            jax.ShapeDtypeStruct((tokens, DH), jnp.float32),
            jax.ShapeDtypeStruct((tokens, DV), jnp.float32),
        ],
        name="retain",
        interpret=INTERPRET,
    )(made, turn, log_decay.reshape(1))


def pass_on_kernel(spread_ref, made_ref, weight_ref, send_ref):
    tokens = made_ref.shape[0]
    query = made_ref[:, : 2 * DH] * jnp.bfloat16(DH ** (-0.5))
    total = jnp.zeros((DH, DV), jnp.float32)
    for i in range(spread_ref.shape[0]):
        total = total + spread_ref[i, tokens:].astype(jnp.float32) * weight_ref[i]
    for k in range(send_ref.shape[0]):
        send_ref[k, :tokens] = query
        send_ref[k, tokens:] = total.astype(jnp.bfloat16)


def pass_on(spread, made, weight, count):
    return pl.pallas_call(
        pass_on_kernel,
        in_specs=[VMEM, VMEM, SMEM],
        out_shape=jax.ShapeDtypeStruct((count, *spread.shape[1:]), jnp.bfloat16),
        name="pass_on",
        interpret=INTERPRET,
    )(spread, made, weight)


def attend_kernel(
    where_ref, q_ref, mine_ref, other_ref, out_ref, k_ref, vt_ref, qt_ref, m_ref, l_ref, o_ref
):
    step = pl.program_id(0)
    z = where_ref[0]
    y = where_ref[1]
    keys = k_ref.shape[0]
    tokens = q_ref.shape[1]

    def prepare(key_ref, value_ref):
        for i in range(key_ref.shape[0]):
            at = slice(i * tokens, (i + 1) * tokens)
            k_ref[at] = key_ref[i, :tokens]
            vt_ref[:, at] = value_ref[i, :tokens].T

    @pl.when((step == 0) & (where_ref[2] == 0))
    def _():
        prepare(mine_ref, other_ref)

    @pl.when((step == 0) & (where_ref[2] != 0))
    def _():
        prepare(other_ref, mine_ref)

    def visit(start, count, masked):
        s = jnp.dot(k_ref[pl.ds(start, count)], qt_ref[...], preferred_element_type=jnp.float32)
        if masked:
            rows = lax.broadcasted_iota(jnp.int32, s.shape, 0) + start
            cols = lax.broadcasted_iota(jnp.int32, s.shape, 1) % tokens + y * tokens
            allowed = (rows // SEG) <= (cols // SEG)
            s = jnp.where(allowed, s, NEG)
        old = m_ref[...]
        top = jnp.maximum(old, jnp.max(s, axis=0, keepdims=True))
        w = jnp.exp(s - top)
        factor = jnp.exp(old - top)
        m_ref[...] = top
        l_ref[...] = l_ref[...] * factor + jnp.sum(w, axis=0, keepdims=True)
        o_ref[...] = o_ref[...] * factor + jnp.dot(
            vt_ref[:, pl.ds(start, count)],
            w.astype(jnp.bfloat16),
            preferred_element_type=jnp.float32,
        )

    @pl.when(step >= z)
    def _():
        q = q_ref[0]
        lane = lax.broadcasted_iota(jnp.int32, q.shape, 1)
        zero = jnp.zeros_like(q)
        q = jnp.concatenate([jnp.where(lane < DH, q, zero), jnp.where(lane < DH, zero, q)], axis=0)
        qt_ref[...] = q.T
        m_ref[...] = jnp.full(m_ref.shape, NEG, jnp.float32)
        l_ref[...] = jnp.zeros(l_ref.shape, jnp.float32)
        o_ref[...] = jnp.zeros(o_ref.shape, jnp.float32)

    @pl.when(step == z)
    def _():
        def body(i, _):
            visit(pl.multiple_of(i * KEYS, KEYS), KEYS, True)
            return 0

        lax.fori_loop(0, (y * tokens) // KEYS + 1, body, 0)

    @pl.when(step > z)
    def _():
        for start in range(0, keys, KEYS):
            visit(start, KEYS, False)

    @pl.when(step >= z)
    def _():
        total = l_ref[...]
        out_ref[0, :DV] = (o_ref[...] / total).astype(jnp.bfloat16)
        weight = m_ref[...] + jnp.log(total)
        high = weight.astype(jnp.bfloat16)
        rest = weight - high.astype(jnp.float32)
        middle = rest.astype(jnp.bfloat16)
        low = (rest - middle.astype(jnp.float32)).astype(jnp.bfloat16)
        pad = jnp.zeros((ROWS - DV - 3, weight.shape[1]), jnp.bfloat16)
        out_ref[0, DV:] = jnp.concatenate([high, middle, low, pad], axis=0)

    @pl.when(step < z)
    def _():
        out_ref[0, :DV] = jnp.zeros((DV, 2 * tokens), jnp.bfloat16)
        row = lax.broadcasted_iota(jnp.int32, (ROWS - DV, 2 * tokens), 0)
        out_ref[0, DV:] = jnp.where(row == 0, NEG, 0.0).astype(jnp.bfloat16)


def attend(where, along, mine, other, tokens):
    blocks = along.shape[0]
    count = mine.shape[0] * tokens

    def whole(shape):
        return pl.BlockSpec(shape, lambda g, w: (0,) * len(shape))

    return pl.pallas_call(
        attend_kernel,
        grid_spec=pltpu.PrefetchScalarGridSpec(
            num_scalar_prefetch=1,
            grid=(blocks,),
            in_specs=[
                pl.BlockSpec((1, tokens, 2 * DH), lambda g, w: (g, 0, 0)),
                whole(mine.shape),
                whole(other.shape),
            ],
            out_specs=pl.BlockSpec((1, ROWS, 2 * tokens), lambda g, w: (g, 0, 0)),
            scratch_shapes=[
                pltpu.VMEM((count, 2 * DH), jnp.bfloat16),
                pltpu.VMEM((DV, count), jnp.bfloat16),
                pltpu.VMEM((2 * DH, 2 * tokens), jnp.bfloat16),
                pltpu.VMEM((1, 2 * tokens), jnp.float32),
                pltpu.VMEM((1, 2 * tokens), jnp.float32),
                pltpu.VMEM((DV, 2 * tokens), jnp.float32),
            ],
        ),
        out_shape=jax.ShapeDtypeStruct((blocks, ROWS, 2 * tokens), jnp.bfloat16),
        compiler_params=pltpu.CompilerParams(dimension_semantics=("arbitrary",)),
        cost_estimate=pl.CostEstimate(
            flops=blocks * count * tokens * 4 * 256,
            bytes_accessed=blocks * tokens * 1024 + count * 512,
            transcendentals=blocks * count * tokens * 2,
        ),
        name="attend",
        interpret=INTERPRET,
    )(where, along, mine, other)


def finish_kernel(
    parts_ref, mix_ref, gain_ref, spread_ref, along_ref, weight_ref, query_ref, within_ref, out_ref
):
    blocks = parts_ref.shape[0]
    tokens = query_ref.shape[0]
    logs = []
    for i in range(blocks):
        rows = parts_ref[i, DV:].astype(jnp.float32)
        logs.append(rows[0:1] + rows[1:2] + rows[2:3])
    top = functools.reduce(jnp.maximum, logs)
    shares = [jnp.exp(log - top) for log in logs]
    total = functools.reduce(jnp.add, shares)
    acc = jnp.zeros((DV, 2 * tokens), jnp.float32)
    for i in range(blocks):
        acc = acc + parts_ref[i, :DV].astype(jnp.float32) * (shares[i] / total)
    att = acc[:, :tokens] - mix_ref[0] * acc[:, tokens:]
    att = att * lax.rsqrt(jnp.mean(att * att, axis=0, keepdims=True) + EPSILON)
    att = (att.T * gain_ref[0:1]).astype(jnp.bfloat16)
    carried = jnp.zeros((DH, DV), jnp.float32)
    chips = spread_ref.shape[0]
    for i in range(chips):
        carried = carried + spread_ref[i, tokens:].astype(jnp.float32) * weight_ref[i]
    for i in range(blocks):
        carried = carried + along_ref[i, tokens:].astype(jnp.float32) * weight_ref[chips + i]
    ret = within_ref[...] + exact(query_ref[...], carried, ((1,), (0,)))
    ret = ret * lax.rsqrt(jnp.mean(ret * ret, axis=1, keepdims=True) + EPSILON)
    ret = (ret * gain_ref[1:2]).astype(jnp.bfloat16)
    half = tokens // 2
    for i in range(2):
        out_ref[i, :, :DV] = att[i * half : (i + 1) * half]
        out_ref[i, :, DV:] = ret[i * half : (i + 1) * half]


def finish(parts, mixing, gains, spread, along, weights, query, within):
    tokens = query.shape[0]
    return pl.pallas_call(
        finish_kernel,
        in_specs=[VMEM, SMEM, VMEM, VMEM, VMEM, SMEM, VMEM, VMEM],
        out_shape=jax.ShapeDtypeStruct((2, tokens // 2, 2 * DV), jnp.bfloat16),
        name="finish",
        interpret=INTERPRET,
    )(parts, mixing.reshape(1), gains, spread, along, weights, query, within)


def decay_log(head, length):
    pair = (head // 2).astype(jnp.float32)
    quick = jnp.log1p(-jnp.exp2(-5.0 - pair / 4.0))
    slow = jnp.log1p(-1.0 / (length * (1.0 + pair)))
    return jnp.where(head % 2 == 0, quick, slow)


def layer(
    features,
    norm_gain,
    att_query,
    att_key,
    att_value,
    att_lambda,
    att_gain,
    ret_query,
    ret_key,
    ret_value,
    ret_gain,
    out_weight,
):
    z = lax.axis_index(Z)
    y = lax.axis_index("y")
    c = lax.axis_index("c")
    x = lax.axis_index("tp")
    ny = lax.axis_size("y")
    nz = lax.axis_size(Z)
    nl = lax.axis_size("zl")
    groups = lax.axis_size("tp")
    chip = z * ny + y
    tokens = 2 * features.shape[0]

    sent = pack(2 * ny, att_query, att_key, att_value, ret_query, ret_key, ret_value)
    rows, width = sent.shape[2:]
    sent = sent.reshape(4 * ny, rows, width)
    even = jnp.arange(0, DH, 2).astype(jnp.float32)
    small = (even, jnp.arange(ny), jnp.arange(nz), chip, z, y, c, x)
    sent, small = lax.optimization_barrier((sent, small))
    w_own = lax.all_to_all(sent, ("zh", "y", "c"), 0, 0, tiled=True)
    w_own = w_own.reshape(4 * ny * rows, width)
    inputs = (features, norm_gain, att_lambda, att_gain, ret_gain)
    w_own, inputs, small = lax.optimization_barrier((w_own, inputs, small))
    features, norm_gain, att_lambda, att_gain, ret_gain = inputs
    even, ys, zs, chip, z, y, c, x = small
    w_before, w_after, w_low, w_high = two_steps(w_own, 2 * ny * rows)

    residues = [(z + k) % nl for k in (0, nl - 1, 1, 2)]

    pieces = [features] + [
        lax.ppermute(features, "tp", [(i, (i + k) % groups) for i in range(groups)])
        for k in range(1, groups)
    ]
    gathered = jnp.zeros((groups, *features.shape), features.dtype)
    for k, piece in enumerate(pieces):
        gathered = lax.dynamic_update_index_in_dim(gathered, piece, (x - k) % groups, 0)
    floats = gathered.astype(jnp.float32)
    mean_sq = jnp.sum(floats * floats, axis=(0, 2)) / norm_gain.shape[0]
    gain = norm_gain.reshape(groups, 1, -1)
    scaled = floats * lax.rsqrt(mean_sq + EPSILON)[None, :, None] * gain
    scaled = scaled.astype(jnp.bfloat16)
    per_tp = nz // groups
    wide = scaled.shape[2] // per_tp
    by_z = jnp.stack([scaled[i // per_tp][:, (i % per_tp) * wide :][:, :wide] for i in range(nz)])
    across = swapped(by_z)
    both = jnp.stack([jnp.where(c == 0, by_z, across), jnp.where(c == 0, across, by_z)])

    log_decay = decay_log(x * 2 + c, float(nz * ny * tokens))
    positions = (chip * tokens + jnp.arange(tokens)).astype(jnp.float32)
    inverse = 10000.0 ** (-even / DH)
    angles = positions[:, None] * inverse[None, :]
    turn = jnp.stack([jnp.tile(jnp.cos(angles), (1, 4)), jnp.tile(jnp.sin(angles), (1, 4))])
    span = log_decay * tokens
    to_end = jnp.exp(span * (ny - 1 - ys).astype(jnp.float32))
    y_steps = jnp.maximum(y - 1 - ys, 0).astype(jnp.float32)
    z_steps = jnp.maximum(ny * (z - 1 - zs) + y, 0).astype(jnp.float32)
    before = jnp.concatenate(
        [
            jnp.where(ys < y, jnp.exp(span * y_steps), 0.0),
            jnp.where(zs < z, jnp.exp(span * z_steps), 0.0),
        ]
    )
    where = jnp.stack([z, y, c]).astype(jnp.int32)
    mixing = lax.dynamic_index_in_dim(att_lambda, c, 0, keepdims=False)
    gains = jnp.stack([att_gain, ret_gain])

    def made_by(k, high, matrix):
        left = lax.dynamic_index_in_dim(both, high * nl + residues[k], 1, keepdims=False)
        left = left.reshape(tokens, wide)
        return jnp.dot(left, matrix, preferred_element_type=jnp.float32)

    made = made_by(0, 0, w_own[:wide]) + made_by(0, 1, w_own[wide:])
    made = made + made_by(1, 0, w_before[:wide]) + made_by(1, 1, w_before[wide:])
    made = made + made_by(2, 0, w_after[:wide]) + made_by(2, 1, w_after[wide:])
    made = made + made_by(3, 0, w_low) + made_by(3, 1, w_high)
    made = made.astype(jnp.bfloat16)
    made, turn, log_decay, to_end, before, where, mixing, gains = lax.optimization_barrier(
        (made, turn, log_decay, to_end, before, where, mixing, gains)
    )

    send, query, within = retain(made, turn, log_decay, ny)
    spread = lax.all_to_all(send, "y", 0, 0, tiled=True)
    send = pass_on(spread, made, to_end, nz)
    along = lax.all_to_all(send, Z, 0, 0, tiled=True)
    spread, along = lax.optimization_barrier((spread, along))
    parts = attend(where, along, spread, swapped(spread), tokens)
    parts = lax.all_to_all(parts, Z, 0, 0, tiled=True)

    heads = finish(parts, mixing, gains, spread, along, before, query, within)
    heads = lax.all_to_all(heads, "c", 0, 0, tiled=True)
    joined = jnp.concatenate(
        [heads[0, :, :DV], heads[1, :, :DV], heads[0, :, DV:], heads[1, :, DV:]], axis=1
    )
    partial = jnp.dot(
        joined, out_weight.reshape(-1, out_weight.shape[2]), preferred_element_type=jnp.float32
    ).astype(jnp.bfloat16)
    partial = lax.all_to_all(
        partial.reshape(groups, -1, partial.shape[1]), "tp", 0, 0, tiled=True
    )
    return jnp.sum(partial.astype(jnp.float32), axis=0)


def solution(mesh):
    devices = mesh.devices
    torus = Mesh(devices.reshape(2, 4, -1, 2, devices.shape[-1]), SP_TP)
    return jax.shard_map(
        layer,
        mesh=torus,
        in_specs=(
            P(SP, "tp"),
            P(),
            P(SP, "tp"),
            P(SP, "tp"),
            P(SP, "tp"),
            P("tp"),
            P(),
            P(SP, "tp"),
            P(SP, "tp"),
            P(SP, "tp"),
            P(),
            P(None, "tp", None),
        ),
        out_specs=P(SP_TP, None),
        check_vma=False,
    )
```

time: 222 us -> 231 us (1.041)
  blocking collectives: 37.4 us -> 138 us
  waiting for transfers between devices: 99.1 us -> 6.84 us
  Pallas kernels: 22.6 us -> 31.3 us
  starting transfers between devices: 36 us -> 31 us
    all_to_all x1 -> x4, blocking collectives: 21 us -> 121 us  [the longest x1 37.7 us: layer(): w_own = lax.all_to_all(sent, ('zh', 'y', 'c'), 0, 0, tiled=True)]
    all_to_all x4 -> x0, waiting for transfers between devices: 93.4 us -> none  [the longest x3 66.7 us: to_all(): lax.all_to_all(jnp.broadcast_to(value[None], (count, *value.shape)), axes...]
    all_to_all x4 -> x0, starting transfers between devices: 19.9 us -> none  [the longest x3 16.2 us: to_all(): lax.all_to_all(jnp.broadcast_to(value[None], (count, *value.shape)), axes...]
    ppermute x0 -> x4, starting transfers between devices: none -> 10.7 us  [shifted(): lax.ppermute(value, Z, [(i, (i + step) % count) for i in range(count)])]
    pallas_call x1 -> x4, Pallas kernels: 2.38 us -> 10.8 us  [the longest x1 3.71 us: finish(): pl.pallas_call(finish_kernel, in_specs=[VMEM, SMEM, VMEM, VMEM, VMEM, SME...]
    ppermute x2, starting transfers between devices: 5.54 us -> 11 us  [swapped(): return lax.ppermute(value, 'c', [(0, 1), (1, 0)])]
    ppermute x0 -> x4, waiting for transfers between devices: none -> 5 us  [shifted(): lax.ppermute(value, Z, [(i, (i + step) % count) for i in range(count)])]
    broadcast_in_dim x5 -> x0, local copies, waits for them, and re-layouts: 4.58 us -> none  [the longest x3 3.37 us: to_all(): jnp.broadcast_to(value[None], (count, *value.shape))]
  transfers between devices with their start and end apart: 9 -> 9, of which waited for: 8 -> 2; matrix products, arithmetic and copies ran while one was open for 4% -> 8% of each run, Pallas kernels for 0% -> 0%
where the time goes in v1:
time: 231 us; the launch traced here: 229 us
  blocking collectives  138 us (60%)
  Pallas kernels  31.3 us (14%)
  starting transfers between devices  31 us (13%)
  local copies, waits for them, and re-layouts  11.1 us (5%)
  waiting for transfers between devices  6.84 us (3%)
  other arithmetic  5.74 us (2%)
  matrix products  4.9 us (2%)
    all_to_all x1, blocking collectives, layer(): w_own = lax.all_to_all(sent, ('zh', 'y', 'c'), 0, 0, tiled=True)  37.7 us
    all_to_all x1, blocking collectives, layer(): parts = lax.all_to_all(parts, Z, 0, 0, tiled=True)  36.2 us
    all_to_all x1, blocking collectives, layer(): along = lax.all_to_all(send, Z, 0, 0, tiled=True)  23.9 us
    all_to_all x1, blocking collectives, layer(): spread = lax.all_to_all(send, 'y', 0, 0, tiled=True)  23.3 us
    pallas_call x1, Pallas kernels, attend(): pl.pallas_call(attend_kernel, grid_spec=pltpu.PrefetchScalarGridSpec(num_...  20.5 us
    all_to_all x1, blocking collectives, layer(): lax.all_to_all(partial.reshape(groups, -1, partial.shape[1]), 'tp', 0, 0,...  11.8 us
    ppermute x2, starting transfers between devices, swapped(): return lax.ppermute(value, 'c', [(0, 1), (1, 0)])  11 us
    ppermute x4, starting transfers between devices, shifted(): lax.ppermute(value, Z, [(i, (i + step) % count) for i in range(count)])  10.7 us
  transfers between devices with their start and end apart: 9, of which 2 were waited for; matrix products, arithmetic and copies ran while one was open for 8% of the time, Pallas kernels for 0%

profile of v1, /device:TPU:1, one launch (start us, length us, event | category | flops | bytes accessed | tf_op | source)
XLA Modules:
  0.0 229.4 jit_solution(17907527538605325909)
XLA Ops:
  0.0 1.9 pack.1
  1.9 37.7 %all_to_all.30 = bf16[32,16,512]{2,1,0:T(8,128)(2,1)S(1)} all-to-all(bf16[32,16,512]{2,1,0:T(8,128)(2,1)} %bitcast.98), channel_id=1, replica_groups=mesh['zh'=2,'zl'=4,'y'=8,'c'=2,'tp'=4] {'zh','y','c'}, dimensions={0} | all-to-all | bytes 1048576 | tf_op jit(solution)/shard_map/all_to_all | solution.py:343
  39.6 4.4 %collective-permute-start.2 = (bf16[128,512]{1,0:T(8,128)(2,1)}, bf16[128,512]{1,0:T(8,128)(2,1)}, u32[]{:S(2)}, u32[]{:S(2)}) collective-permute-start(bf16[128,512]{1,0:T(8,128)(2,1)} %param.12), channel_id=1, source_target_pairs={{0,3},{1,0},{2,1},{3,2},{4,7},{5,4},{6,5},{7,6},{8,11},{9,8},{10,9... | collective-permute-start | bytes 393224 | tf_op jit(solution)/shard_map/ppermute | solution.py:354
  44.0 2.4 %collective-permute-start.1 = (bf16[128,512]{1,0:T(8,128)(2,1)}, bf16[128,512]{1,0:T(8,128)(2,1)}, u32[]{:S(2)}, u32[]{:S(2)}) collective-permute-start(bf16[128,512]{1,0:T(8,128)(2,1)} %param.12), channel_id=1, source_target_pairs={{0,2},{1,3},{2,0},{3,1},{4,6},{5,7},{6,4},{7,5},{8,10},{9,11},{10,... | collective-permute-start | bytes 393224 | tf_op jit(solution)/shard_map/ppermute | solution.py:354
  46.4 2.5 %collective-permute-start = (bf16[128,512]{1,0:T(8,128)(2,1)}, bf16[128,512]{1,0:T(8,128)(2,1)}, u32[]{:S(2)}, u32[]{:S(2)}) collective-permute-start(bf16[128,512]{1,0:T(8,128)(2,1)} %param.12), channel_id=1, source_target_pairs={{0,1},{1,2},{2,3},{3,0},{4,5},{5,6},{6,7},{7,4},{8,9},{9,10},{10,1... | collective-permute-start | bytes 393224 | tf_op jit(solution)/shard_map/ppermute | solution.py:354
  48.9 2.3 collective-permute-start.5
  51.2 3.0 %collective-permute-start.4 = (bf16[512,512]{1,0:T(8,128)(2,1)S(1)}, bf16[512,512]{1,0:T(8,128)(2,1)}, u32[]{:S(2)}, u32[]{:S(2)}) collective-permute-start(bf16[512,512]{1,0:T(8,128)(2,1)S(1)} %bitcast.95), channel_id=1, source_target_pairs={{0,64},{64,128},{128,192},{192,256},{256,320},{320,384},{384,448},... | collective-permute-start | bytes 1572872 | tf_op jit(solution)/shard_map/ppermute | solution.py:32
  63.7 5.4 %collective-permute-start.3 = (bf16[8,128,256]{2,1,0:T(8,128)(2,1)}, bf16[8,128,256]{2,1,0:T(8,128)(2,1)}, u32[]{:S(2)}, u32[]{:S(2)}) collective-permute-start(bf16[8,128,256]{2,1,0:T(8,128)(2,1)} %fusion.31), channel_id=1, source_target_pairs={{0,4},{4,0},{1,5},{5,1},{2,6},{6,2},{3,7},{7,3},{8,12},{12,8},{9,1... | collective-permute-start | bytes 1572872 | tf_op jit(solution)/shard_map/ppermute | solution.py:27
  69.8 1.3 dynamic_slice.37
  73.6 3.5 %collective-permute-start.7 = (bf16[256,512]{1,0:T(8,128)(2,1)S(1)}, bf16[256,512]{1,0:T(8,128)(2,1)S(1)}, u32[]{:S(2)}, u32[]{:S(2)}) collective-permute-start(bf16[256,512]{1,0:T(8,128)(2,1)S(1)} %slice.109), channel_id=1, source_target_pairs={{0,448},{64,0},{128,64},{192,128},{256,192},{320,256},{384,320},{4... | collective-permute-start | bytes 786440 | tf_op jit(solution)/shard_map/ppermute | solution.py:32
  78.1 1.9 collective-permute-start.6
  83.8 5.0 %collective-permute-done.6 = bf16[256,512]{1,0:T(8,128)(2,1)S(1)} collective-permute-done((bf16[256,512]{1,0:T(8,128)(2,1)S(1)}, bf16[256,512]{1,0:T(8,128)(2,1)S(1)}, u32[]{:S(2)}, u32[]{:S(2)}) %collective-permute-start.6) | collective-permute-done | bytes 262176 | tf_op jit(solution)/shard_map/ppermute | solution.py:32
  89.0 2.0 fusion.5.made_ref
  90.9 3.1 %retain.1 = (bf16[8,320,128]{2,1,0:T(8,128)(2,1)}, f32[256,64]{1,0:T(8,128)}, f32[256,128]{1,0:T(8,128)}) custom-call(bf16[256,512]{1,0:T(8,128)(2,1)} %fusion.5.made_ref, f32[2,256,128]{2,1,0:T(8,128)} %pad_maximum_fusion.turn_ref, f32[1]{0:T(128)} %bitcast.36.decay_ref), custom_call_target="tpu_custom_call" | custom-call | tf_op jit(solution)/shard_map/retain/pallas_call | solution.py:103
  94.1 23.3 %all_to_all.31.spread_ref.mine_ref = bf16[8,320,128]{2,1,0:T(8,128)(2,1)} all-to-all(bf16[8,320,128]{2,1,0:T(8,128)(2,1)} %get-tuple-element.68), channel_id=1, replica_groups=mesh['zh'=2,'zl'=4,'y'=8,'c'=2,'tp'=4] {'y'}, dimensions={0} | all-to-all | bytes 1310720 | tf_op jit(solution)/shard_map/all_to_all | solution.py:405
  117.4 2.1 pass_on.1
  119.5 23.9 %all_to_all.32.q_ref.along_ref = bf16[8,320,128]{2,1,0:T(8,128)(2,1)} all-to-all(bf16[8,320,128]{2,1,0:T(8,128)(2,1)} %pass_on.1), channel_id=1, replica_groups=mesh['zh'=2,'zl'=4,'y'=8,'c'=2,'tp'=4] {'zh','zl'}, dimensions={0} | all-to-all | bytes 1310720 | tf_op jit(solution)/shard_map/all_to_all | solution.py:407
  143.4 5.7 %collective-permute-start.8 = (bf16[8,320,128]{2,1,0:T(8,128)(2,1)S(1)}, bf16[8,320,128]{2,1,0:T(8,128)(2,1)}, u32[]{:S(2)}, u32[]{:S(2)}) collective-permute-start(bf16[8,320,128]{2,1,0:T(8,128)(2,1)S(1)} %copy-done.1), channel_id=1, source_target_pairs={{0,4},{4,0},{1,5},{5,1},{2,6},{6,2},{3,7},{7,3},{8,12},{12,8},{9,1... | collective-permute-start | bytes 1966088 | tf_op jit(solution)/shard_map/ppermute | solution.py:27
  149.1 1.8 collective-permute-done.8.other_ref
  150.9 20.5 %attend.1 = bf16[8,144,512]{2,1,0:T(8,128)(2,1)} custom-call(s32[3]{0:T(128)} %pad_add_fusion.where_ref, bf16[8,320,128]{2,1,0:T(8,128)(2,1)} %all_to_all.32.q_ref.along_ref, bf16[8,320,128]{2,1,0:T(8,128)(2,1)} %all_to_all.31.spread_ref.mine_ref, bf16[8,320,128]{2,1,0:T(8,128)(2,1)} %collective-permute-done.8.other_ref), custom_call_target="tpu_custom_call" | custom-call | flops 4294967296 | bytes 3145728 | tf_op jit(solution)/shard_map/attend/pallas_call | solution.py:229
  171.4 36.2 %all_to_all.33.parts_ref = bf16[8,144,512]{2,1,0:T(8,128)(2,1)} all-to-all(bf16[8,144,512]{2,1,0:T(8,128)(2,1)} %attend.1), channel_id=1, replica_groups=mesh['zh'=2,'zl'=4,'y'=8,'c'=2,'tp'=4] {'zh','zl'}, dimensions={0} | all-to-all | bytes 2359296 | tf_op jit(solution)/shard_map/all_to_all | solution.py:410
  207.7 3.7 %finish.1 = bf16[2,128,256]{2,1,0:T(8,128)(2,1)} custom-call(bf16[8,144,512]{2,1,0:T(8,128)(2,1)} %all_to_all.33.parts_ref, f32[1]{0:T(128)} %bitcast.37.mix_ref, f32[2,128]{1,0:T(2,128)} %pad_maximum_fusion.1.gain_ref, bf16[8,320,128]{2,1,0:T(8,128)(2,1)} %all_to_all.31.spread_ref.mine_ref, bf16[8,320,128]{2,1,0:T(8,128)(2,1)} %all_to_all.32.q_ref.along_ref, ...), custom_call_target="tpu_custom_call" | custom-call | tf_op jit(solution)/shard_map/finish/pallas_call | solution.py:296
  211.4 5.0 %all_to_all.34 = bf16[2,128,256]{2,1,0:T(8,128)(2,1)S(1)} all-to-all(bf16[2,128,256]{2,1,0:T(8,128)(2,1)} %finish.1), channel_id=1, replica_groups=mesh['zh'=2,'zl'=4,'y'=8,'c'=2,'tp'=4] {'c'}, dimensions={0} | all-to-all | bytes 262144 | tf_op jit(solution)/shard_map/all_to_all | solution.py:413
  216.8 11.8 %all_to_all.35 = bf16[4,32,2048]{2,1,0:T(8,128)(2,1)S(1)} all-to-all(bf16[4,32,2048]{2,1,0:T(8,128)(2,1)S(1)} %bitcast.99), channel_id=1, replica_groups=mesh['zh'=2,'zl'=4,'y'=8,'c'=2,'tp'=4] {'tp'}, dimensions={0} | all-to-all | bytes 1048576 | tf_op jit(solution)/shard_map/all_to_all | solution.py:420
  (64 shorter events, 18.5 us)
Async XLA Ops:
  0.0 216.4 %copy-start = (bf16[2,256,2048]{2,1,0:T(8,128)(2,1)S(1)}, bf16[2,256,2048]{2,1,0:T(8,128)(2,1)}, u32[]{:S(2)}) copy-start(bf16[2,256,2048]{2,1,0:T(8,128)(2,1)} %param.23) | copy-start | bytes 6291460
  0.0 55.2 %copy-start.2 = (bf16[128,512]{1,0:T(8,128)(2,1)S(1)}, bf16[128,512]{1,0:T(8,128)(2,1)}, u32[]{:S(2)}) copy-start(bf16[128,512]{1,0:T(8,128)(2,1)} %param.12) | copy-start | bytes 393220
  39.6 17.7 %collective-permute-start.2 = (bf16[128,512]{1,0:T(8,128)(2,1)}, bf16[128,512]{1,0:T(8,128)(2,1)}, u32[]{:S(2)}, u32[]{:S(2)}) collective-permute-start(bf16[128,512]{1,0:T(8,128)(2,1)} %param.12), channel_id=1, source_target_pairs={{0,3},{1,0},{2,1},{3,2},{4,7},{5,4},{6,5},{7,6},{8,11},{9,8},{10,9... | collective-permute-start | bytes 393224 | tf_op jit(solution)/shard_map/ppermute | solution.py:354
  44.0 12.4 %collective-permute-start.1 = (bf16[128,512]{1,0:T(8,128)(2,1)}, bf16[128,512]{1,0:T(8,128)(2,1)}, u32[]{:S(2)}, u32[]{:S(2)}) collective-permute-start(bf16[128,512]{1,0:T(8,128)(2,1)} %param.12), channel_id=1, source_target_pairs={{0,2},{1,3},{2,0},{3,1},{4,6},{5,7},{6,4},{7,5},{8,10},{9,11},{10,... | collective-permute-start | bytes 393224 | tf_op jit(solution)/shard_map/ppermute | solution.py:354
  46.4 9.0 %collective-permute-start = (bf16[128,512]{1,0:T(8,128)(2,1)}, bf16[128,512]{1,0:T(8,128)(2,1)}, u32[]{:S(2)}, u32[]{:S(2)}) collective-permute-start(bf16[128,512]{1,0:T(8,128)(2,1)} %param.12), channel_id=1, source_target_pairs={{0,1},{1,2},{2,3},{3,0},{4,5},{5,6},{6,7},{7,4},{8,9},{9,10},{10,1... | collective-permute-start | bytes 393224 | tf_op jit(solution)/shard_map/ppermute | solution.py:354
  48.9 24.7 %collective-permute-start.5 = (bf16[512,512]{1,0:T(8,128)(2,1)S(1)}, bf16[512,512]{1,0:T(8,128)(2,1)S(1)}, u32[]{:S(2)}, u32[]{:S(2)}) collective-permute-start(bf16[512,512]{1,0:T(8,128)(2,1)S(1)} %bitcast.94), channel_id=1, source_target_pairs={{0,448},{64,0},{128,64},{192,128},{256,192},{320,256},{384,320},{4... | collective-permute-start | bytes 1572872 | tf_op jit(solution)/shard_map/ppermute | solution.py:32
  51.2 25.9 %collective-permute-start.4 = (bf16[512,512]{1,0:T(8,128)(2,1)S(1)}, bf16[512,512]{1,0:T(8,128)(2,1)}, u32[]{:S(2)}, u32[]{:S(2)}) collective-permute-start(bf16[512,512]{1,0:T(8,128)(2,1)S(1)} %bitcast.95), channel_id=1, source_target_pairs={{0,64},{64,128},{128,192},{192,256},{256,320},{320,384},{384,448},... | collective-permute-start | bytes 1572872 | tf_op jit(solution)/shard_map/ppermute | solution.py:32
  58.4 13.9 %copy-start.3 = (f32[128]{0:T(128)S(1)}, f32[128]{0:T(128)}, u32[]{:S(2)}) copy-start(f32[128]{0:T(128)} %param.22) | copy-start | bytes 1540
  58.4 13.9 %copy-start.4 = (f32[128]{0:T(128)S(1)}, f32[128]{0:T(128)}, u32[]{:S(2)}) copy-start(f32[128]{0:T(128)} %param.18) | copy-start | bytes 1540
  63.7 16.3 %collective-permute-start.3 = (bf16[8,128,256]{2,1,0:T(8,128)(2,1)}, bf16[8,128,256]{2,1,0:T(8,128)(2,1)}, u32[]{:S(2)}, u32[]{:S(2)}) collective-permute-start(bf16[8,128,256]{2,1,0:T(8,128)(2,1)} %fusion.31), channel_id=1, source_target_pairs={{0,4},{4,0},{1,5},{5,1},{2,6},{6,2},{3,7},{7,3},{8,12},{12,8},{9,1... | collective-permute-start | bytes 1572872 | tf_op jit(solution)/shard_map/ppermute | solution.py:27
  73.6 9.9 %collective-permute-start.7 = (bf16[256,512]{1,0:T(8,128)(2,1)S(1)}, bf16[256,512]{1,0:T(8,128)(2,1)S(1)}, u32[]{:S(2)}, u32[]{:S(2)}) collective-permute-start(bf16[256,512]{1,0:T(8,128)(2,1)S(1)} %slice.109), channel_id=1, source_target_pairs={{0,448},{64,0},{128,64},{192,128},{256,192},{320,256},{384,320},{4... | collective-permute-start | bytes 786440 | tf_op jit(solution)/shard_map/ppermute | solution.py:32
  78.1 10.7 %collective-permute-start.6 = (bf16[256,512]{1,0:T(8,128)(2,1)S(1)}, bf16[256,512]{1,0:T(8,128)(2,1)S(1)}, u32[]{:S(2)}, u32[]{:S(2)}) collective-permute-start(bf16[256,512]{1,0:T(8,128)(2,1)S(1)} %slice.106), channel_id=1, source_target_pairs={{0,64},{64,128},{128,192},{192,256},{256,320},{320,384},{384,448},... | collective-permute-start | bytes 786440 | tf_op jit(solution)/shard_map/ppermute | solution.py:32
  117.4 26.0 %copy-start.1 = (bf16[8,320,128]{2,1,0:T(8,128)(2,1)S(1)}, bf16[8,320,128]{2,1,0:T(8,128)(2,1)}, u32[]{:S(2)}) copy-start(bf16[8,320,128]{2,1,0:T(8,128)(2,1)} %all_to_all.31.spread_ref.mine_ref) | copy-start | bytes 1966084
  143.4 7.5 %collective-permute-start.8 = (bf16[8,320,128]{2,1,0:T(8,128)(2,1)S(1)}, bf16[8,320,128]{2,1,0:T(8,128)(2,1)}, u32[]{:S(2)}, u32[]{:S(2)}) collective-permute-start(bf16[8,320,128]{2,1,0:T(8,128)(2,1)S(1)} %copy-done.1), channel_id=1, source_target_pairs={{0,4},{4,0},{1,5},{5,1},{2,6},{6,2},{3,7},{7,3},{8,12},{12,8},{9,1... | collective-permute-start | bytes 1966088 | tf_op jit(solution)/shard_map/ppermute | solution.py:27

commit v2 on v1

--- a/solution.py
+++ b/solution.py
@@ -18,6 +18,7 @@
 NEG = -1e30
 KEYS = 512
 ROWS = 144
+MIB = 1 << 20
 VMEM = pl.BlockSpec(memory_space=pltpu.VMEM)
 SMEM = pl.BlockSpec(memory_space=pltpu.SMEM)
 INTERPRET = False
@@ -59,20 +60,85 @@
     return pl.pallas_call(
         pack_kernel,
         out_shape=jax.ShapeDtypeStruct((count, 2, rows, 512), jnp.bfloat16),
+        compiler_params=pltpu.CompilerParams(vmem_limit_bytes=4 * MIB),
         name="pack",
         interpret=INTERPRET,
     )(*matrices)
 
 
-def exact(a, b, dims):
+def rounded(a, b, dims):
     return lax.dot_general(
-        a, b, (dims, ((), ())), precision=lax.Precision.HIGHEST, preferred_element_type=jnp.float32
+        a.astype(jnp.bfloat16),
+        b.astype(jnp.bfloat16),
+        (dims, ((), ())),
+        preferred_element_type=jnp.float32,
     )
 
 
-def retain_kernel(made_ref, turn_ref, decay_ref, send_ref, query_ref, within_ref):
-    tokens = made_ref.shape[0]
-    pair = made_ref[:, 256:384].astype(jnp.float32)
+def norm_kernel(*refs):
+    *piece_refs, place_ref, gain_ref, out_ref = refs
+    groups = len(piece_refs)
+    blocks, _, wide = out_ref.shape
+    per_tp = blocks // groups
+    total = 0.0
+    for ref in piece_refs:
+        floats = ref[...].astype(jnp.float32)
+        total = total + jnp.sum(floats * floats, axis=1, keepdims=True)
+    scale = lax.rsqrt(total / (blocks * wide) + EPSILON)
+    for k, ref in enumerate(piece_refs):
+        for i in range(per_tp):
+            at = place_ref[k] * per_tp + i
+            part = ref[:, i * wide : (i + 1) * wide].astype(jnp.float32)
+            out_ref[at] = (part * scale * gain_ref[at]).astype(jnp.bfloat16)
+
+
+def norm(pieces, place, gain, blocks):
+    rows, width = pieces[0].shape
+    wide = width * len(pieces) // blocks
+    return pl.pallas_call(
+        norm_kernel,
+        in_specs=[VMEM] * len(pieces) + [SMEM, VMEM],
+        out_shape=jax.ShapeDtypeStruct((blocks, rows, wide), jnp.bfloat16),
+        compiler_params=pltpu.CompilerParams(vmem_limit_bytes=6 * MIB),
+        name="norm",
+        interpret=INTERPRET,
+    )(*pieces, place, gain.reshape(blocks, 1, wide))
+
+
+def project_kernel(
+    own_ref,
+    across_ref,
+    w_own_ref,
+    w_before_ref,
+    w_after_ref,
+    w_low_ref,
+    w_high_ref,
+    place_ref,
+    turn_ref,
+    decay_ref,
+    send_ref,
+    att_ref,
+    query_ref,
+    within_ref,
+):
+    half, wide = own_ref.shape[1:]
+    tokens = 2 * half
+    low, high = slice(0, wide), slice(wide, 2 * wide)
+    weights = [(w_own_ref, low), (w_own_ref, high), (w_before_ref, low), (w_before_ref, high)]
+    weights += [(w_after_ref, low), (w_after_ref, high), (w_low_ref, low), (w_high_ref, low)]
+    made = jnp.zeros((tokens, w_own_ref.shape[1]), jnp.float32)
+    for k, (ref, at) in enumerate(weights):
+        block = place_ref[1 + k]
+        left = jnp.concatenate([own_ref[block], across_ref[block]], axis=0)
+        made = made + jnp.dot(left, ref[at], preferred_element_type=jnp.float32)
+    first = place_ref[0] == 0
+    made = jnp.concatenate(
+        [jnp.where(first, made[:half], made[half:]), jnp.where(first, made[half:], made[:half])],
+        axis=0,
+    ).astype(jnp.bfloat16)
+    att_ref[...] = made[:, : 2 * DH] * jnp.bfloat16(DH ** (-0.5))
+
+    pair = made[:, 256:384].astype(jnp.float32)
     lane = lax.broadcasted_iota(jnp.int32, pair.shape, 1)
     quarter = DH // 2
     ahead = pltpu.roll(pair, 2 * DH - quarter, 1)
@@ -81,57 +147,59 @@
     turned = pair * turn_ref[0] + crossed * turn_ref[1]
     query = turned[:, :DH]
     key = turned[:, DH:] * DH ** (-0.5)
-    value = made_ref[:, 384:512].astype(jnp.float32)
+    value = made[:, 384:512]
     log_decay = decay_ref[0]
     offset = lax.broadcasted_iota(jnp.int32, (tokens, 1), 0).astype(jnp.float32)
+    state = rounded(key * jnp.exp(log_decay * (tokens - 1.0 - offset)), value, ((0,), (0,)))
+    state = state.astype(jnp.bfloat16)
+    for k in range(send_ref.shape[0]):
+        send_ref[k, :tokens] = made[:, 128:256]
+        send_ref[k, tokens:] = state
     i = lax.broadcasted_iota(jnp.int32, (tokens, tokens), 0)
     j = lax.broadcasted_iota(jnp.int32, (tokens, tokens), 1)
     distance = (i - j).astype(jnp.float32)
     inside = jnp.where(i >= j, jnp.exp(log_decay * jnp.maximum(distance, 0.0)), 0.0)
-    scores = exact(query, key, ((1,), (1,))) * inside
-    within_ref[...] = exact(scores, value, ((1,), (0,)))
+    scores = rounded(query, key, ((1,), (1,))) * inside
+    within_ref[...] = rounded(scores, value, ((1,), (0,)))
     query_ref[...] = query * jnp.exp(log_decay * (offset + 1.0))
-    state = exact(key * jnp.exp(log_decay * (tokens - 1.0 - offset)), value, ((0,), (0,)))
-    kv = made_ref[:, 128:256]
-    for k in range(send_ref.shape[0]):
-        send_ref[k, :tokens] = kv
-        send_ref[k, tokens:] = state.astype(jnp.bfloat16)
-
-
-def retain(made, turn, log_decay, count):
-    tokens = made.shape[0]
+
+
+def project(own, across, weights, place, turn, log_decay, count):
+    tokens = 2 * own.shape[1]
     return pl.pallas_call(
-        retain_kernel,
-        in_specs=[VMEM, VMEM, SMEM],
+        project_kernel,
+        in_specs=[VMEM] * 7 + [SMEM, VMEM, SMEM],
         out_shape=[
             jax.ShapeDtypeStruct((count, tokens + DH, DV), jnp.bfloat16),
+            jax.ShapeDtypeStruct((tokens, 2 * DH), jnp.bfloat16),
             jax.ShapeDtypeStruct((tokens, DH), jnp.float32),
             jax.ShapeDtypeStruct((tokens, DV), jnp.float32),
         ],
-        name="retain",
+        compiler_params=pltpu.CompilerParams(vmem_limit_bytes=12 * MIB),
+        name="project",
         interpret=INTERPRET,
-    )(made, turn, log_decay.reshape(1))
-
-
-def pass_on_kernel(spread_ref, made_ref, weight_ref, send_ref):
-    tokens = made_ref.shape[0]
-    query = made_ref[:, : 2 * DH] * jnp.bfloat16(DH ** (-0.5))
+    )(own, across, *weights, place, turn, log_decay.reshape(1))
+
+
+def pass_on_kernel(spread_ref, att_ref, weight_ref, send_ref):
+    tokens = att_ref.shape[0]
     total = jnp.zeros((DH, DV), jnp.float32)
     for i in range(spread_ref.shape[0]):
         total = total + spread_ref[i, tokens:].astype(jnp.float32) * weight_ref[i]
     for k in range(send_ref.shape[0]):
-        send_ref[k, :tokens] = query
+        send_ref[k, :tokens] = att_ref[...]
         send_ref[k, tokens:] = total.astype(jnp.bfloat16)
 
 
-def pass_on(spread, made, weight, count):
+def pass_on(spread, att, weight, count):
     return pl.pallas_call(
         pass_on_kernel,
         in_specs=[VMEM, VMEM, SMEM],
         out_shape=jax.ShapeDtypeStruct((count, *spread.shape[1:]), jnp.bfloat16),
+        compiler_params=pltpu.CompilerParams(vmem_limit_bytes=6 * MIB),
         name="pass_on",
         interpret=INTERPRET,
-    )(spread, made, weight)
+    )(spread, att, weight)
 
 
 def attend_kernel(
@@ -247,7 +315,9 @@
             ],
         ),
         out_shape=jax.ShapeDtypeStruct((blocks, ROWS, 2 * tokens), jnp.bfloat16),
-        compiler_params=pltpu.CompilerParams(dimension_semantics=("arbitrary",)),
+        compiler_params=pltpu.CompilerParams(
+            dimension_semantics=("arbitrary",), vmem_limit_bytes=24 * MIB
+        ),
         cost_estimate=pl.CostEstimate(
             flops=blocks * count * tokens * 4 * 256,
             bytes_accessed=blocks * tokens * 1024 + count * 512,
@@ -282,7 +352,7 @@
         carried = carried + spread_ref[i, tokens:].astype(jnp.float32) * weight_ref[i]
     for i in range(blocks):
         carried = carried + along_ref[i, tokens:].astype(jnp.float32) * weight_ref[chips + i]
-    ret = within_ref[...] + exact(query_ref[...], carried, ((1,), (0,)))
+    ret = within_ref[...] + rounded(query_ref[...], carried, ((1,), (0,)))
     ret = ret * lax.rsqrt(jnp.mean(ret * ret, axis=1, keepdims=True) + EPSILON)
     ret = (ret * gain_ref[1:2]).astype(jnp.bfloat16)
     half = tokens // 2
@@ -297,6 +367,7 @@
         finish_kernel,
         in_specs=[VMEM, SMEM, VMEM, VMEM, VMEM, SMEM, VMEM, VMEM],
         out_shape=jax.ShapeDtypeStruct((2, tokens // 2, 2 * DV), jnp.bfloat16),
+        compiler_params=pltpu.CompilerParams(vmem_limit_bytes=8 * MIB),
         name="finish",
         interpret=INTERPRET,
     )(parts, mixing.reshape(1), gains, spread, along, weights, query, within)
@@ -346,27 +417,16 @@
     w_own, inputs, small = lax.optimization_barrier((w_own, inputs, small))
     features, norm_gain, att_lambda, att_gain, ret_gain = inputs
     even, ys, zs, chip, z, y, c, x = small
-    w_before, w_after, w_low, w_high = two_steps(w_own, 2 * ny * rows)
-
-    residues = [(z + k) % nl for k in (0, nl - 1, 1, 2)]
+    weights = (w_own, *two_steps(w_own, 2 * ny * rows))
+    blocks = [high * nl + (z + k) % nl for k in (0, nl - 1, 1, 2) for high in range(2)]
 
     pieces = [features] + [
         lax.ppermute(features, "tp", [(i, (i + k) % groups) for i in range(groups)])
         for k in range(1, groups)
     ]
-    gathered = jnp.zeros((groups, *features.shape), features.dtype)
-    for k, piece in enumerate(pieces):
-        gathered = lax.dynamic_update_index_in_dim(gathered, piece, (x - k) % groups, 0)
-    floats = gathered.astype(jnp.float32)
-    mean_sq = jnp.sum(floats * floats, axis=(0, 2)) / norm_gain.shape[0]
-    gain = norm_gain.reshape(groups, 1, -1)
-    scaled = floats * lax.rsqrt(mean_sq + EPSILON)[None, :, None] * gain
-    scaled = scaled.astype(jnp.bfloat16)
-    per_tp = nz // groups
-    wide = scaled.shape[2] // per_tp
-    by_z = jnp.stack([scaled[i // per_tp][:, (i % per_tp) * wide :][:, :wide] for i in range(nz)])
-    across = swapped(by_z)
-    both = jnp.stack([jnp.where(c == 0, by_z, across), jnp.where(c == 0, across, by_z)])
+    origin = jnp.stack([(x - k) % groups for k in range(groups)]).astype(jnp.int32)
+    normed = norm(pieces, origin, norm_gain, nz)
+    across = swapped(normed)
 
     log_decay = decay_log(x * 2 + c, float(nz * ny * tokens))
     positions = (chip * tokens + jnp.arange(tokens)).astype(jnp.float32)
@@ -384,26 +444,19 @@
         ]
     )
     where = jnp.stack([z, y, c]).astype(jnp.int32)
+    place = jnp.stack([c, *blocks]).astype(jnp.int32)
     mixing = lax.dynamic_index_in_dim(att_lambda, c, 0, keepdims=False)
     gains = jnp.stack([att_gain, ret_gain])
 
-    def made_by(k, high, matrix):
-        left = lax.dynamic_index_in_dim(both, high * nl + residues[k], 1, keepdims=False)
-        left = left.reshape(tokens, wide)
-        return jnp.dot(left, matrix, preferred_element_type=jnp.float32)
-
-    made = made_by(0, 0, w_own[:wide]) + made_by(0, 1, w_own[wide:])
-    made = made + made_by(1, 0, w_before[:wide]) + made_by(1, 1, w_before[wide:])
-    made = made + made_by(2, 0, w_after[:wide]) + made_by(2, 1, w_after[wide:])
-    made = made + made_by(3, 0, w_low) + made_by(3, 1, w_high)
-    made = made.astype(jnp.bfloat16)
-    made, turn, log_decay, to_end, before, where, mixing, gains = lax.optimization_barrier(
-        (made, turn, log_decay, to_end, before, where, mixing, gains)
+    normed, across, weights, turn, log_decay, to_end, before, where, place, mixing, gains = (
+        lax.optimization_barrier(
+            (normed, across, weights, turn, log_decay, to_end, before, where, place, mixing, gains)
+        )
     )
 
-    send, query, within = retain(made, turn, log_decay, ny)
+    send, att, query, within = project(normed, across, weights, place, turn, log_decay, ny)
     spread = lax.all_to_all(send, "y", 0, 0, tiled=True)
-    send = pass_on(spread, made, to_end, nz)
+    send = pass_on(spread, att, to_end, nz)
     along = lax.all_to_all(send, Z, 0, 0, tiled=True)
     spread, along = lax.optimization_barrier((spread, along))
     parts = attend(where, along, spread, swapped(spread), tokens)

time: 231 us -> 210 us (0.909)
  Pallas kernels: 31.3 us -> 24.2 us
  blocking collectives: 138 us -> 131 us
  matrix products: 4.9 us -> 0.45 us
  waiting for transfers between devices: 6.84 us -> 3.05 us
  local copies, waits for them, and re-layouts: 11.1 us -> 13.7 us
    dot_general x8 -> x0, matrix products: 4.45 us -> none  [made_by(): return jnp.dot(left, matrix, preferred_element_type=jnp.float32)]
    all_to_all x1, blocking collectives: 23.3 us -> 19.3 us  [layer(): spread = lax.all_to_all(send, 'y', 0, 0, tiled=True)]
    ppermute x4, waiting for transfers between devices: 5 us -> 0.98 us  [shifted(): lax.ppermute(value, Z, [(i, (i + step) % count) for i in range(count)])]
    dynamic_update_slice x4 -> x0, local copies, waits for them, and re-layouts: 2.78 us -> none  [layer(): lax.dynamic_update_index_in_dim(gathered, piece, (x - k) % groups, 0)]
    slice x2, local copies, waits for them, and re-layouts: 0.99 us -> 3.36 us  [the longest x1 1.69 us: two_steps(): high = shifted(after[half:], -1)]
    unnamed x17 -> x18, local copies, waits for them, and re-layouts: 4.41 us -> 5.88 us
  transfers between devices with their start and end apart: 9 -> 9, of which waited for: 2 -> 3; matrix products, arithmetic and copies ran while one was open for 8% -> 5% of each run, Pallas kernels for 0% -> 0%
where the time goes in v2:
time: 210 us; the launch traced here: 209 us
  blocking collectives  131 us (62%)
  starting transfers between devices  32.4 us (15%)
  Pallas kernels  24.2 us (12%)
  local copies, waits for them, and re-layouts  13.7 us (7%)
  other arithmetic  3.53 us (2%)
  waiting for transfers between devices  3.05 us (1%)
    all_to_all x1, blocking collectives, layer(): w_own = lax.all_to_all(sent, ('zh', 'y', 'c'), 0, 0, tiled=True)  37.5 us
    all_to_all x1, blocking collectives, layer(): parts = lax.all_to_all(parts, Z, 0, 0, tiled=True)  34.4 us
    all_to_all x1, blocking collectives, layer(): along = lax.all_to_all(send, Z, 0, 0, tiled=True)  23.9 us
    all_to_all x1, blocking collectives, layer(): spread = lax.all_to_all(send, 'y', 0, 0, tiled=True)  19.3 us
    pallas_call x1, Pallas kernels, attend(): pl.pallas_call(attend_kernel, grid_spec=pltpu.PrefetchScalarGridSpec(num_...  18.2 us
    all_to_all x1, blocking collectives, layer(): lax.all_to_all(partial.reshape(groups, -1, partial.shape[1]), 'tp', 0, 0,...  12.5 us
    ppermute x2, starting transfers between devices, swapped(): return lax.ppermute(value, 'c', [(0, 1), (1, 0)])  12.4 us
    ppermute x4, starting transfers between devices, shifted(): lax.ppermute(value, Z, [(i, (i + step) % count) for i in range(count)])  10.7 us
  transfers between devices with their start and end apart: 9, of which 3 were waited for; matrix products, arithmetic and copies ran while one was open for 5% of the time, Pallas kernels for 0%

profile of v2, /device:TPU:1, one launch (start us, length us, event | category | flops | bytes accessed | tf_op | source)
XLA Modules:
  0.0 209.2 jit_solution(12553807339341988964)
XLA Ops:
  4.4 37.5 %all_to_all.30 = bf16[32,16,512]{2,1,0:T(8,128)(2,1)S(1)} all-to-all(bf16[32,16,512]{2,1,0:T(8,128)(2,1)S(1)} %bitcast.40), channel_id=1, replica_groups=mesh['zh'=2,'zl'=4,'y'=8,'c'=2,'tp'=4] {'zh','y','c'}, dimensions={0} | all-to-all | bytes 1048576 | tf_op jit(solution)/shard_map/all_to_all | solution.py:414
  41.9 4.4 %collective-permute-start.2 = (bf16[128,512]{1,0:T(8,128)(2,1)}, bf16[128,512]{1,0:T(8,128)(2,1)S(1)}, u32[]{:S(2)}, u32[]{:S(2)}) collective-permute-start(bf16[128,512]{1,0:T(8,128)(2,1)} %refs_0_), channel_id=1, source_target_pairs={{0,3},{1,0},{2,1},{3,2},{4,7},{5,4},{6,5},{7,6},{8,11},{9,8},{10,9... | collective-permute-start | bytes 393224 | tf_op jit(solution)/shard_map/ppermute | solution.py:424
  46.3 2.4 %collective-permute-start.1 = (bf16[128,512]{1,0:T(8,128)(2,1)}, bf16[128,512]{1,0:T(8,128)(2,1)S(1)}, u32[]{:S(2)}, u32[]{:S(2)}) collective-permute-start(bf16[128,512]{1,0:T(8,128)(2,1)} %refs_0_), channel_id=1, source_target_pairs={{0,2},{1,3},{2,0},{3,1},{4,6},{5,7},{6,4},{7,5},{8,10},{9,11},{10,... | collective-permute-start | bytes 393224 | tf_op jit(solution)/shard_map/ppermute | solution.py:424
  48.7 2.5 %collective-permute-start = (bf16[128,512]{1,0:T(8,128)(2,1)}, bf16[128,512]{1,0:T(8,128)(2,1)S(1)}, u32[]{:S(2)}, u32[]{:S(2)}) collective-permute-start(bf16[128,512]{1,0:T(8,128)(2,1)} %refs_0_), channel_id=1, source_target_pairs={{0,1},{1,2},{2,3},{3,0},{4,5},{5,6},{6,7},{7,4},{8,9},{9,10},{10,1... | collective-permute-start | bytes 393224 | tf_op jit(solution)/shard_map/ppermute | solution.py:424
  51.3 2.3 %collective-permute-start.5 = (bf16[512,512]{1,0:T(8,128)(2,1)S(1)}, bf16[512,512]{1,0:T(8,128)(2,1)}, u32[]{:S(2)}, u32[]{:S(2)}) collective-permute-start(bf16[512,512]{1,0:T(8,128)(2,1)S(1)} %bitcast.37), channel_id=1, source_target_pairs={{0,448},{64,0},{128,64},{192,128},{256,192},{320,256},{384,320},{4... | collective-permute-start | bytes 1572872 | tf_op jit(solution)/shard_map/ppermute | solution.py:33
  53.5 3.0 %collective-permute-start.4 = (bf16[512,512]{1,0:T(8,128)(2,1)S(1)}, bf16[512,512]{1,0:T(8,128)(2,1)}, u32[]{:S(2)}, u32[]{:S(2)}) collective-permute-start(bf16[512,512]{1,0:T(8,128)(2,1)S(1)} %bitcast.38), channel_id=1, source_target_pairs={{0,64},{64,128},{128,192},{192,256},{256,320},{320,384},{384,448},... | collective-permute-start | bytes 1572872 | tf_op jit(solution)/shard_map/ppermute | solution.py:33
  59.8 5.0 %collective-permute-start.3 = (bf16[8,128,256]{2,1,0:T(8,128)(2,1)S(1)}, bf16[8,128,256]{2,1,0:T(8,128)(2,1)}, u32[]{:S(2)}, u32[]{:S(2)}) collective-permute-start(bf16[8,128,256]{2,1,0:T(8,128)(2,1)S(1)} %norm.1.own_ref), channel_id=1, source_target_pairs={{0,4},{4,0},{1,5},{5,1},{2,6},{6,2},{3,7},{7,3},{8,12},{12,8},{9,1... | collective-permute-start | bytes 1572872 | tf_op jit(solution)/shard_map/ppermute | solution.py:28
  65.7 1.7 slice.25
  67.4 3.5 %collective-permute-start.7 = (bf16[256,512]{1,0:T(8,128)(2,1)}, bf16[256,512]{1,0:T(8,128)(2,1)S(1)}, u32[]{:S(2)}, u32[]{:S(2)}) collective-permute-start(bf16[256,512]{1,0:T(8,128)(2,1)} %slice.25), channel_id=1, source_target_pairs={{0,448},{64,0},{128,64},{192,128},{256,192},{320,256},{384,320},{4... | collective-permute-start | bytes 786440 | tf_op jit(solution)/shard_map/ppermute | solution.py:33
  70.9 1.7 slice.24
  72.5 1.9 collective-permute-start.6
  77.5 1.3 dynamic_slice.4
  79.6 1.0 pad_maximum_fusion.turn_ref
  80.6 1.0 collective-permute-done.6.w_low_ref
  81.6 2.6 %project.1 = (bf16[8,320,128]{2,1,0:T(8,128)(2,1)S(1)}, bf16[256,128]{1,0:T(8,128)(2,1)S(1)}, f32[256,64]{1,0:T(8,128)S(1)}, f32[256,128]{1,0:T(8,128)S(1)}) custom-call(bf16[8,128,256]{2,1,0:T(8,128)(2,1)S(1)} %norm.1.own_ref, bf16[8,128,256]{2,1,0:T(8,128)(2,1)} %collective-permute-done.3.across_ref, bf16[512,512]{1,0:T(8,128)(2,1)S(1)} %bitcast.39, ...), custom_call_target="tpu_custom_call" | custom-call | tf_op jit(solution)/shard_map/project/pallas_call | solution.py:169
  84.2 19.3 %all_to_all.31.spread_ref.mine_ref = bf16[8,320,128]{2,1,0:T(8,128)(2,1)S(1)} all-to-all(bf16[8,320,128]{2,1,0:T(8,128)(2,1)S(1)} %get-tuple-element.83), channel_id=1, replica_groups=mesh['zh'=2,'zl'=4,'y'=8,'c'=2,'tp'=4] {'y'}, dimensions={0} | all-to-all | bytes 1310720 | tf_op jit(solution)/shard_map/all_to_all | solution.py:458
  104.1 23.9 %all_to_all.32.q_ref.along_ref = bf16[8,320,128]{2,1,0:T(8,128)(2,1)S(1)} all-to-all(bf16[8,320,128]{2,1,0:T(8,128)(2,1)S(1)} %pass_on.1), channel_id=1, replica_groups=mesh['zh'=2,'zl'=4,'y'=8,'c'=2,'tp'=4] {'zh','zl'}, dimensions={0} | all-to-all | bytes 1310720 | tf_op jit(solution)/shard_map/all_to_all | solution.py:460
  128.0 7.3 %collective-permute-start.8 = (bf16[8,320,128]{2,1,0:T(8,128)(2,1)S(1)}, bf16[8,320,128]{2,1,0:T(8,128)(2,1)S(1)}, u32[]{:S(2)}, u32[]{:S(2)}) collective-permute-start(bf16[8,320,128]{2,1,0:T(8,128)(2,1)S(1)} %all_to_all.31.spread_ref.mine_ref), channel_id=1, source_target_pairs={{0,4},{4,0},{1,5},{5,1},{2,6},{6,2},{3,7},{7,3},{8,12},{12,8},{9,1... | collective-permute-start | bytes 1966088 | tf_op jit(solution)/shard_map/ppermute | solution.py:28
  135.3 1.7 collective-permute-done.8.other_ref
  137.0 18.2 %attend.1 = bf16[8,144,512]{2,1,0:T(8,128)(2,1)S(1)} custom-call(s32[3]{0:T(128)S(1)} %pad_add_fusion.1.where_ref, bf16[8,320,128]{2,1,0:T(8,128)(2,1)S(1)} %all_to_all.32.q_ref.along_ref, bf16[8,320,128]{2,1,0:T(8,128)(2,1)S(1)} %all_to_all.31.spread_ref.mine_ref, bf16[8,320,128]{2,1,0:T(8,128)(2,1)S(1)} %collective-permute-done.8.other_ref), custom_call_target="tpu_custom_call" | custom-call | flops 4294967296 | bytes 3145728 | tf_op jit(solution)/shard_map/attend/pallas_call | solution.py:297
  155.3 34.4 %all_to_all.33.parts_ref = bf16[8,144,512]{2,1,0:T(8,128)(2,1)S(1)} all-to-all(bf16[8,144,512]{2,1,0:T(8,128)(2,1)S(1)} %attend.1), channel_id=1, replica_groups=mesh['zh'=2,'zl'=4,'y'=8,'c'=2,'tp'=4] {'zh','zl'}, dimensions={0} | all-to-all | bytes 2359296 | tf_op jit(solution)/shard_map/all_to_all | solution.py:463
  189.7 1.8 finish.1
  191.4 4.0 %all_to_all.34 = bf16[2,128,256]{2,1,0:T(8,128)(2,1)S(1)} all-to-all(bf16[2,128,256]{2,1,0:T(8,128)(2,1)S(1)} %finish.1), channel_id=1, replica_groups=mesh['zh'=2,'zl'=4,'y'=8,'c'=2,'tp'=4] {'c'}, dimensions={0} | all-to-all | bytes 262144 | tf_op jit(solution)/shard_map/all_to_all | solution.py:466
  195.9 12.5 %all_to_all.35 = bf16[4,32,2048]{2,1,0:T(8,128)(2,1)S(1)} all-to-all(bf16[4,32,2048]{2,1,0:T(8,128)(2,1)S(1)} %bitcast.42), channel_id=1, replica_groups=mesh['zh'=2,'zl'=4,'y'=8,'c'=2,'tp'=4] {'tp'}, dimensions={0} | all-to-all | bytes 1048576 | tf_op jit(solution)/shard_map/all_to_all | solution.py:473
  (46 shorter events, 13.9 us)
Async XLA Ops:
  0.0 195.5 %copy-start = (bf16[2,256,2048]{2,1,0:T(8,128)(2,1)S(1)}, bf16[2,256,2048]{2,1,0:T(8,128)(2,1)}, u32[]{:S(2)}) copy-start(bf16[2,256,2048]{2,1,0:T(8,128)(2,1)} %param.23) | copy-start | bytes 6291460
  0.0 0.8 copy-start.2
  0.9 0.7 copy-start.3
  1.6 0.7 copy-start.5
  2.3 0.7 copy-start.6
  2.9 0.7 copy-start.7
  3.6 0.7 copy-start.8
  41.9 15.1 %collective-permute-start.2 = (bf16[128,512]{1,0:T(8,128)(2,1)}, bf16[128,512]{1,0:T(8,128)(2,1)S(1)}, u32[]{:S(2)}, u32[]{:S(2)}) collective-permute-start(bf16[128,512]{1,0:T(8,128)(2,1)} %refs_0_), channel_id=1, source_target_pairs={{0,3},{1,0},{2,1},{3,2},{4,7},{5,4},{6,5},{7,6},{8,11},{9,8},{10,9... | collective-permute-start | bytes 393224 | tf_op jit(solution)/shard_map/ppermute | solution.py:424
  46.3 10.7 %collective-permute-start.1 = (bf16[128,512]{1,0:T(8,128)(2,1)}, bf16[128,512]{1,0:T(8,128)(2,1)S(1)}, u32[]{:S(2)}, u32[]{:S(2)}) collective-permute-start(bf16[128,512]{1,0:T(8,128)(2,1)} %refs_0_), channel_id=1, source_target_pairs={{0,2},{1,3},{2,0},{3,1},{4,6},{5,7},{6,4},{7,5},{8,10},{9,11},{10,... | collective-permute-start | bytes 393224 | tf_op jit(solution)/shard_map/ppermute | solution.py:424
  48.7 8.6 %collective-permute-start = (bf16[128,512]{1,0:T(8,128)(2,1)}, bf16[128,512]{1,0:T(8,128)(2,1)S(1)}, u32[]{:S(2)}, u32[]{:S(2)}) collective-permute-start(bf16[128,512]{1,0:T(8,128)(2,1)} %refs_0_), channel_id=1, source_target_pairs={{0,1},{1,2},{2,3},{3,0},{4,5},{5,6},{6,7},{7,4},{8,9},{9,10},{10,1... | collective-permute-start | bytes 393224 | tf_op jit(solution)/shard_map/ppermute | solution.py:424
  51.3 14.4 %collective-permute-start.5 = (bf16[512,512]{1,0:T(8,128)(2,1)S(1)}, bf16[512,512]{1,0:T(8,128)(2,1)}, u32[]{:S(2)}, u32[]{:S(2)}) collective-permute-start(bf16[512,512]{1,0:T(8,128)(2,1)S(1)} %bitcast.37), channel_id=1, source_target_pairs={{0,448},{64,0},{128,64},{192,128},{256,192},{320,256},{384,320},{4... | collective-permute-start | bytes 1572872 | tf_op jit(solution)/shard_map/ppermute | solution.py:33
  53.5 17.3 %collective-permute-start.4 = (bf16[512,512]{1,0:T(8,128)(2,1)S(1)}, bf16[512,512]{1,0:T(8,128)(2,1)}, u32[]{:S(2)}, u32[]{:S(2)}) collective-permute-start(bf16[512,512]{1,0:T(8,128)(2,1)S(1)} %bitcast.38), channel_id=1, source_target_pairs={{0,64},{64,128},{128,192},{192,256},{256,320},{320,384},{384,448},... | collective-permute-start | bytes 1572872 | tf_op jit(solution)/shard_map/ppermute | solution.py:33
  57.4 0.9 copy-start.1
  58.3 0.7 copy-start.4
  59.8 20.8 %collective-permute-start.3 = (bf16[8,128,256]{2,1,0:T(8,128)(2,1)S(1)}, bf16[8,128,256]{2,1,0:T(8,128)(2,1)}, u32[]{:S(2)}, u32[]{:S(2)}) collective-permute-start(bf16[8,128,256]{2,1,0:T(8,128)(2,1)S(1)} %norm.1.own_ref), channel_id=1, source_target_pairs={{0,4},{4,0},{1,5},{5,1},{2,6},{6,2},{3,7},{7,3},{8,12},{12,8},{9,1... | collective-permute-start | bytes 1572872 | tf_op jit(solution)/shard_map/ppermute | solution.py:28
  67.4 13.2 %collective-permute-start.7 = (bf16[256,512]{1,0:T(8,128)(2,1)}, bf16[256,512]{1,0:T(8,128)(2,1)S(1)}, u32[]{:S(2)}, u32[]{:S(2)}) collective-permute-start(bf16[256,512]{1,0:T(8,128)(2,1)} %slice.25), channel_id=1, source_target_pairs={{0,448},{64,0},{128,64},{192,128},{256,192},{320,256},{384,320},{4... | collective-permute-start | bytes 786440 | tf_op jit(solution)/shard_map/ppermute | solution.py:33
  72.5 9.1 %collective-permute-start.6 = (bf16[256,512]{1,0:T(8,128)(2,1)}, bf16[256,512]{1,0:T(8,128)(2,1)}, u32[]{:S(2)}, u32[]{:S(2)}) collective-permute-start(bf16[256,512]{1,0:T(8,128)(2,1)} %slice.24), channel_id=1, source_target_pairs={{0,64},{64,128},{128,192},{192,256},{256,320},{320,384},{384,448},... | collective-permute-start | bytes 786440 | tf_op jit(solution)/shard_map/ppermute | solution.py:33
  128.0 9.1 %collective-permute-start.8 = (bf16[8,320,128]{2,1,0:T(8,128)(2,1)S(1)}, bf16[8,320,128]{2,1,0:T(8,128)(2,1)S(1)}, u32[]{:S(2)}, u32[]{:S(2)}) collective-permute-start(bf16[8,320,128]{2,1,0:T(8,128)(2,1)S(1)} %all_to_all.31.spread_ref.mine_ref), channel_id=1, source_target_pairs={{0,4},{4,0},{1,5},{5,1},{2,6},{6,2},{3,7},{7,3},{8,12},{12,8},{9,1... | collective-permute-start | bytes 1966088 | tf_op jit(solution)/shard_map/ppermute | solution.py:28

commit v3 on v2

--- a/solution.py
+++ b/solution.py
@@ -41,29 +41,50 @@
     return before, after, low, high
 
 
-def pack_kernel(query_ref, key_ref, value_ref, rq_ref, rk_ref, rv_ref, out_ref):
-    for h, whole in enumerate((key_ref, value_ref)):
-        parts = []
-        for ref in (query_ref, None, rq_ref, rk_ref, rv_ref):
-            if ref is None:
-                parts.append(whole[...])
-            else:
-                width = ref.shape[1] // 2
-                parts.append(ref[:, h * width : (h + 1) * width])
+def pack_kernel(*refs):
+    count = len(refs) // 2
+    sources, (out_ref, wide_ref), scratch, sems = (
+        refs[: count - 1],
+        refs[count - 1 : count + 1],
+        refs[count + 1 : -1],
+        refs[-1],
+    )
+    copies = [
+        pltpu.make_async_copy(source, buffer, sems.at[i])
+        for i, (source, buffer) in enumerate(zip(sources, scratch))
+    ]
+    for copy in copies:
+        copy.start()
+    for copy in copies:
+        copy.wait()
+    query, key, value, rq, rk, rv, features = (buffer[...] for buffer in scratch)
+    for h, whole in enumerate((key, value)):
+        parts = [query, whole, rq, rk, rv]
+        for k in (0, 2, 3, 4):
+            width = parts[k].shape[1] // 2
+            parts[k] = parts[k][:, h * width : (h + 1) * width]
         row = jnp.concatenate(parts, axis=1)
         for i in range(out_ref.shape[0]):
             out_ref[i, h] = row
-
-
-def pack(count, *matrices):
-    rows = matrices[0].shape[0]
+    for i in range(wide_ref.shape[0]):
+        wide_ref[i] = features
+
+
+def pack(count, groups, *arrays):
+    rows = arrays[0].shape[0]
     return pl.pallas_call(
         pack_kernel,
-        out_shape=jax.ShapeDtypeStruct((count, 2, rows, 512), jnp.bfloat16),
+        in_specs=[pl.BlockSpec(memory_space=pltpu.HBM)] * len(arrays),
+        out_shape=[
+            jax.ShapeDtypeStruct((count, 2, rows, 512), jnp.bfloat16),
+            jax.ShapeDtypeStruct((groups, *arrays[-1].shape), jnp.bfloat16),
+        ],
+        scratch_shapes=[pltpu.VMEM(a.shape, a.dtype) for a in arrays]
+        + [pltpu.SemaphoreType.DMA((len(arrays),))],
         compiler_params=pltpu.CompilerParams(vmem_limit_bytes=4 * MIB),
         name="pack",
         interpret=INTERPRET,
-    )(*matrices)
+    )(*(pltpu.with_memory_space_constraint(a, pltpu.HBM) for a in arrays))
 
 
 def rounded(a, b, dims):
@@ -75,34 +96,32 @@
     )
 
 
-def norm_kernel(*refs):
-    *piece_refs, place_ref, gain_ref, out_ref = refs
-    groups = len(piece_refs)
+def norm_kernel(gathered_ref, gain_ref, out_ref):
+    groups = gathered_ref.shape[0]
     blocks, _, wide = out_ref.shape
     per_tp = blocks // groups
     total = 0.0
-    for ref in piece_refs:
-        floats = ref[...].astype(jnp.float32)
+    for g in range(groups):
+        floats = gathered_ref[g].astype(jnp.float32)
         total = total + jnp.sum(floats * floats, axis=1, keepdims=True)
     scale = lax.rsqrt(total / (blocks * wide) + EPSILON)
-    for k, ref in enumerate(piece_refs):
-        for i in range(per_tp):
-            at = place_ref[k] * per_tp + i
-            part = ref[:, i * wide : (i + 1) * wide].astype(jnp.float32)
-            out_ref[at] = (part * scale * gain_ref[at]).astype(jnp.bfloat16)
-
-
-def norm(pieces, place, gain, blocks):
-    rows, width = pieces[0].shape
-    wide = width * len(pieces) // blocks
+    for at in range(blocks):
+        i = at % per_tp
+        part = gathered_ref[at // per_tp, :, i * wide : (i + 1) * wide].astype(jnp.float32)
+        out_ref[at] = (part * scale * gain_ref[at]).astype(jnp.bfloat16)
+
+
+def norm(gathered, gain, blocks):
+    groups, rows, width = gathered.shape
+    wide = width * groups // blocks
     return pl.pallas_call(
         norm_kernel,
-        in_specs=[VMEM] * len(pieces) + [SMEM, VMEM],
+        in_specs=[VMEM, VMEM],
         out_shape=jax.ShapeDtypeStruct((blocks, rows, wide), jnp.bfloat16),
         compiler_params=pltpu.CompilerParams(vmem_limit_bytes=6 * MIB),
         name="norm",
         interpret=INTERPRET,
-    )(*pieces, place, gain.reshape(blocks, 1, wide))
+    )(gathered, gain.reshape(blocks, 1, wide))
 
 
 def project_kernel(
@@ -114,7 +133,8 @@
     w_low_ref,
     w_high_ref,
     place_ref,
-    turn_ref,
+    cosine_ref,
+    sine_ref,
     decay_ref,
     send_ref,
     att_ref,
@@ -144,7 +164,9 @@
     ahead = pltpu.roll(pair, 2 * DH - quarter, 1)
     behind = pltpu.roll(pair, quarter, 1)
     crossed = jnp.where((lane & quarter) == 0, -ahead, behind)
-    turned = pair * turn_ref[0] + crossed * turn_ref[1]
+    cosine = jnp.concatenate([cosine_ref[...]] * 4, axis=1)
+    sine = jnp.concatenate([sine_ref[...]] * 4, axis=1)
+    turned = pair * cosine + crossed * sine
     query = turned[:, :DH]
     key = turned[:, DH:] * DH ** (-0.5)
     value = made[:, 384:512]
@@ -164,11 +186,11 @@
     query_ref[...] = query * jnp.exp(log_decay * (offset + 1.0))
 
 
-def project(own, across, weights, place, turn, log_decay, count):
+def project(own, across, weights, place, cosine, sine, log_decay, count):
     tokens = 2 * own.shape[1]
     return pl.pallas_call(
         project_kernel,
-        in_specs=[VMEM] * 7 + [SMEM, VMEM, SMEM],
+        in_specs=[VMEM] * 7 + [SMEM, VMEM, VMEM, SMEM],
         out_shape=[
             jax.ShapeDtypeStruct((count, tokens + DH, DV), jnp.bfloat16),
             jax.ShapeDtypeStruct((tokens, 2 * DH), jnp.bfloat16),
@@ -178,7 +200,7 @@
         compiler_params=pltpu.CompilerParams(vmem_limit_bytes=12 * MIB),
         name="project",
         interpret=INTERPRET,
-    )(own, across, *weights, place, turn, log_decay.reshape(1))
+    )(own, across, *weights, place, cosine, sine, log_decay.reshape(1))
 
 
 def pass_on_kernel(spread_ref, att_ref, weight_ref, send_ref):
@@ -405,7 +427,8 @@
     chip = z * ny + y
     tokens = 2 * features.shape[0]
 
-    sent = pack(2 * ny, att_query, att_key, att_value, ret_query, ret_key, ret_value)
+    matrices = (att_query, att_key, att_value, ret_query, ret_key, ret_value)
+    sent, features = pack(2 * ny, groups, *matrices, features)
     rows, width = sent.shape[2:]
     sent = sent.reshape(4 * ny, rows, width)
     even = jnp.arange(0, DH, 2).astype(jnp.float32)
@@ -420,19 +443,15 @@
     weights = (w_own, *two_steps(w_own, 2 * ny * rows))
     blocks = [high * nl + (z + k) % nl for k in (0, nl - 1, 1, 2) for high in range(2)]
 
-    pieces = [features] + [
-        lax.ppermute(features, "tp", [(i, (i + k) % groups) for i in range(groups)])
-        for k in range(1, groups)
-    ]
-    origin = jnp.stack([(x - k) % groups for k in range(groups)]).astype(jnp.int32)
-    normed = norm(pieces, origin, norm_gain, nz)
+    gathered = lax.all_to_all(features, "tp", 0, 0, tiled=True)
+    normed = norm(gathered, norm_gain, nz)
     across = swapped(normed)
 
     log_decay = decay_log(x * 2 + c, float(nz * ny * tokens))
     positions = (chip * tokens + jnp.arange(tokens)).astype(jnp.float32)
     inverse = 10000.0 ** (-even / DH)
     angles = positions[:, None] * inverse[None, :]
-    turn = jnp.stack([jnp.tile(jnp.cos(angles), (1, 4)), jnp.tile(jnp.sin(angles), (1, 4))])
+    cosine, sine = jnp.cos(angles), jnp.sin(angles)
     span = log_decay * tokens
     to_end = jnp.exp(span * (ny - 1 - ys).astype(jnp.float32))
     y_steps = jnp.maximum(y - 1 - ys, 0).astype(jnp.float32)
@@ -448,13 +467,13 @@
     mixing = lax.dynamic_index_in_dim(att_lambda, c, 0, keepdims=False)
     gains = jnp.stack([att_gain, ret_gain])
 
-    normed, across, weights, turn, log_decay, to_end, before, where, place, mixing, gains = (
-        lax.optimization_barrier(
-            (normed, across, weights, turn, log_decay, to_end, before, where, place, mixing, gains)
-        )
-    )
-
-    send, att, query, within = project(normed, across, weights, place, turn, log_decay, ny)
+    tables = (cosine, sine, log_decay, to_end, before, where, place, mixing, gains)
+    normed, across, weights, tables = lax.optimization_barrier((normed, across, weights, tables))
+    cosine, sine, log_decay, to_end, before, where, place, mixing, gains = tables
+
+    send, att, query, within = project(
+        normed, across, weights, place, cosine, sine, log_decay, ny
+    )
     spread = lax.all_to_all(send, "y", 0, 0, tiled=True)
     send = pass_on(spread, att, to_end, nz)
     along = lax.all_to_all(send, Z, 0, 0, tiled=True)

time: 210 us -> 209 us (level)
  waiting for transfers between devices: 3.05 us -> 16.3 us
  local copies, waits for them, and re-layouts: 13.7 us -> 5.93 us
  starting transfers between devices: 32.4 us -> 26.3 us
    ppermute x3 -> x0, starting transfers between devices: 9.32 us -> none  [layer(): lax.ppermute(features, 'tp', [(i, (i + k) % groups) for i in range(groups)])]
    all_to_all x0 -> x1, waiting for transfers between devices: none -> 6.81 us  [layer(): gathered = lax.all_to_all(features, 'tp', 0, 0, tiled=True)]
    ppermute x4, waiting for transfers between devices: 0.98 us -> 7.79 us  [shifted(): lax.ppermute(value, Z, [(i, (i + step) % count) for i in range(count)])]
    all_to_all x0 -> x1, starting transfers between devices: none -> 4.02 us  [layer(): gathered = lax.all_to_all(features, 'tp', 0, 0, tiled=True)]
    unnamed x18 -> x16, local copies, waits for them, and re-layouts: 5.88 us -> 1.89 us
    another operation x4 -> x0, local copies, waits for them, and re-layouts: 3.01 us -> none  [the longest x2 1.51 us: layer(): jnp.tile(jnp.cos(angles), (1, 4))]
    all_to_all x1, blocking collectives: 19.3 us -> 22 us  [layer(): spread = lax.all_to_all(send, 'y', 0, 0, tiled=True)]
  transfers between devices with their start and end apart: 9 -> 7, of which waited for: 3 -> 4; matrix products, arithmetic and copies ran while one was open for 5% -> 2% of each run, Pallas kernels for 0% -> 0%
where the time goes in v3:
time: 209 us; the launch traced here: 208 us
  blocking collectives  133 us (64%)
  starting transfers between devices  26.3 us (13%)
  Pallas kernels  24.7 us (12%)
  waiting for transfers between devices  16.3 us (8%)
  local copies, waits for them, and re-layouts  5.93 us (3%)
    all_to_all x1, blocking collectives, layer(): w_own = lax.all_to_all(sent, ('zh', 'y', 'c'), 0, 0, tiled=True)  37.6 us
    all_to_all x1, blocking collectives, layer(): parts = lax.all_to_all(parts, Z, 0, 0, tiled=True)  34.4 us
    all_to_all x1, blocking collectives, layer(): along = lax.all_to_all(send, Z, 0, 0, tiled=True)  23.2 us
    all_to_all x1, blocking collectives, layer(): spread = lax.all_to_all(send, 'y', 0, 0, tiled=True)  22 us
    pallas_call x1, Pallas kernels, attend(): pl.pallas_call(attend_kernel, grid_spec=pltpu.PrefetchScalarGridSpec(num_...  18.2 us
    all_to_all x1, blocking collectives, layer(): lax.all_to_all(partial.reshape(groups, -1, partial.shape[1]), 'tp', 0, 0,...  11.6 us
    ppermute x2, starting transfers between devices, swapped(): return lax.ppermute(value, 'c', [(0, 1), (1, 0)])  11.6 us
    ppermute x4, starting transfers between devices, shifted(): lax.ppermute(value, Z, [(i, (i + step) % count) for i in range(count)])  10.6 us
  transfers between devices with their start and end apart: 7, of which 4 were waited for; matrix products, arithmetic and copies ran while one was open for 2% of the time, Pallas kernels for 0%

profile of v3, /device:TPU:1, one launch (start us, length us, event | category | flops | bytes accessed | tf_op | source)
XLA Modules:
  0.0 208.5 jit_solution(5393511581706111753)
XLA Ops:
  0.0 1.3 pack.1
  1.4 37.6 %all_to_all.35 = bf16[32,16,512]{2,1,0:T(8,128)(2,1)S(1)} all-to-all(bf16[32,16,512]{2,1,0:T(8,128)(2,1)S(1)} %bitcast.34), channel_id=1, replica_groups=mesh['zh'=2,'zl'=4,'y'=8,'c'=2,'tp'=4] {'zh','y','c'}, dimensions={0} | all-to-all | bytes 1048576 | tf_op jit(solution)/shard_map/all_to_all | solution.py:437
  39.0 2.3 %collective-permute-start.2 = (bf16[512,512]{1,0:T(8,128)(2,1)S(1)}, bf16[512,512]{1,0:T(8,128)(2,1)}, u32[]{:S(2)}, u32[]{:S(2)}) collective-permute-start(bf16[512,512]{1,0:T(8,128)(2,1)S(1)} %bitcast.31), channel_id=1, source_target_pairs={{0,448},{64,0},{128,64},{192,128},{256,192},{320,256},{384,320},{4... | collective-permute-start | bytes 1572872 | tf_op jit(solution)/shard_map/ppermute | solution.py:33
  41.3 3.0 %collective-permute-start.1 = (bf16[512,512]{1,0:T(8,128)(2,1)S(1)}, bf16[512,512]{1,0:T(8,128)(2,1)}, u32[]{:S(2)}, u32[]{:S(2)}) collective-permute-start(bf16[512,512]{1,0:T(8,128)(2,1)S(1)} %bitcast.32), channel_id=1, source_target_pairs={{0,64},{64,128},{128,192},{192,256},{256,320},{320,384},{384,448},... | collective-permute-start | bytes 1572872 | tf_op jit(solution)/shard_map/ppermute | solution.py:33
  44.5 4.0 %all-to-all-start.1 = ((bf16[4,128,512]{2,1,0:T(8,128)(2,1)}), bf16[4,128,512]{2,1,0:T(8,128)(2,1)S(1)}, u32[]{:S(2)}, u32[]{:S(2)}) async-start(bf16[4,128,512]{2,1,0:T(8,128)(2,1)} %copy-done.3), calls=%async_computation.1 | async-start | bytes 1048576 | tf_op jit(solution)/shard_map/all_to_all | solution.py:446
  48.6 6.8 %all-to-all-done.1.gathered_ref = bf16[4,128,512]{2,1,0:T(8,128)(2,1)S(1)} async-done(((bf16[4,128,512]{2,1,0:T(8,128)(2,1)}), bf16[4,128,512]{2,1,0:T(8,128)(2,1)S(1)}, u32[]{:S(2)}, u32[]{:S(2)}) %all-to-all-start.1) | async-done | bytes 524320 | tf_op jit(solution)/shard_map/all_to_all | solution.py:446
  56.3 1.0 copy-done.2
  57.6 6.0 %collective-permute-start = (bf16[8,128,256]{2,1,0:T(8,128)(2,1)S(1)}, bf16[8,128,256]{2,1,0:T(8,128)(2,1)}, u32[]{:S(2)}, u32[]{:S(2)}) collective-permute-start(bf16[8,128,256]{2,1,0:T(8,128)(2,1)S(1)} %norm.1.own_ref), channel_id=1, source_target_pairs={{0,4},{4,0},{1,5},{5,1},{2,6},{6,2},{3,7},{7,3},{8,12},{12,8},{9,1... | collective-permute-start | bytes 1572872 | tf_op jit(solution)/shard_map/ppermute | solution.py:28
  63.6 1.7 slice.25
  65.3 3.5 %collective-permute-start.4 = (bf16[256,512]{1,0:T(8,128)(2,1)}, bf16[256,512]{1,0:T(8,128)(2,1)S(1)}, u32[]{:S(2)}, u32[]{:S(2)}) collective-permute-start(bf16[256,512]{1,0:T(8,128)(2,1)} %slice.25), channel_id=1, source_target_pairs={{0,448},{64,0},{128,64},{192,128},{256,192},{320,256},{384,320},{4... | collective-permute-start | bytes 786440 | tf_op jit(solution)/shard_map/ppermute | solution.py:33
  68.7 1.7 slice.24
  70.4 1.9 collective-permute-start.3
  73.6 1.6 collective-permute-done.4.w_high_ref
  75.2 6.2 %collective-permute-done.3.w_low_ref = bf16[256,512]{1,0:T(8,128)(2,1)} collective-permute-done((bf16[256,512]{1,0:T(8,128)(2,1)}, bf16[256,512]{1,0:T(8,128)(2,1)}, u32[]{:S(2)}, u32[]{:S(2)}) %collective-permute-start.3) | collective-permute-done | bytes 262176 | tf_op jit(solution)/shard_map/ppermute | solution.py:33
  81.4 2.7 %project.1 = (bf16[8,320,128]{2,1,0:T(8,128)(2,1)S(1)}, bf16[256,128]{1,0:T(8,128)(2,1)S(1)}, f32[256,64]{1,0:T(8,128)S(1)}, f32[256,128]{1,0:T(8,128)S(1)}) custom-call(bf16[8,128,256]{2,1,0:T(8,128)(2,1)S(1)} %norm.1.own_ref, bf16[8,128,256]{2,1,0:T(8,128)(2,1)} %collective-permute-done.across_ref, bf16[512,512]{1,0:T(8,128)(2,1)S(1)} %bitcast.33, ...), custom_call_target="tpu_custom_call" | custom-call | tf_op jit(solution)/shard_map/project/pallas_call | solution.py:191
  84.1 22.0 %all_to_all.36.spread_ref.mine_ref = bf16[8,320,128]{2,1,0:T(8,128)(2,1)S(1)} all-to-all(bf16[8,320,128]{2,1,0:T(8,128)(2,1)S(1)} %get-tuple-element.89), channel_id=1, replica_groups=mesh['zh'=2,'zl'=4,'y'=8,'c'=2,'tp'=4] {'y'}, dimensions={0} | all-to-all | bytes 1310720 | tf_op jit(solution)/shard_map/all_to_all | solution.py:477
  106.7 23.2 %all_to_all.37.q_ref.along_ref = bf16[8,320,128]{2,1,0:T(8,128)(2,1)S(1)} all-to-all(bf16[8,320,128]{2,1,0:T(8,128)(2,1)S(1)} %pass_on.1), channel_id=1, replica_groups=mesh['zh'=2,'zl'=4,'y'=8,'c'=2,'tp'=4] {'zh','zl'}, dimensions={0} | all-to-all | bytes 1310720 | tf_op jit(solution)/shard_map/all_to_all | solution.py:479
  129.9 5.7 %collective-permute-start.5 = (bf16[8,320,128]{2,1,0:T(8,128)(2,1)S(1)}, bf16[8,320,128]{2,1,0:T(8,128)(2,1)S(1)}, u32[]{:S(2)}, u32[]{:S(2)}) collective-permute-start(bf16[8,320,128]{2,1,0:T(8,128)(2,1)S(1)} %all_to_all.36.spread_ref.mine_ref), channel_id=1, source_target_pairs={{0,4},{4,0},{1,5},{5,1},{2,6},{6,2},{3,7},{7,3},{8,12},{12,8},{9,1... | collective-permute-start | bytes 1966088 | tf_op jit(solution)/shard_map/ppermute | solution.py:28
  135.5 1.7 collective-permute-done.5.other_ref
  137.3 18.2 %attend.1 = bf16[8,144,512]{2,1,0:T(8,128)(2,1)S(1)} custom-call(s32[3]{0:T(128)S(1)} %pad_add_fusion.where_ref, bf16[8,320,128]{2,1,0:T(8,128)(2,1)S(1)} %all_to_all.37.q_ref.along_ref, bf16[8,320,128]{2,1,0:T(8,128)(2,1)S(1)} %all_to_all.36.spread_ref.mine_ref, bf16[8,320,128]{2,1,0:T(8,128)(2,1)S(1)} %collective-permute-done.5.other_ref), custom_call_target="tpu_custom_call" | custom-call | flops 4294967296 | bytes 3145728 | tf_op jit(solution)/shard_map/attend/pallas_call | solution.py:319
  155.5 34.4 %all_to_all.38.parts_ref = bf16[8,144,512]{2,1,0:T(8,128)(2,1)S(1)} all-to-all(bf16[8,144,512]{2,1,0:T(8,128)(2,1)S(1)} %attend.1), channel_id=1, replica_groups=mesh['zh'=2,'zl'=4,'y'=8,'c'=2,'tp'=4] {'zh','zl'}, dimensions={0} | all-to-all | bytes 2359296 | tf_op jit(solution)/shard_map/all_to_all | solution.py:482
  189.9 1.7 finish.1
  191.6 4.0 %all_to_all.39 = bf16[2,128,256]{2,1,0:T(8,128)(2,1)S(1)} all-to-all(bf16[2,128,256]{2,1,0:T(8,128)(2,1)S(1)} %finish.1), channel_id=1, replica_groups=mesh['zh'=2,'zl'=4,'y'=8,'c'=2,'tp'=4] {'c'}, dimensions={0} | all-to-all | bytes 262144 | tf_op jit(solution)/shard_map/all_to_all | solution.py:485
  196.1 11.6 %all_to_all.40 = bf16[4,32,2048]{2,1,0:T(8,128)(2,1)S(1)} all-to-all(bf16[4,32,2048]{2,1,0:T(8,128)(2,1)S(1)} %bitcast.36), channel_id=1, replica_groups=mesh['zh'=2,'zl'=4,'y'=8,'c'=2,'tp'=4] {'tp'}, dimensions={0} | all-to-all | bytes 1048576 | tf_op jit(solution)/shard_map/all_to_all | solution.py:492
  (34 shorter events, 4.4 us)
Async XLA Ops:
  0.0 195.6 %copy-start = (bf16[2,256,2048]{2,1,0:T(8,128)(2,1)S(1)}, bf16[2,256,2048]{2,1,0:T(8,128)(2,1)}, u32[]{:S(2)}) copy-start(bf16[2,256,2048]{2,1,0:T(8,128)(2,1)} %param.23) | copy-start | bytes 6291460
  0.0 48.6 %copy-start.5 = (f32[128]{0:T(128)S(1)}, f32[128]{0:T(128)}, u32[]{:S(2)}) copy-start(f32[128]{0:T(128)} %param.22) | copy-start | bytes 1540
  0.0 48.6 %copy-start.6 = (f32[128]{0:T(128)S(1)}, f32[128]{0:T(128)}, u32[]{:S(2)}) copy-start(f32[128]{0:T(128)} %param.18) | copy-start | bytes 1540
  0.0 56.2 %copy-start.4 = (f32[2048]{0:T(1024)S(1)}, f32[2048]{0:T(1024)}, u32[]{:S(2)}) copy-start(f32[2048]{0:T(1024)} %param.13) | copy-start | bytes 24580
  1.3 43.1 %copy-start.3 = (bf16[4,128,512]{2,1,0:T(8,128)(2,1)}, bf16[4,128,512]{2,1,0:T(8,128)(2,1)S(1)}, u32[]{:S(2)}) copy-start(bf16[4,128,512]{2,1,0:T(8,128)(2,1)S(1)} %get-tuple-element.63) | copy-start | bytes 1572868
  1.4 71.1 %copy-start.7 = (f32[2]{0:T(128)S(1)}, f32[2]{0:T(128)}, u32[]{:S(2)}) copy-start(f32[2]{0:T(128)} %param.17) | copy-start | bytes 28
  39.0 24.6 %collective-permute-start.2 = (bf16[512,512]{1,0:T(8,128)(2,1)S(1)}, bf16[512,512]{1,0:T(8,128)(2,1)}, u32[]{:S(2)}, u32[]{:S(2)}) collective-permute-start(bf16[512,512]{1,0:T(8,128)(2,1)S(1)} %bitcast.31), channel_id=1, source_target_pairs={{0,448},{64,0},{128,64},{192,128},{256,192},{320,256},{384,320},{4... | collective-permute-start | bytes 1572872 | tf_op jit(solution)/shard_map/ppermute | solution.py:33
  41.3 27.5 %collective-permute-start.1 = (bf16[512,512]{1,0:T(8,128)(2,1)S(1)}, bf16[512,512]{1,0:T(8,128)(2,1)}, u32[]{:S(2)}, u32[]{:S(2)}) collective-permute-start(bf16[512,512]{1,0:T(8,128)(2,1)S(1)} %bitcast.32), channel_id=1, source_target_pairs={{0,64},{64,128},{128,192},{192,256},{256,320},{320,384},{384,448},... | collective-permute-start | bytes 1572872 | tf_op jit(solution)/shard_map/ppermute | solution.py:33
  44.5 11.0 %all-to-all-start.1 = ((bf16[4,128,512]{2,1,0:T(8,128)(2,1)}), bf16[4,128,512]{2,1,0:T(8,128)(2,1)S(1)}, u32[]{:S(2)}, u32[]{:S(2)}) async-start(bf16[4,128,512]{2,1,0:T(8,128)(2,1)} %copy-done.3), calls=%async_computation.1 | async-start | bytes 1048576 | tf_op jit(solution)/shard_map/all_to_all | solution.py:446
  55.4 0.8 copy-start.1
  56.2 1.0 copy-start.2
  57.6 23.8 %collective-permute-start = (bf16[8,128,256]{2,1,0:T(8,128)(2,1)S(1)}, bf16[8,128,256]{2,1,0:T(8,128)(2,1)}, u32[]{:S(2)}, u32[]{:S(2)}) collective-permute-start(bf16[8,128,256]{2,1,0:T(8,128)(2,1)S(1)} %norm.1.own_ref), channel_id=1, source_target_pairs={{0,4},{4,0},{1,5},{5,1},{2,6},{6,2},{3,7},{7,3},{8,12},{12,8},{9,1... | collective-permute-start | bytes 1572872 | tf_op jit(solution)/shard_map/ppermute | solution.py:28
  65.3 9.9 %collective-permute-start.4 = (bf16[256,512]{1,0:T(8,128)(2,1)}, bf16[256,512]{1,0:T(8,128)(2,1)S(1)}, u32[]{:S(2)}, u32[]{:S(2)}) collective-permute-start(bf16[256,512]{1,0:T(8,128)(2,1)} %slice.25), channel_id=1, source_target_pairs={{0,448},{64,0},{128,64},{192,128},{256,192},{320,256},{384,320},{4... | collective-permute-start | bytes 786440 | tf_op jit(solution)/shard_map/ppermute | solution.py:33
  70.4 11.0 %collective-permute-start.3 = (bf16[256,512]{1,0:T(8,128)(2,1)}, bf16[256,512]{1,0:T(8,128)(2,1)}, u32[]{:S(2)}, u32[]{:S(2)}) collective-permute-start(bf16[256,512]{1,0:T(8,128)(2,1)} %slice.24), channel_id=1, source_target_pairs={{0,64},{64,128},{128,192},{192,256},{256,320},{320,384},{384,448},... | collective-permute-start | bytes 786440 | tf_op jit(solution)/shard_map/ppermute | solution.py:33
  129.9 7.4 %collective-permute-start.5 = (bf16[8,320,128]{2,1,0:T(8,128)(2,1)S(1)}, bf16[8,320,128]{2,1,0:T(8,128)(2,1)S(1)}, u32[]{:S(2)}, u32[]{:S(2)}) collective-permute-start(bf16[8,320,128]{2,1,0:T(8,128)(2,1)S(1)} %all_to_all.36.spread_ref.mine_ref), channel_id=1, source_target_pairs={{0,4},{4,0},{1,5},{5,1},{2,6},{6,2},{3,7},{7,3},{8,12},{12,8},{9,1... | collective-permute-start | bytes 1966088 | tf_op jit(solution)/shard_map/ppermute | solution.py:28

commit v4 on v3

--- a/solution.py
+++ b/solution.py
@@ -33,11 +33,11 @@
     return lax.ppermute(value, Z, [(i, (i + step) % count) for i in range(count)])
 
 
-def two_steps(own, half):
+def around(own, half):
     before = shifted(own, 1)
     after = shifted(own, -1)
-    low = shifted(before[:half], 1)
-    high = shifted(after[half:], -1)
+    low = shifted(own[:half], 2)
+    high = shifted(own[half:], -2)
     return before, after, low, high
 
 
@@ -266,7 +266,7 @@
             preferred_element_type=jnp.float32,
         )
 
-    @pl.when(step >= z)
+    @pl.when(step >= 0)
     def _():
         q = q_ref[0]
         lane = lax.broadcasted_iota(jnp.int32, q.shape, 1)
@@ -285,7 +285,7 @@
 
         lax.fori_loop(0, (y * tokens) // KEYS + 1, body, 0)
 
-    @pl.when(step > z)
+    @pl.when(step != z)
     def _():
         for start in range(0, keys, KEYS):
             visit(start, KEYS, False)
@@ -440,7 +440,7 @@
     w_own, inputs, small = lax.optimization_barrier((w_own, inputs, small))
     features, norm_gain, att_lambda, att_gain, ret_gain = inputs
     even, ys, zs, chip, z, y, c, x = small
-    weights = (w_own, *two_steps(w_own, 2 * ny * rows))
+    weights = (w_own, *around(w_own, 2 * ny * rows))
     blocks = [high * nl + (z + k) % nl for k in (0, nl - 1, 1, 2) for high in range(2)]
 
     gathered = lax.all_to_all(features, "tp", 0, 0, tiled=True)

time: 209 us -> 200 us (0.957)
  waiting for transfers between devices: 16.3 us -> 2.84 us
  blocking collectives: 133 us -> 138 us
    ppermute x4, waiting for transfers between devices: 7.79 us -> 0.52 us  [shifted(): lax.ppermute(value, Z, [(i, (i + step) % count) for i in range(count)])]
    all_to_all x1, waiting for transfers between devices: 6.81 us -> 0.62 us  [layer(): gathered = lax.all_to_all(features, 'tp', 0, 0, tiled=True)]
    all_to_all x1, blocking collectives: 23.2 us -> 26.3 us  [layer(): along = lax.all_to_all(send, Z, 0, 0, tiled=True)]
    slice x2 -> x1, local copies, waits for them, and re-layouts: 3.36 us -> 0.83 us  [around(): high = shifted(own[half:], -2)]
  transfers between devices with their start and end apart: 7 -> 7, of which waited for: 4 -> 3; matrix products, arithmetic and copies ran while one was open for 2% -> 1% of each run, Pallas kernels for 0% -> 0%
where the time goes in v4:
time: 200 us
  blocking collectives  138 us (69%)
  starting transfers between devices  27.1 us (14%)
  Pallas kernels  24.8 us (12%)
  local copies, waits for them, and re-layouts  4.27 us (2%)
  waiting for transfers between devices  2.84 us (1%)
    all_to_all x1, blocking collectives, layer(): w_own = lax.all_to_all(sent, ('zh', 'y', 'c'), 0, 0, tiled=True)  37.6 us
    all_to_all x1, blocking collectives, layer(): parts = lax.all_to_all(parts, Z, 0, 0, tiled=True)  34.4 us
    all_to_all x1, blocking collectives, layer(): along = lax.all_to_all(send, Z, 0, 0, tiled=True)  26.3 us
    all_to_all x1, blocking collectives, layer(): spread = lax.all_to_all(send, 'y', 0, 0, tiled=True)  23.5 us
    pallas_call x1, Pallas kernels, attend(): pl.pallas_call(attend_kernel, grid_spec=pltpu.PrefetchScalarGridSpec(num_...  18.2 us
    all_to_all x1, blocking collectives, layer(): lax.all_to_all(partial.reshape(groups, -1, partial.shape[1]), 'tp', 0, 0,...  12.5 us
    ppermute x2, starting transfers between devices, swapped(): return lax.ppermute(value, 'c', [(0, 1), (1, 0)])  11.6 us
    ppermute x4, starting transfers between devices, shifted(): lax.ppermute(value, Z, [(i, (i + step) % count) for i in range(count)])  11.4 us
  transfers between devices with their start and end apart: 7, of which 3 were waited for; matrix products, arithmetic and copies ran while one was open for 1% of the time, Pallas kernels for 0%

profile of v4, /device:TPU:1, one launch (start us, length us, event | category | flops | bytes accessed | tf_op | source)
XLA Modules:
  0.0 199.7 jit_solution(13378284967538362720)
XLA Ops:
  0.0 1.3 pack.1
  1.3 0.8 copy-done.3
  2.2 37.6 %all_to_all.35 = bf16[32,16,512]{2,1,0:T(8,128)(2,1)S(1)} all-to-all(bf16[32,16,512]{2,1,0:T(8,128)(2,1)S(1)} %bitcast.35), channel_id=1, replica_groups=mesh['zh'=2,'zl'=4,'y'=8,'c'=2,'tp'=4] {'zh','y','c'}, dimensions={0} | all-to-all | bytes 1048576 | tf_op jit(solution)/shard_map/all_to_all | solution.py:437
  39.8 0.8 fusion.8
  40.6 2.3 %collective-permute-start.2 = (bf16[512,512]{1,0:T(8,128)(2,1)S(1)}, bf16[512,512]{1,0:T(8,128)(2,1)}, u32[]{:S(2)}, u32[]{:S(2)}) collective-permute-start(bf16[512,512]{1,0:T(8,128)(2,1)S(1)} %bitcast.32), channel_id=1, source_target_pairs={{0,448},{64,0},{128,64},{192,128},{256,192},{320,256},{384,320},{4... | collective-permute-start | bytes 1572872 | tf_op jit(solution)/shard_map/ppermute | solution.py:33
  42.9 3.0 %collective-permute-start.1 = (bf16[512,512]{1,0:T(8,128)(2,1)S(1)}, bf16[512,512]{1,0:T(8,128)(2,1)}, u32[]{:S(2)}, u32[]{:S(2)}) collective-permute-start(bf16[512,512]{1,0:T(8,128)(2,1)S(1)} %bitcast.33), channel_id=1, source_target_pairs={{0,64},{64,128},{128,192},{192,256},{256,320},{320,384},{384,448},... | collective-permute-start | bytes 1572872 | tf_op jit(solution)/shard_map/ppermute | solution.py:33
  46.1 4.0 %all-to-all-start.1 = ((bf16[4,128,512]{2,1,0:T(8,128)(2,1)}), bf16[4,128,512]{2,1,0:T(8,128)(2,1)S(1)}, u32[]{:S(2)}, u32[]{:S(2)}) async-start(bf16[4,128,512]{2,1,0:T(8,128)(2,1)} %copy-done.3), calls=%async_computation.1 | async-start | bytes 1048576 | tf_op jit(solution)/shard_map/all_to_all | solution.py:446
  50.1 2.3 %collective-permute-start.4 = (bf16[256,512]{1,0:T(8,128)(2,1)}, bf16[256,512]{1,0:T(8,128)(2,1)S(1)}, u32[]{:S(2)}, u32[]{:S(2)}) collective-permute-start(bf16[256,512]{1,0:T(8,128)(2,1)} %get-tuple-element.99), channel_id=1, source_target_pairs={{0,384},{64,448},{128,0},{192,64},{256,128},{320,192},{384,256},{4... | collective-permute-start | bytes 786440 | tf_op jit(solution)/shard_map/ppermute | solution.py:33
  52.4 3.9 %collective-permute-start.3 = (bf16[256,512]{1,0:T(8,128)(2,1)}, bf16[256,512]{1,0:T(8,128)(2,1)}, u32[]{:S(2)}, u32[]{:S(2)}) collective-permute-start(bf16[256,512]{1,0:T(8,128)(2,1)} %get-tuple-element.100), channel_id=1, source_target_pairs={{0,128},{64,192},{128,256},{192,320},{256,384},{320,448},{384,0},{... | collective-permute-start | bytes 786440 | tf_op jit(solution)/shard_map/ppermute | solution.py:33
  57.0 0.8 copy-done.1
  57.9 1.0 copy-done.2
  59.2 6.0 %collective-permute-start = (bf16[8,128,256]{2,1,0:T(8,128)(2,1)S(1)}, bf16[8,128,256]{2,1,0:T(8,128)(2,1)}, u32[]{:S(2)}, u32[]{:S(2)}) collective-permute-start(bf16[8,128,256]{2,1,0:T(8,128)(2,1)S(1)} %norm.1.own_ref), channel_id=1, source_target_pairs={{0,4},{4,0},{1,5},{5,1},{2,6},{6,2},{3,7},{7,3},{8,12},{12,8},{9,1... | collective-permute-start | bytes 1572872 | tf_op jit(solution)/shard_map/ppermute | solution.py:28
  65.2 0.6 dynamic_slice.4
  67.1 2.7 %project.1 = (bf16[8,320,128]{2,1,0:T(8,128)(2,1)S(1)}, bf16[256,128]{1,0:T(8,128)(2,1)S(1)}, f32[256,64]{1,0:T(8,128)S(1)}, f32[256,128]{1,0:T(8,128)S(1)}) custom-call(bf16[8,128,256]{2,1,0:T(8,128)(2,1)S(1)} %norm.1.own_ref, bf16[8,128,256]{2,1,0:T(8,128)(2,1)} %collective-permute-done.across_ref, bf16[512,512]{1,0:T(8,128)(2,1)S(1)} %bitcast.34, ...), custom_call_target="tpu_custom_call" | custom-call | tf_op jit(solution)/shard_map/project/pallas_call | solution.py:191
  69.7 23.5 %all_to_all.36.spread_ref.mine_ref = bf16[8,320,128]{2,1,0:T(8,128)(2,1)S(1)} all-to-all(bf16[8,320,128]{2,1,0:T(8,128)(2,1)S(1)} %get-tuple-element.89), channel_id=1, replica_groups=mesh['zh'=2,'zl'=4,'y'=8,'c'=2,'tp'=4] {'y'}, dimensions={0} | all-to-all | bytes 1310720 | tf_op jit(solution)/shard_map/all_to_all | solution.py:477
  93.8 26.3 %all_to_all.37.q_ref.along_ref = bf16[8,320,128]{2,1,0:T(8,128)(2,1)S(1)} all-to-all(bf16[8,320,128]{2,1,0:T(8,128)(2,1)S(1)} %pass_on.1), channel_id=1, replica_groups=mesh['zh'=2,'zl'=4,'y'=8,'c'=2,'tp'=4] {'zh','zl'}, dimensions={0} | all-to-all | bytes 1310720 | tf_op jit(solution)/shard_map/all_to_all | solution.py:479
  120.2 5.7 %collective-permute-start.5 = (bf16[8,320,128]{2,1,0:T(8,128)(2,1)S(1)}, bf16[8,320,128]{2,1,0:T(8,128)(2,1)S(1)}, u32[]{:S(2)}, u32[]{:S(2)}) collective-permute-start(bf16[8,320,128]{2,1,0:T(8,128)(2,1)S(1)} %all_to_all.36.spread_ref.mine_ref), channel_id=1, source_target_pairs={{0,4},{4,0},{1,5},{5,1},{2,6},{6,2},{3,7},{7,3},{8,12},{12,8},{9,1... | collective-permute-start | bytes 1966088 | tf_op jit(solution)/shard_map/ppermute | solution.py:28
  125.8 1.7 collective-permute-done.5.other_ref
  127.5 18.2 %attend.1 = bf16[8,144,512]{2,1,0:T(8,128)(2,1)S(1)} custom-call(s32[3]{0:T(128)S(1)} %pad_add_fusion.where_ref, bf16[8,320,128]{2,1,0:T(8,128)(2,1)S(1)} %all_to_all.37.q_ref.along_ref, bf16[8,320,128]{2,1,0:T(8,128)(2,1)S(1)} %all_to_all.36.spread_ref.mine_ref, bf16[8,320,128]{2,1,0:T(8,128)(2,1)S(1)} %collective-permute-done.5.other_ref), custom_call_target="tpu_custom_call" | custom-call | flops 4294967296 | bytes 3145728 | tf_op jit(solution)/shard_map/attend/pallas_call | solution.py:319
  145.8 34.4 %all_to_all.38.parts_ref = bf16[8,144,512]{2,1,0:T(8,128)(2,1)S(1)} all-to-all(bf16[8,144,512]{2,1,0:T(8,128)(2,1)S(1)} %attend.1), channel_id=1, replica_groups=mesh['zh'=2,'zl'=4,'y'=8,'c'=2,'tp'=4] {'zh','zl'}, dimensions={0} | all-to-all | bytes 2359296 | tf_op jit(solution)/shard_map/all_to_all | solution.py:482
  180.1 1.8 finish.1
  181.9 4.0 %all_to_all.39 = bf16[2,128,256]{2,1,0:T(8,128)(2,1)S(1)} all-to-all(bf16[2,128,256]{2,1,0:T(8,128)(2,1)S(1)} %finish.1), channel_id=1, replica_groups=mesh['zh'=2,'zl'=4,'y'=8,'c'=2,'tp'=4] {'c'}, dimensions={0} | all-to-all | bytes 262144 | tf_op jit(solution)/shard_map/all_to_all | solution.py:485
  186.4 12.5 %all_to_all.40 = bf16[4,32,2048]{2,1,0:T(8,128)(2,1)S(1)} all-to-all(bf16[4,32,2048]{2,1,0:T(8,128)(2,1)S(1)} %bitcast.37), channel_id=1, replica_groups=mesh['zh'=2,'zl'=4,'y'=8,'c'=2,'tp'=4] {'tp'}, dimensions={0} | all-to-all | bytes 1048576 | tf_op jit(solution)/shard_map/all_to_all | solution.py:492
  198.9 0.8 convert_reduce_fusion
  (33 shorter events, 3.3 us)
Async XLA Ops:
  0.0 185.9 %copy-start = (bf16[2,256,2048]{2,1,0:T(8,128)(2,1)S(1)}, bf16[2,256,2048]{2,1,0:T(8,128)(2,1)}, u32[]{:S(2)}) copy-start(bf16[2,256,2048]{2,1,0:T(8,128)(2,1)} %param.23) | copy-start | bytes 6291460
  0.0 56.4 %copy-start.5 = (f32[128]{0:T(128)S(1)}, f32[128]{0:T(128)}, u32[]{:S(2)}) copy-start(f32[128]{0:T(128)} %param.22) | copy-start | bytes 1540
  0.0 56.4 %copy-start.6 = (f32[128]{0:T(128)S(1)}, f32[128]{0:T(128)}, u32[]{:S(2)}) copy-start(f32[128]{0:T(128)} %param.18) | copy-start | bytes 1540
  0.0 57.8 %copy-start.4 = (f32[2048]{0:T(1024)S(1)}, f32[2048]{0:T(1024)}, u32[]{:S(2)}) copy-start(f32[2048]{0:T(1024)} %param.13) | copy-start | bytes 24580
  1.3 0.8 copy-start.3
  2.2 63.1 %copy-start.7 = (f32[2]{0:T(128)S(1)}, f32[2]{0:T(128)}, u32[]{:S(2)}) copy-start(f32[2]{0:T(128)} %param.17) | copy-start | bytes 28
  40.6 26.4 %collective-permute-start.2 = (bf16[512,512]{1,0:T(8,128)(2,1)S(1)}, bf16[512,512]{1,0:T(8,128)(2,1)}, u32[]{:S(2)}, u32[]{:S(2)}) collective-permute-start(bf16[512,512]{1,0:T(8,128)(2,1)S(1)} %bitcast.32), channel_id=1, source_target_pairs={{0,448},{64,0},{128,64},{192,128},{256,192},{320,256},{384,320},{4... | collective-permute-start | bytes 1572872 | tf_op jit(solution)/shard_map/ppermute | solution.py:33
  42.9 24.2 %collective-permute-start.1 = (bf16[512,512]{1,0:T(8,128)(2,1)S(1)}, bf16[512,512]{1,0:T(8,128)(2,1)}, u32[]{:S(2)}, u32[]{:S(2)}) collective-permute-start(bf16[512,512]{1,0:T(8,128)(2,1)S(1)} %bitcast.33), channel_id=1, source_target_pairs={{0,64},{64,128},{128,192},{192,256},{256,320},{320,384},{384,448},... | collective-permute-start | bytes 1572872 | tf_op jit(solution)/shard_map/ppermute | solution.py:33
  46.1 11.0 %all-to-all-start.1 = ((bf16[4,128,512]{2,1,0:T(8,128)(2,1)}), bf16[4,128,512]{2,1,0:T(8,128)(2,1)S(1)}, u32[]{:S(2)}, u32[]{:S(2)}) async-start(bf16[4,128,512]{2,1,0:T(8,128)(2,1)} %copy-done.3), calls=%async_computation.1 | async-start | bytes 1048576 | tf_op jit(solution)/shard_map/all_to_all | solution.py:446
  50.1 16.9 %collective-permute-start.4 = (bf16[256,512]{1,0:T(8,128)(2,1)}, bf16[256,512]{1,0:T(8,128)(2,1)S(1)}, u32[]{:S(2)}, u32[]{:S(2)}) collective-permute-start(bf16[256,512]{1,0:T(8,128)(2,1)} %get-tuple-element.99), channel_id=1, source_target_pairs={{0,384},{64,448},{128,0},{192,64},{256,128},{320,192},{384,256},{4... | collective-permute-start | bytes 786440 | tf_op jit(solution)/shard_map/ppermute | solution.py:33
  52.4 14.7 %collective-permute-start.3 = (bf16[256,512]{1,0:T(8,128)(2,1)}, bf16[256,512]{1,0:T(8,128)(2,1)}, u32[]{:S(2)}, u32[]{:S(2)}) collective-permute-start(bf16[256,512]{1,0:T(8,128)(2,1)} %get-tuple-element.100), channel_id=1, source_target_pairs={{0,128},{64,192},{128,256},{192,320},{256,384},{320,448},{384,0},{... | collective-permute-start | bytes 786440 | tf_op jit(solution)/shard_map/ppermute | solution.py:33
  57.0 0.8 copy-start.1
  57.9 1.0 copy-start.2
  59.2 7.9 %collective-permute-start = (bf16[8,128,256]{2,1,0:T(8,128)(2,1)S(1)}, bf16[8,128,256]{2,1,0:T(8,128)(2,1)}, u32[]{:S(2)}, u32[]{:S(2)}) collective-permute-start(bf16[8,128,256]{2,1,0:T(8,128)(2,1)S(1)} %norm.1.own_ref), channel_id=1, source_target_pairs={{0,4},{4,0},{1,5},{5,1},{2,6},{6,2},{3,7},{7,3},{8,12},{12,8},{9,1... | collective-permute-start | bytes 1572872 | tf_op jit(solution)/shard_map/ppermute | solution.py:28
  120.2 7.4 %collective-permute-start.5 = (bf16[8,320,128]{2,1,0:T(8,128)(2,1)S(1)}, bf16[8,320,128]{2,1,0:T(8,128)(2,1)S(1)}, u32[]{:S(2)}, u32[]{:S(2)}) collective-permute-start(bf16[8,320,128]{2,1,0:T(8,128)(2,1)S(1)} %all_to_all.36.spread_ref.mine_ref), channel_id=1, source_target_pairs={{0,4},{4,0},{1,5},{5,1},{2,6},{6,2},{3,7},{7,3},{8,12},{12,8},{9,1... | collective-permute-start | bytes 1966088 | tf_op jit(solution)/shard_map/ppermute | solution.py:28

commit v5 on v4

--- a/solution.py
+++ b/solution.py
@@ -266,7 +266,7 @@
             preferred_element_type=jnp.float32,
         )
 
-    @pl.when(step >= 0)
+    @pl.when(step >= z)
     def _():
         q = q_ref[0]
         lane = lax.broadcasted_iota(jnp.int32, q.shape, 1)
@@ -285,7 +285,7 @@
 
         lax.fori_loop(0, (y * tokens) // KEYS + 1, body, 0)
 
-    @pl.when(step != z)
+    @pl.when(step > z)
     def _():
         for start in range(0, keys, KEYS):
             visit(start, KEYS, False)
@@ -477,8 +477,8 @@
     spread = lax.all_to_all(send, "y", 0, 0, tiled=True)
     send = pass_on(spread, att, to_end, nz)
     along = lax.all_to_all(send, Z, 0, 0, tiled=True)
-    spread, along = lax.optimization_barrier((spread, along))
-    parts = attend(where, along, spread, swapped(spread), tokens)
+    other = swapped(spread)
+    parts = attend(where, along, spread, other, tokens)
     parts = lax.all_to_all(parts, Z, 0, 0, tiled=True)
 
     heads = finish(parts, mixing, gains, spread, along, before, query, within)

time: 200 us -> 198 us (0.990)
  the two profiles are of different devices: /device:TPU:1 before, /device:TPU:48 now
where the time goes in v5:
time: 198 us; the launch traced here: 197 us
  blocking collectives  108 us (55%)
  starting transfers between devices  30.1 us (15%)
  Pallas kernels  27.9 us (14%)
  waiting for transfers between devices  22.5 us (11%)
  local copies, waits for them, and re-layouts  6.18 us (3%)
  other arithmetic  2.04 us (1%)
    all_to_all x1, blocking collectives, layer(): parts = lax.all_to_all(parts, Z, 0, 0, tiled=True)  34.5 us
    all_to_all x1, blocking collectives, layer(): w_own = lax.all_to_all(sent, ('zh', 'y', 'c'), 0, 0, tiled=True)  34 us
    all_to_all x1, blocking collectives, layer(): spread = lax.all_to_all(send, 'y', 0, 0, tiled=True)  21.7 us
    pallas_call x1, Pallas kernels, attend(): pl.pallas_call(attend_kernel, grid_spec=pltpu.PrefetchScalarGridSpec(num_...  20.5 us
    all_to_all x1, waiting for transfers between devices, layer(): along = lax.all_to_all(send, Z, 0, 0, tiled=True)  15.1 us
    all_to_all x1, blocking collectives, layer(): lax.all_to_all(partial.reshape(groups, -1, partial.shape[1]), 'tp', 0, 0,...  13.8 us
    ppermute x4, starting transfers between devices, shifted(): lax.ppermute(value, Z, [(i, (i + step) % count) for i in range(count)])  12.6 us
    all_to_all x1, starting transfers between devices, layer(): along = lax.all_to_all(send, Z, 0, 0, tiled=True)  9.35 us
  transfers between devices with their start and end apart: 8, of which 4 were waited for; matrix products, arithmetic and copies ran while one was open for 1% of the time, Pallas kernels for 0%

profile of v5, /device:TPU:48, one launch (start us, length us, event | category | flops | bytes accessed | tf_op | source)
XLA Modules:
  0.0 197.5 jit_solution(9565701075508171271)
XLA Ops:
  0.0 1.3 pack.1
  2.2 34.0 %all_to_all.35 = bf16[32,16,512]{2,1,0:T(8,128)(2,1)S(1)} all-to-all(bf16[32,16,512]{2,1,0:T(8,128)(2,1)S(1)} %bitcast.35), channel_id=1, replica_groups=mesh['zh'=2,'zl'=4,'y'=8,'c'=2,'tp'=4] {'zh','y','c'}, dimensions={0} | all-to-all | bytes 1048576 | tf_op jit(solution)/shard_map/all_to_all | solution.py:437
  37.0 3.2 %collective-permute-start.2 = (bf16[512,512]{1,0:T(8,128)(2,1)S(1)}, bf16[512,512]{1,0:T(8,128)(2,1)}, u32[]{:S(2)}, u32[]{:S(2)}) collective-permute-start(bf16[512,512]{1,0:T(8,128)(2,1)S(1)} %bitcast.32), channel_id=1, source_target_pairs={{0,448},{64,0},{128,64},{192,128},{256,192},{320,256},{384,320},{4... | collective-permute-start | bytes 1572872 | tf_op jit(solution)/shard_map/ppermute | solution.py:33
  40.3 2.6 %collective-permute-start.1 = (bf16[512,512]{1,0:T(8,128)(2,1)S(1)}, bf16[512,512]{1,0:T(8,128)(2,1)}, u32[]{:S(2)}, u32[]{:S(2)}) collective-permute-start(bf16[512,512]{1,0:T(8,128)(2,1)S(1)} %bitcast.33), channel_id=1, source_target_pairs={{0,64},{64,128},{128,192},{192,256},{256,320},{320,384},{384,448},... | collective-permute-start | bytes 1572872 | tf_op jit(solution)/shard_map/ppermute | solution.py:33
  43.1 4.3 %all-to-all-start.1 = ((bf16[4,128,512]{2,1,0:T(8,128)(2,1)}), bf16[4,128,512]{2,1,0:T(8,128)(2,1)S(1)}, u32[]{:S(2)}, u32[]{:S(2)}) async-start(bf16[4,128,512]{2,1,0:T(8,128)(2,1)} %copy-done.3), calls=%async_computation.1 | async-start | bytes 1048576 | tf_op jit(solution)/shard_map/all_to_all | solution.py:446
  47.4 3.2 %collective-permute-start.4 = (bf16[256,512]{1,0:T(8,128)(2,1)}, bf16[256,512]{1,0:T(8,128)(2,1)S(1)}, u32[]{:S(2)}, u32[]{:S(2)}) collective-permute-start(bf16[256,512]{1,0:T(8,128)(2,1)} %get-tuple-element.95), channel_id=1, source_target_pairs={{0,384},{64,448},{128,0},{192,64},{256,128},{320,192},{384,256},{4... | collective-permute-start | bytes 786440 | tf_op jit(solution)/shard_map/ppermute | solution.py:33
  50.6 3.5 %collective-permute-start.3 = (bf16[256,512]{1,0:T(8,128)(2,1)}, bf16[256,512]{1,0:T(8,128)(2,1)}, u32[]{:S(2)}, u32[]{:S(2)}) collective-permute-start(bf16[256,512]{1,0:T(8,128)(2,1)} %get-tuple-element.96), channel_id=1, source_target_pairs={{0,128},{64,192},{128,256},{192,320},{256,384},{320,448},{384,0},{... | collective-permute-start | bytes 786440 | tf_op jit(solution)/shard_map/ppermute | solution.py:33
  54.3 2.9 %all-to-all-done.1.gathered_ref = bf16[4,128,512]{2,1,0:T(8,128)(2,1)S(1)} async-done(((bf16[4,128,512]{2,1,0:T(8,128)(2,1)}), bf16[4,128,512]{2,1,0:T(8,128)(2,1)S(1)}, u32[]{:S(2)}, u32[]{:S(2)}) %all-to-all-start.1) | async-done | bytes 524320 | tf_op jit(solution)/shard_map/all_to_all | solution.py:446
  58.0 1.0 copy-done.2
  59.3 1.9 collective-permute-start
  63.1 2.5 %collective-permute-done.4.w_high_ref = bf16[256,512]{1,0:T(8,128)(2,1)S(1)} collective-permute-done((bf16[256,512]{1,0:T(8,128)(2,1)}, bf16[256,512]{1,0:T(8,128)(2,1)S(1)}, u32[]{:S(2)}, u32[]{:S(2)}) %collective-permute-start.4) | collective-permute-done | bytes 262176 | tf_op jit(solution)/shard_map/ppermute | solution.py:33
  65.6 2.7 %project.1 = (bf16[8,320,128]{2,1,0:T(8,128)(2,1)S(1)}, bf16[256,128]{1,0:T(8,128)(2,1)S(1)}, f32[256,64]{1,0:T(8,128)S(1)}, f32[256,128]{1,0:T(8,128)S(1)}) custom-call(bf16[8,128,256]{2,1,0:T(8,128)(2,1)S(1)} %norm.1.own_ref, bf16[8,128,256]{2,1,0:T(8,128)(2,1)} %collective-permute-done.across_ref, bf16[512,512]{1,0:T(8,128)(2,1)S(1)} %bitcast.34, ...), custom_call_target="tpu_custom_call" | custom-call | tf_op jit(solution)/shard_map/project/pallas_call | solution.py:191
  68.2 21.7 %all_to_all.36.spread_ref.mine_ref = bf16[8,320,128]{2,1,0:T(8,128)(2,1)S(1)} all-to-all(bf16[8,320,128]{2,1,0:T(8,128)(2,1)S(1)} %get-tuple-element.87), channel_id=1, replica_groups=mesh['zh'=2,'zl'=4,'y'=8,'c'=2,'tp'=4] {'y'}, dimensions={0} | all-to-all | bytes 1310720 | tf_op jit(solution)/shard_map/all_to_all | solution.py:477
  89.9 1.5 pass_on.1
  91.4 9.4 %all-to-all-start.3 = ((bf16[8,320,128]{2,1,0:T(8,128)(2,1)}), bf16[8,320,128]{2,1,0:T(8,128)(2,1)S(1)}, u32[]{:S(2)}, u32[]{:S(2)}) async-start(bf16[8,320,128]{2,1,0:T(8,128)(2,1)} %pass_on.1), calls=%async_computation.3 | async-start | bytes 1310720 | tf_op jit(solution)/shard_map/all_to_all | solution.py:479
  100.8 1.9 collective-permute-start.5
  102.7 2.1 %collective-permute-done.5.other_ref = bf16[8,320,128]{2,1,0:T(8,128)(2,1)S(1)} collective-permute-done((bf16[8,320,128]{2,1,0:T(8,128)(2,1)S(1)}, bf16[8,320,128]{2,1,0:T(8,128)(2,1)S(1)}, u32[]{:S(2)}, u32[]{:S(2)}) %collective-permute-start.5) | collective-permute-done | bytes 655392 | tf_op jit(solution)/shard_map/ppermute | solution.py:28
  105.6 15.1 %all-to-all-done.3.q_ref.along_ref = bf16[8,320,128]{2,1,0:T(8,128)(2,1)S(1)} async-done(((bf16[8,320,128]{2,1,0:T(8,128)(2,1)}), bf16[8,320,128]{2,1,0:T(8,128)(2,1)S(1)}, u32[]{:S(2)}, u32[]{:S(2)}) %all-to-all-start.3) | async-done | bytes 655392 | tf_op jit(solution)/shard_map/all_to_all | solution.py:479
  120.7 1.1 copy-done.9
  121.8 20.5 %attend.1 = bf16[8,144,512]{2,1,0:T(8,128)(2,1)S(1)} custom-call(s32[3]{0:T(128)S(1)} %copy-done.7, bf16[8,320,128]{2,1,0:T(8,128)(2,1)S(1)} %all-to-all-done.3.q_ref.along_ref, bf16[8,320,128]{2,1,0:T(8,128)(2,1)S(1)} %all_to_all.36.spread_ref.mine_ref, bf16[8,320,128]{2,1,0:T(8,128)(2,1)S(1)} %copy-done.9), custom_call_target="tpu_custom_call" | custom-call | flops 4294967296 | bytes 3145728 | tf_op jit(solution)/shard_map/attend/pallas_call | solution.py:319
  142.3 34.5 %all_to_all.37.parts_ref = bf16[8,144,512]{2,1,0:T(8,128)(2,1)S(1)} all-to-all(bf16[8,144,512]{2,1,0:T(8,128)(2,1)S(1)} %attend.1), channel_id=1, replica_groups=mesh['zh'=2,'zl'=4,'y'=8,'c'=2,'tp'=4] {'zh','zl'}, dimensions={0} | all-to-all | bytes 2359296 | tf_op jit(solution)/shard_map/all_to_all | solution.py:482
  176.8 1.7 finish.1
  178.6 3.8 %all_to_all.38 = bf16[2,128,256]{2,1,0:T(8,128)(2,1)S(1)} all-to-all(bf16[2,128,256]{2,1,0:T(8,128)(2,1)S(1)} %finish.1), channel_id=1, replica_groups=mesh['zh'=2,'zl'=4,'y'=8,'c'=2,'tp'=4] {'c'}, dimensions={0} | all-to-all | bytes 262144 | tf_op jit(solution)/shard_map/all_to_all | solution.py:485
  182.9 13.8 %all_to_all.39 = bf16[4,32,2048]{2,1,0:T(8,128)(2,1)S(1)} all-to-all(bf16[4,32,2048]{2,1,0:T(8,128)(2,1)S(1)} %bitcast.37), channel_id=1, replica_groups=mesh['zh'=2,'zl'=4,'y'=8,'c'=2,'tp'=4] {'tp'}, dimensions={0} | all-to-all | bytes 1048576 | tf_op jit(solution)/shard_map/all_to_all | solution.py:492
  (44 shorter events, 6.8 us)
Async XLA Ops:
  0.0 182.4 %copy-start = (bf16[2,256,2048]{2,1,0:T(8,128)(2,1)S(1)}, bf16[2,256,2048]{2,1,0:T(8,128)(2,1)}, u32[]{:S(2)}) copy-start(bf16[2,256,2048]{2,1,0:T(8,128)(2,1)} %param.23) | copy-start | bytes 6291460
  0.0 54.2 %copy-start.10 = (f32[128]{0:T(128)S(1)}, f32[128]{0:T(128)}, u32[]{:S(2)}) copy-start(f32[128]{0:T(128)} %param.22) | copy-start | bytes 1540
  0.0 54.2 %copy-start.11 = (f32[128]{0:T(128)S(1)}, f32[128]{0:T(128)}, u32[]{:S(2)}) copy-start(f32[128]{0:T(128)} %param.18) | copy-start | bytes 1540
  0.0 58.0 %copy-start.6 = (f32[2048]{0:T(1024)S(1)}, f32[2048]{0:T(1024)}, u32[]{:S(2)}) copy-start(f32[2048]{0:T(1024)} %param.13) | copy-start | bytes 24580
  1.3 0.8 copy-start.3
  2.2 59.7 %copy-start.12 = (f32[2]{0:T(128)S(1)}, f32[2]{0:T(128)}, u32[]{:S(2)}) copy-start(f32[2]{0:T(128)} %param.17) | copy-start | bytes 28
  37.0 28.5 %collective-permute-start.2 = (bf16[512,512]{1,0:T(8,128)(2,1)S(1)}, bf16[512,512]{1,0:T(8,128)(2,1)}, u32[]{:S(2)}, u32[]{:S(2)}) collective-permute-start(bf16[512,512]{1,0:T(8,128)(2,1)S(1)} %bitcast.32), channel_id=1, source_target_pairs={{0,448},{64,0},{128,64},{192,128},{256,192},{320,256},{384,320},{4... | collective-permute-start | bytes 1572872 | tf_op jit(solution)/shard_map/ppermute | solution.py:33
  40.3 25.3 %collective-permute-start.1 = (bf16[512,512]{1,0:T(8,128)(2,1)S(1)}, bf16[512,512]{1,0:T(8,128)(2,1)}, u32[]{:S(2)}, u32[]{:S(2)}) collective-permute-start(bf16[512,512]{1,0:T(8,128)(2,1)S(1)} %bitcast.33), channel_id=1, source_target_pairs={{0,64},{64,128},{128,192},{192,256},{256,320},{320,384},{384,448},... | collective-permute-start | bytes 1572872 | tf_op jit(solution)/shard_map/ppermute | solution.py:33
  43.1 14.1 %all-to-all-start.1 = ((bf16[4,128,512]{2,1,0:T(8,128)(2,1)}), bf16[4,128,512]{2,1,0:T(8,128)(2,1)S(1)}, u32[]{:S(2)}, u32[]{:S(2)}) async-start(bf16[4,128,512]{2,1,0:T(8,128)(2,1)} %copy-done.3), calls=%async_computation.1 | async-start | bytes 1048576 | tf_op jit(solution)/shard_map/all_to_all | solution.py:446
  47.4 18.1 %collective-permute-start.4 = (bf16[256,512]{1,0:T(8,128)(2,1)}, bf16[256,512]{1,0:T(8,128)(2,1)S(1)}, u32[]{:S(2)}, u32[]{:S(2)}) collective-permute-start(bf16[256,512]{1,0:T(8,128)(2,1)} %get-tuple-element.95), channel_id=1, source_target_pairs={{0,384},{64,448},{128,0},{192,64},{256,128},{320,192},{384,256},{4... | collective-permute-start | bytes 786440 | tf_op jit(solution)/shard_map/ppermute | solution.py:33
  50.6 14.9 %collective-permute-start.3 = (bf16[256,512]{1,0:T(8,128)(2,1)}, bf16[256,512]{1,0:T(8,128)(2,1)}, u32[]{:S(2)}, u32[]{:S(2)}) collective-permute-start(bf16[256,512]{1,0:T(8,128)(2,1)} %get-tuple-element.96), channel_id=1, source_target_pairs={{0,128},{64,192},{128,256},{192,320},{256,384},{320,448},{384,0},{... | collective-permute-start | bytes 786440 | tf_op jit(solution)/shard_map/ppermute | solution.py:33
  57.2 0.8 copy-start.1
  58.0 1.0 copy-start.2
  59.3 6.2 %collective-permute-start = (bf16[8,128,256]{2,1,0:T(8,128)(2,1)S(1)}, bf16[8,128,256]{2,1,0:T(8,128)(2,1)}, u32[]{:S(2)}, u32[]{:S(2)}) collective-permute-start(bf16[8,128,256]{2,1,0:T(8,128)(2,1)S(1)} %norm.1.own_ref), channel_id=1, source_target_pairs={{0,4},{4,0},{1,5},{5,1},{2,6},{6,2},{3,7},{7,3},{8,12},{12,8},{9,1... | collective-permute-start | bytes 1572872 | tf_op jit(solution)/shard_map/ppermute | solution.py:28
  68.2 21.7 %copy-start.4 = (f32[256,128]{1,0:T(8,128)}, f32[256,128]{1,0:T(8,128)S(1)}, u32[]{:S(2)}) copy-start(f32[256,128]{1,0:T(8,128)S(1)} %get-tuple-element.94.within_ref) | copy-start | bytes 393220
  68.2 52.5 %copy-start.7 = (s32[3]{0:T(128)S(1)}, s32[3]{0:T(128)}, u32[]{:S(2)}) copy-start(s32[3]{0:T(128)} %pad_add_fusion.where_ref) | copy-start | bytes 40
  91.4 29.3 %all-to-all-start.3 = ((bf16[8,320,128]{2,1,0:T(8,128)(2,1)}), bf16[8,320,128]{2,1,0:T(8,128)(2,1)S(1)}, u32[]{:S(2)}, u32[]{:S(2)}) async-start(bf16[8,320,128]{2,1,0:T(8,128)(2,1)} %pass_on.1), calls=%async_computation.3 | async-start | bytes 1310720 | tf_op jit(solution)/shard_map/all_to_all | solution.py:479
  100.8 4.0 %collective-permute-start.5 = (bf16[8,320,128]{2,1,0:T(8,128)(2,1)S(1)}, bf16[8,320,128]{2,1,0:T(8,128)(2,1)S(1)}, u32[]{:S(2)}, u32[]{:S(2)}) collective-permute-start(bf16[8,320,128]{2,1,0:T(8,128)(2,1)S(1)} %all_to_all.36.spread_ref.mine_ref), channel_id=1, source_target_pairs={{0,4},{4,0},{1,5},{5,1},{2,6},{6,2},{3,7},{7,3},{8,12},{12,8},{9,1... | collective-permute-start | bytes 1966088 | tf_op jit(solution)/shard_map/ppermute | solution.py:28
  104.8 0.9 copy-start.8
  120.7 1.1 copy-start.9
  142.3 34.6 %copy-start.5 = (f32[256,128]{1,0:T(8,128)S(1)}, f32[256,128]{1,0:T(8,128)}, u32[]{:S(2)}) copy-start(f32[256,128]{1,0:T(8,128)} %copy-done.4) | copy-start | bytes 393220

commit v6 on v5

--- a/solution.py
+++ b/solution.py
@@ -17,10 +17,11 @@
 EPSILON = 1e-06
 NEG = -1e30
 KEYS = 512
-ROWS = 144
+ROWS = 136
 MIB = 1 << 20
 VMEM = pl.BlockSpec(memory_space=pltpu.VMEM)
 SMEM = pl.BlockSpec(memory_space=pltpu.SMEM)
+HBM = pl.BlockSpec(memory_space=pltpu.HBM)
 INTERPRET = False
 
 
@@ -74,7 +75,7 @@
     rows = arrays[0].shape[0]
     return pl.pallas_call(
         pack_kernel,
-        in_specs=[pl.BlockSpec(memory_space=pltpu.HBM)] * len(arrays),
+        in_specs=[HBM] * len(arrays),
         out_shape=[
             jax.ShapeDtypeStruct((count, 2, rows, 512), jnp.bfloat16),
             jax.ShapeDtypeStruct((groups, *arrays[-1].shape), jnp.bfloat16),
@@ -96,12 +97,18 @@
     )
 
 
-def norm_kernel(gathered_ref, gain_ref, out_ref):
+def norm_kernel(far_ref, gain_ref, out_ref, gathered_ref, sems):
     groups = gathered_ref.shape[0]
     blocks, _, wide = out_ref.shape
     per_tp = blocks // groups
+    copies = [
+        pltpu.make_async_copy(far_ref.at[g], gathered_ref.at[g], sems.at[g]) for g in range(groups)
+    ]
+    for copy in copies:
+        copy.start()
     total = 0.0
     for g in range(groups):
+        copies[g].wait()
         floats = gathered_ref[g].astype(jnp.float32)
         total = total + jnp.sum(floats * floats, axis=1, keepdims=True)
     scale = lax.rsqrt(total / (blocks * wide) + EPSILON)
@@ -116,12 +123,16 @@
     wide = width * groups // blocks
     return pl.pallas_call(
         norm_kernel,
-        in_specs=[VMEM, VMEM],
+        in_specs=[HBM, VMEM],
         out_shape=jax.ShapeDtypeStruct((blocks, rows, wide), jnp.bfloat16),
+        scratch_shapes=[
+            pltpu.VMEM(gathered.shape, gathered.dtype),
+            pltpu.SemaphoreType.DMA((groups,)),
+        ],
         compiler_params=pltpu.CompilerParams(vmem_limit_bytes=6 * MIB),
         name="norm",
         interpret=INTERPRET,
-    )(gathered, gain.reshape(blocks, 1, wide))
+    )(pltpu.with_memory_space_constraint(gathered, pltpu.HBM), gain.reshape(blocks, 1, wide))
 
 
 def project_kernel(
@@ -225,27 +236,55 @@
 
 
 def attend_kernel(
-    where_ref, q_ref, mine_ref, other_ref, out_ref, k_ref, vt_ref, qt_ref, m_ref, l_ref, o_ref
+    where_ref,
+    q_ref,
+    mine_ref,
+    far_ref,
+    out_ref,
+    other_ref,
+    k_ref,
+    vt_ref,
+    qt_ref,
+    m_ref,
+    l_ref,
+    o_ref,
+    sem,
 ):
-    step = pl.program_id(0)
+    copy = pltpu.make_async_copy(far_ref, other_ref, sem)
+    copy.start()
     z = where_ref[0]
     y = where_ref[1]
     keys = k_ref.shape[0]
-    tokens = q_ref.shape[1]
-
-    def prepare(key_ref, value_ref):
-        for i in range(key_ref.shape[0]):
-            at = slice(i * tokens, (i + 1) * tokens)
-            k_ref[at] = key_ref[i, :tokens]
-            vt_ref[:, at] = value_ref[i, :tokens].T
-
-    @pl.when((step == 0) & (where_ref[2] == 0))
+    blocks = out_ref.shape[0]
+    tokens = out_ref.shape[2] // 2
+
+    first = where_ref[2] == 0
+
+    def take_keys(ref):
+        for i in range(ref.shape[0]):
+            k_ref[i * tokens : (i + 1) * tokens] = ref[i, :tokens]
+
+    def take_values(ref):
+        for i in range(ref.shape[0]):
+            vt_ref[:, i * tokens : (i + 1) * tokens] = ref[i, :tokens].T
+
+    @pl.when(first)
     def _():
-        prepare(mine_ref, other_ref)
-
-    @pl.when((step == 0) & (where_ref[2] != 0))
+        take_keys(mine_ref)
+
+    @pl.when(jnp.logical_not(first))
     def _():
-        prepare(other_ref, mine_ref)
+        take_values(mine_ref)
+
+    copy.wait()
+
+    @pl.when(first)
+    def _():
+        take_values(other_ref)
+
+    @pl.when(jnp.logical_not(first))
+    def _():
+        take_keys(other_ref)
 
     def visit(start, count, masked):
         s = jnp.dot(k_ref[pl.ds(start, count)], qt_ref[...], preferred_element_type=jnp.float32)
@@ -266,9 +305,14 @@
             preferred_element_type=jnp.float32,
         )
 
-    @pl.when(step >= z)
-    def _():
-        q = q_ref[0]
+    def empty(step, _):
+        out_ref[step, :DV] = jnp.zeros((DV, 2 * tokens), jnp.bfloat16)
+        row = lax.broadcasted_iota(jnp.int32, (ROWS - DV, 2 * tokens), 0)
+        out_ref[step, DV:] = jnp.where(row == 0, NEG, 0.0).astype(jnp.bfloat16)
+        return 0
+
+    def begin(step):
+        q = q_ref[step, :tokens]
         lane = lax.broadcasted_iota(jnp.int32, q.shape, 1)
         zero = jnp.zeros_like(q)
         q = jnp.concatenate([jnp.where(lane < DH, q, zero), jnp.where(lane < DH, zero, q)], axis=0)
@@ -277,69 +321,53 @@
         l_ref[...] = jnp.zeros(l_ref.shape, jnp.float32)
         o_ref[...] = jnp.zeros(o_ref.shape, jnp.float32)
 
-    @pl.when(step == z)
-    def _():
-        def body(i, _):
-            visit(pl.multiple_of(i * KEYS, KEYS), KEYS, True)
-            return 0
-
-        lax.fori_loop(0, (y * tokens) // KEYS + 1, body, 0)
-
-    @pl.when(step > z)
-    def _():
-        for start in range(0, keys, KEYS):
-            visit(start, KEYS, False)
-
-    @pl.when(step >= z)
-    def _():
+    def end(step):
         total = l_ref[...]
-        out_ref[0, :DV] = (o_ref[...] / total).astype(jnp.bfloat16)
+        out_ref[step, :DV] = (o_ref[...] / total).astype(jnp.bfloat16)
         weight = m_ref[...] + jnp.log(total)
         high = weight.astype(jnp.bfloat16)
         rest = weight - high.astype(jnp.float32)
         middle = rest.astype(jnp.bfloat16)
         low = (rest - middle.astype(jnp.float32)).astype(jnp.bfloat16)
         pad = jnp.zeros((ROWS - DV - 3, weight.shape[1]), jnp.bfloat16)
-        out_ref[0, DV:] = jnp.concatenate([high, middle, low, pad], axis=0)
-
-    @pl.when(step < z)
-    def _():
-        out_ref[0, :DV] = jnp.zeros((DV, 2 * tokens), jnp.bfloat16)
-        row = lax.broadcasted_iota(jnp.int32, (ROWS - DV, 2 * tokens), 0)
-        out_ref[0, DV:] = jnp.where(row == 0, NEG, 0.0).astype(jnp.bfloat16)
+        out_ref[step, DV:] = jnp.concatenate([high, middle, low, pad], axis=0)
+
+    def masked(i, _):
+        visit(pl.multiple_of(i * KEYS, KEYS), KEYS, True)
+        return 0
+
+    def full(step, _):
+        begin(step)
+        for start in range(0, keys, KEYS):
+            visit(start, KEYS, False)
+        end(step)
+        return 0
+
+    lax.fori_loop(0, z, empty, 0)
+    begin(z)
+    lax.fori_loop(0, (y * tokens) // KEYS + 1, masked, 0)
+    end(z)
+    lax.fori_loop(z + 1, blocks, full, 0)
 
 
 def attend(where, along, mine, other, tokens):
     blocks = along.shape[0]
     count = mine.shape[0] * tokens
-
-    def whole(shape):
-        return pl.BlockSpec(shape, lambda g, w: (0,) * len(shape))
-
     return pl.pallas_call(
         attend_kernel,
-        grid_spec=pltpu.PrefetchScalarGridSpec(
-            num_scalar_prefetch=1,
-            grid=(blocks,),
-            in_specs=[
-                pl.BlockSpec((1, tokens, 2 * DH), lambda g, w: (g, 0, 0)),
-                whole(mine.shape),
-                whole(other.shape),
-            ],
-            out_specs=pl.BlockSpec((1, ROWS, 2 * tokens), lambda g, w: (g, 0, 0)),
-            scratch_shapes=[
-                pltpu.VMEM((count, 2 * DH), jnp.bfloat16),
-                pltpu.VMEM((DV, count), jnp.bfloat16),
-                pltpu.VMEM((2 * DH, 2 * tokens), jnp.bfloat16),
-                pltpu.VMEM((1, 2 * tokens), jnp.float32),
-                pltpu.VMEM((1, 2 * tokens), jnp.float32),
-                pltpu.VMEM((DV, 2 * tokens), jnp.float32),
-            ],
-        ),
+        in_specs=[SMEM, VMEM, VMEM, HBM],
+        scratch_shapes=[
+            pltpu.VMEM(other.shape, other.dtype),
+            pltpu.VMEM((count, 2 * DH), jnp.bfloat16),
+            pltpu.VMEM((DV, count), jnp.bfloat16),
+            pltpu.VMEM((2 * DH, 2 * tokens), jnp.bfloat16),
+            pltpu.VMEM((1, 2 * tokens), jnp.float32),
+            pltpu.VMEM((1, 2 * tokens), jnp.float32),
+            pltpu.VMEM((DV, 2 * tokens), jnp.float32),
+            pltpu.SemaphoreType.DMA,
+        ],
         out_shape=jax.ShapeDtypeStruct((blocks, ROWS, 2 * tokens), jnp.bfloat16),
-        compiler_params=pltpu.CompilerParams(
-            dimension_semantics=("arbitrary",), vmem_limit_bytes=24 * MIB
-        ),
+        compiler_params=pltpu.CompilerParams(vmem_limit_bytes=16 * MIB),
         cost_estimate=pl.CostEstimate(
             flops=blocks * count * tokens * 4 * 256,
             bytes_accessed=blocks * tokens * 1024 + count * 512,
@@ -347,7 +375,7 @@
         ),
         name="attend",
         interpret=INTERPRET,
-    )(where, along, mine, other)
+    )(where, along, mine, pltpu.with_memory_space_constraint(other, pltpu.HBM))
 
 
 def finish_kernel(

time: 198 us -> 196 us (0.990)
  local copies, waits for them, and re-layouts: 6.18 us -> 2.37 us
  Pallas kernels: 27.9 us -> 30.1 us
  blocking collectives: 108 us -> 106 us
    unnamed x26 -> x18, local copies, waits for them, and re-layouts: 4.65 us -> 0.83 us
    pallas_call x3, Pallas kernels: 22 us -> 24.2 us  [the longest x1 20.7 us: attend(): pl.pallas_call(attend_kernel, in_specs=[SMEM, VMEM, VMEM, HBM], scratch_s...]
  transfers between devices with their start and end apart: 8 -> 8, of which waited for: 4 -> 4; matrix products, arithmetic and copies ran while one was open for 1% -> 1% of each run, Pallas kernels for 0% -> 1%
where the time goes in v6:
time: 196 us; the launch traced here: 195 us
  blocking collectives  106 us (54%)
  Pallas kernels  30.1 us (15%)
  starting transfers between devices  30.1 us (15%)
  waiting for transfers between devices  23.3 us (12%)
  local copies, waits for them, and re-layouts  2.37 us (1%)
  other arithmetic  2.03 us (1%)
    all_to_all x1, blocking collectives, layer(): w_own = lax.all_to_all(sent, ('zh', 'y', 'c'), 0, 0, tiled=True)  33.9 us
    all_to_all x1, blocking collectives, layer(): parts = lax.all_to_all(parts, Z, 0, 0, tiled=True)  33 us
    all_to_all x1, blocking collectives, layer(): spread = lax.all_to_all(send, 'y', 0, 0, tiled=True)  21.7 us
    pallas_call x1, Pallas kernels, attend(): pl.pallas_call(attend_kernel, in_specs=[SMEM, VMEM, VMEM, HBM], scratch_s...  20.7 us
    all_to_all x1, waiting for transfers between devices, layer(): along = lax.all_to_all(send, Z, 0, 0, tiled=True)  15.8 us
    all_to_all x1, blocking collectives, layer(): lax.all_to_all(partial.reshape(groups, -1, partial.shape[1]), 'tp', 0, 0,...  13.8 us
    ppermute x4, starting transfers between devices, shifted(): lax.ppermute(value, Z, [(i, (i + step) % count) for i in range(count)])  12.6 us
    all_to_all x1, starting transfers between devices, layer(): along = lax.all_to_all(send, Z, 0, 0, tiled=True)  9.35 us
  transfers between devices with their start and end apart: 8, of which 4 were waited for; matrix products, arithmetic and copies ran while one was open for 1% of the time, Pallas kernels for 1%

profile of v6, /device:TPU:48, one launch (start us, length us, event | category | flops | bytes accessed | tf_op | source)
XLA Modules:
  0.0 194.9 jit_solution(9850818300333664668)
XLA Ops:
  0.0 2.0 %pack.1 = (bf16[16,2,16,512]{3,2,1,0:T(8,128)(2,1)S(1)}, bf16[4,128,512]{2,1,0:T(8,128)(2,1)}) custom-call(bf16[16,256]{1,0:T(8,128)(2,1)} %refs_0_.1, bf16[16,128]{1,0:T(8,128)(2,1)} %refs_1_.1, bf16[16,128]{1,0:T(8,128)(2,1)} %refs_2_.1, bf16[16,128]{1,0:T(8,128)(2,1)} %refs_3_.1, bf16[16,128]{1,0:T(8,128)(2,1)} %refs_4_.1, bf16[16,256]{1,0:T(8,128)(2,1)} %refs_5_.1, ...), custom_call_target="tpu_custom_call" | custom-call | tf_op jit(solution)/shard_map/pack/pallas_call | solution.py:76
  2.1 33.9 %all_to_all.35 = bf16[32,16,512]{2,1,0:T(8,128)(2,1)S(1)} all-to-all(bf16[32,16,512]{2,1,0:T(8,128)(2,1)S(1)} %bitcast.35), channel_id=1, replica_groups=mesh['zh'=2,'zl'=4,'y'=8,'c'=2,'tp'=4] {'zh','y','c'}, dimensions={0} | all-to-all | bytes 1048576 | tf_op jit(solution)/shard_map/all_to_all | solution.py:465
  36.0 0.8 fusion.8
  36.9 3.2 %collective-permute-start.2 = (bf16[512,512]{1,0:T(8,128)(2,1)S(1)}, bf16[512,512]{1,0:T(8,128)(2,1)}, u32[]{:S(2)}, u32[]{:S(2)}) collective-permute-start(bf16[512,512]{1,0:T(8,128)(2,1)S(1)} %bitcast.32), channel_id=1, source_target_pairs={{0,448},{64,0},{128,64},{192,128},{256,192},{320,256},{384,320},{4... | collective-permute-start | bytes 1572872 | tf_op jit(solution)/shard_map/ppermute | solution.py:34
  40.1 2.6 %collective-permute-start.1 = (bf16[512,512]{1,0:T(8,128)(2,1)S(1)}, bf16[512,512]{1,0:T(8,128)(2,1)}, u32[]{:S(2)}, u32[]{:S(2)}) collective-permute-start(bf16[512,512]{1,0:T(8,128)(2,1)S(1)} %bitcast.33), channel_id=1, source_target_pairs={{0,64},{64,128},{128,192},{192,256},{256,320},{320,384},{384,448},... | collective-permute-start | bytes 1572872 | tf_op jit(solution)/shard_map/ppermute | solution.py:34
  42.9 4.3 %all-to-all-start.1 = ((bf16[4,128,512]{2,1,0:T(8,128)(2,1)}), bf16[4,128,512]{2,1,0:T(8,128)(2,1)S(1)}, u32[]{:S(2)}, u32[]{:S(2)}) async-start(bf16[4,128,512]{2,1,0:T(8,128)(2,1)} %get-tuple-element.61), calls=%async_computation.1 | async-start | bytes 1048576 | tf_op jit(solution)/shard_map/all_to_all | solution.py:474
  47.2 3.2 %collective-permute-start.4 = (bf16[256,512]{1,0:T(8,128)(2,1)}, bf16[256,512]{1,0:T(8,128)(2,1)S(1)}, u32[]{:S(2)}, u32[]{:S(2)}) collective-permute-start(bf16[256,512]{1,0:T(8,128)(2,1)} %get-tuple-element.95), channel_id=1, source_target_pairs={{0,384},{64,448},{128,0},{192,64},{256,128},{320,192},{384,256},{4... | collective-permute-start | bytes 786440 | tf_op jit(solution)/shard_map/ppermute | solution.py:34
  50.4 3.5 %collective-permute-start.3 = (bf16[256,512]{1,0:T(8,128)(2,1)}, bf16[256,512]{1,0:T(8,128)(2,1)}, u32[]{:S(2)}, u32[]{:S(2)}) collective-permute-start(bf16[256,512]{1,0:T(8,128)(2,1)} %get-tuple-element.96), channel_id=1, source_target_pairs={{0,128},{64,192},{128,256},{192,320},{256,384},{320,448},{384,0},{... | collective-permute-start | bytes 786440 | tf_op jit(solution)/shard_map/ppermute | solution.py:34
  54.1 2.9 %all-to-all-done.1.far_ref = bf16[4,128,512]{2,1,0:T(8,128)(2,1)S(1)} async-done(((bf16[4,128,512]{2,1,0:T(8,128)(2,1)}), bf16[4,128,512]{2,1,0:T(8,128)(2,1)S(1)}, u32[]{:S(2)}, u32[]{:S(2)}) %all-to-all-start.1) | async-done | bytes 524320 | tf_op jit(solution)/shard_map/all_to_all | solution.py:474
  57.8 1.4 norm.1.own_ref
  59.2 1.9 collective-permute-start
  63.0 2.4 %collective-permute-done.4.w_high_ref = bf16[256,512]{1,0:T(8,128)(2,1)S(1)} collective-permute-done((bf16[256,512]{1,0:T(8,128)(2,1)}, bf16[256,512]{1,0:T(8,128)(2,1)S(1)}, u32[]{:S(2)}, u32[]{:S(2)}) %collective-permute-start.4) | collective-permute-done | bytes 262176 | tf_op jit(solution)/shard_map/ppermute | solution.py:34
  65.4 2.7 %project.1 = (bf16[8,320,128]{2,1,0:T(8,128)(2,1)S(1)}, bf16[256,128]{1,0:T(8,128)(2,1)S(1)}, f32[256,64]{1,0:T(8,128)S(1)}, f32[256,128]{1,0:T(8,128)S(1)}) custom-call(bf16[8,128,256]{2,1,0:T(8,128)(2,1)S(1)} %norm.1.own_ref, bf16[8,128,256]{2,1,0:T(8,128)(2,1)} %collective-permute-done.across_ref, bf16[512,512]{1,0:T(8,128)(2,1)S(1)} %bitcast.34, ...), custom_call_target="tpu_custom_call" | custom-call | tf_op jit(solution)/shard_map/project/pallas_call | solution.py:202
  68.1 21.7 %all_to_all.36.spread_ref.mine_ref = bf16[8,320,128]{2,1,0:T(8,128)(2,1)S(1)} all-to-all(bf16[8,320,128]{2,1,0:T(8,128)(2,1)S(1)} %get-tuple-element.87), channel_id=1, replica_groups=mesh['zh'=2,'zl'=4,'y'=8,'c'=2,'tp'=4] {'y'}, dimensions={0} | all-to-all | bytes 1310720 | tf_op jit(solution)/shard_map/all_to_all | solution.py:505
  89.7 1.5 pass_on.1
  91.2 9.4 %all-to-all-start.3 = ((bf16[8,320,128]{2,1,0:T(8,128)(2,1)}), bf16[8,320,128]{2,1,0:T(8,128)(2,1)S(1)}, u32[]{:S(2)}, u32[]{:S(2)}) async-start(bf16[8,320,128]{2,1,0:T(8,128)(2,1)} %pass_on.1), calls=%async_computation.3 | async-start | bytes 1310720 | tf_op jit(solution)/shard_map/all_to_all | solution.py:507
  100.6 1.9 collective-permute-start.5
  102.5 2.2 %collective-permute-done.5.far_ref = bf16[8,320,128]{2,1,0:T(8,128)(2,1)} collective-permute-done((bf16[8,320,128]{2,1,0:T(8,128)(2,1)S(1)}, bf16[8,320,128]{2,1,0:T(8,128)(2,1)}, u32[]{:S(2)}, u32[]{:S(2)}) %collective-permute-start.5) | collective-permute-done | bytes 655392 | tf_op jit(solution)/shard_map/ppermute | solution.py:29
  104.7 15.8 %all-to-all-done.3.q_ref.along_ref = bf16[8,320,128]{2,1,0:T(8,128)(2,1)S(1)} async-done(((bf16[8,320,128]{2,1,0:T(8,128)(2,1)}), bf16[8,320,128]{2,1,0:T(8,128)(2,1)S(1)}, u32[]{:S(2)}, u32[]{:S(2)}) %all-to-all-start.3) | async-done | bytes 655392 | tf_op jit(solution)/shard_map/all_to_all | solution.py:507
  120.5 20.7 %attend.1 = bf16[8,136,512]{2,1,0:T(8,128)(2,1)S(1)} custom-call(s32[3]{0:T(128)S(1)} %copy-done.4, bf16[8,320,128]{2,1,0:T(8,128)(2,1)S(1)} %all-to-all-done.3.q_ref.along_ref, bf16[8,320,128]{2,1,0:T(8,128)(2,1)S(1)} %all_to_all.36.spread_ref.mine_ref, bf16[8,320,128]{2,1,0:T(8,128)(2,1)} %collective-permute-done.5.far_ref), custom_call_target="tpu_custom_call" | custom-call | flops 4294967296 | bytes 3145728 | tf_op jit(solution)/shard_map/attend/pallas_call | solution.py:356
  141.2 33.0 %all_to_all.37.parts_ref = bf16[8,136,512]{2,1,0:T(8,128)(2,1)S(1)} all-to-all(bf16[8,136,512]{2,1,0:T(8,128)(2,1)S(1)} %attend.1), channel_id=1, replica_groups=mesh['zh'=2,'zl'=4,'y'=8,'c'=2,'tp'=4] {'zh','zl'}, dimensions={0} | all-to-all | bytes 2228224 | tf_op jit(solution)/shard_map/all_to_all | solution.py:510
  174.2 1.8 finish.1
  176.0 3.8 %all_to_all.38 = bf16[2,128,256]{2,1,0:T(8,128)(2,1)S(1)} all-to-all(bf16[2,128,256]{2,1,0:T(8,128)(2,1)S(1)} %finish.1), channel_id=1, replica_groups=mesh['zh'=2,'zl'=4,'y'=8,'c'=2,'tp'=4] {'c'}, dimensions={0} | all-to-all | bytes 262144 | tf_op jit(solution)/shard_map/all_to_all | solution.py:513
  180.3 13.8 %all_to_all.39 = bf16[4,32,2048]{2,1,0:T(8,128)(2,1)S(1)} all-to-all(bf16[4,32,2048]{2,1,0:T(8,128)(2,1)S(1)} %bitcast.37), channel_id=1, replica_groups=mesh['zh'=2,'zl'=4,'y'=8,'c'=2,'tp'=4] {'tp'}, dimensions={0} | all-to-all | bytes 1048576 | tf_op jit(solution)/shard_map/all_to_all | solution.py:520
  (36 shorter events, 4.0 us)
Async XLA Ops:
  0.0 179.9 %copy-start = (bf16[2,256,2048]{2,1,0:T(8,128)(2,1)S(1)}, bf16[2,256,2048]{2,1,0:T(8,128)(2,1)}, u32[]{:S(2)}) copy-start(bf16[2,256,2048]{2,1,0:T(8,128)(2,1)} %param.23) | copy-start | bytes 6291460
  0.0 54.1 %copy-start.6 = (f32[128]{0:T(128)S(1)}, f32[128]{0:T(128)}, u32[]{:S(2)}) copy-start(f32[128]{0:T(128)} %param.22) | copy-start | bytes 1540
  0.0 54.1 %copy-start.7 = (f32[128]{0:T(128)S(1)}, f32[128]{0:T(128)}, u32[]{:S(2)}) copy-start(f32[128]{0:T(128)} %param.18) | copy-start | bytes 1540
  0.0 57.7 %copy-start.3 = (f32[2048]{0:T(1024)S(1)}, f32[2048]{0:T(1024)}, u32[]{:S(2)}) copy-start(f32[2048]{0:T(1024)} %param.13) | copy-start | bytes 24580
  2.1 59.7 %copy-start.8 = (f32[2]{0:T(128)S(1)}, f32[2]{0:T(128)}, u32[]{:S(2)}) copy-start(f32[2]{0:T(128)} %param.17) | copy-start | bytes 28
  36.9 28.5 %collective-permute-start.2 = (bf16[512,512]{1,0:T(8,128)(2,1)S(1)}, bf16[512,512]{1,0:T(8,128)(2,1)}, u32[]{:S(2)}, u32[]{:S(2)}) collective-permute-start(bf16[512,512]{1,0:T(8,128)(2,1)S(1)} %bitcast.32), channel_id=1, source_target_pairs={{0,448},{64,0},{128,64},{192,128},{256,192},{320,256},{384,320},{4... | collective-permute-start | bytes 1572872 | tf_op jit(solution)/shard_map/ppermute | solution.py:34
  40.1 25.3 %collective-permute-start.1 = (bf16[512,512]{1,0:T(8,128)(2,1)S(1)}, bf16[512,512]{1,0:T(8,128)(2,1)}, u32[]{:S(2)}, u32[]{:S(2)}) collective-permute-start(bf16[512,512]{1,0:T(8,128)(2,1)S(1)} %bitcast.33), channel_id=1, source_target_pairs={{0,64},{64,128},{128,192},{192,256},{256,320},{320,384},{384,448},... | collective-permute-start | bytes 1572872 | tf_op jit(solution)/shard_map/ppermute | solution.py:34
  42.9 14.1 %all-to-all-start.1 = ((bf16[4,128,512]{2,1,0:T(8,128)(2,1)}), bf16[4,128,512]{2,1,0:T(8,128)(2,1)S(1)}, u32[]{:S(2)}, u32[]{:S(2)}) async-start(bf16[4,128,512]{2,1,0:T(8,128)(2,1)} %get-tuple-element.61), calls=%async_computation.1 | async-start | bytes 1048576 | tf_op jit(solution)/shard_map/all_to_all | solution.py:474
  47.2 18.1 %collective-permute-start.4 = (bf16[256,512]{1,0:T(8,128)(2,1)}, bf16[256,512]{1,0:T(8,128)(2,1)S(1)}, u32[]{:S(2)}, u32[]{:S(2)}) collective-permute-start(bf16[256,512]{1,0:T(8,128)(2,1)} %get-tuple-element.95), channel_id=1, source_target_pairs={{0,384},{64,448},{128,0},{192,64},{256,128},{320,192},{384,256},{4... | collective-permute-start | bytes 786440 | tf_op jit(solution)/shard_map/ppermute | solution.py:34
  50.4 14.9 %collective-permute-start.3 = (bf16[256,512]{1,0:T(8,128)(2,1)}, bf16[256,512]{1,0:T(8,128)(2,1)}, u32[]{:S(2)}, u32[]{:S(2)}) collective-permute-start(bf16[256,512]{1,0:T(8,128)(2,1)} %get-tuple-element.96), channel_id=1, source_target_pairs={{0,128},{64,192},{128,256},{192,320},{256,384},{320,448},{384,0},{... | collective-permute-start | bytes 786440 | tf_op jit(solution)/shard_map/ppermute | solution.py:34
  57.0 0.8 copy-start.5
  59.2 6.1 %collective-permute-start = (bf16[8,128,256]{2,1,0:T(8,128)(2,1)S(1)}, bf16[8,128,256]{2,1,0:T(8,128)(2,1)}, u32[]{:S(2)}, u32[]{:S(2)}) collective-permute-start(bf16[8,128,256]{2,1,0:T(8,128)(2,1)S(1)} %norm.1.own_ref), channel_id=1, source_target_pairs={{0,4},{4,0},{1,5},{5,1},{2,6},{6,2},{3,7},{7,3},{8,12},{12,8},{9,1... | collective-permute-start | bytes 1572872 | tf_op jit(solution)/shard_map/ppermute | solution.py:29
  68.0 21.7 %copy-start.1 = (f32[256,128]{1,0:T(8,128)}, f32[256,128]{1,0:T(8,128)S(1)}, u32[]{:S(2)}) copy-start(f32[256,128]{1,0:T(8,128)S(1)} %get-tuple-element.94.within_ref) | copy-start | bytes 393220
  68.0 52.5 %copy-start.4 = (s32[3]{0:T(128)S(1)}, s32[3]{0:T(128)}, u32[]{:S(2)}) copy-start(s32[3]{0:T(128)} %pad_add_fusion.where_ref) | copy-start | bytes 40
  91.2 29.3 %all-to-all-start.3 = ((bf16[8,320,128]{2,1,0:T(8,128)(2,1)}), bf16[8,320,128]{2,1,0:T(8,128)(2,1)S(1)}, u32[]{:S(2)}, u32[]{:S(2)}) async-start(bf16[8,320,128]{2,1,0:T(8,128)(2,1)} %pass_on.1), calls=%async_computation.3 | async-start | bytes 1310720 | tf_op jit(solution)/shard_map/all_to_all | solution.py:507
  100.6 4.1 %collective-permute-start.5 = (bf16[8,320,128]{2,1,0:T(8,128)(2,1)S(1)}, bf16[8,320,128]{2,1,0:T(8,128)(2,1)}, u32[]{:S(2)}, u32[]{:S(2)}) collective-permute-start(bf16[8,320,128]{2,1,0:T(8,128)(2,1)S(1)} %all_to_all.36.spread_ref.mine_ref), channel_id=1, source_target_pairs={{0,4},{4,0},{1,5},{5,1},{2,6},{6,2},{3,7},{7,3},{8,12},{12,8},{9,1... | collective-permute-start | bytes 1966088 | tf_op jit(solution)/shard_map/ppermute | solution.py:29
  141.2 33.0 %copy-start.2 = (f32[256,128]{1,0:T(8,128)S(1)}, f32[256,128]{1,0:T(8,128)}, u32[]{:S(2)}) copy-start(f32[256,128]{1,0:T(8,128)} %copy-done.1) | copy-start | bytes 393220

commit v7 on v6

--- a/solution.py
+++ b/solution.py
@@ -34,12 +34,13 @@
     return lax.ppermute(value, Z, [(i, (i + step) % count) for i in range(count)])
 
 
-def around(own, half):
+def around(own):
     before = shifted(own, 1)
     after = shifted(own, -1)
-    low = shifted(own[:half], 2)
-    high = shifted(own[half:], -2)
-    return before, after, low, high
+    count = lax.axis_size(Z)
+    pairs = [(2 * i + k, 2 * ((i + (2, -2)[k]) % count) + k) for i in range(count) for k in range(2)]
+    opposite = lax.ppermute(own, (*Z, "c"), pairs)
+    return before, after, opposite
 
 
 def pack_kernel(*refs):
@@ -141,8 +142,7 @@
     w_own_ref,
     w_before_ref,
     w_after_ref,
-    w_low_ref,
-    w_high_ref,
+    w_opposite_ref,
     place_ref,
     cosine_ref,
     sine_ref,
@@ -156,7 +156,8 @@
     tokens = 2 * half
     low, high = slice(0, wide), slice(wide, 2 * wide)
     weights = [(w_own_ref, low), (w_own_ref, high), (w_before_ref, low), (w_before_ref, high)]
-    weights += [(w_after_ref, low), (w_after_ref, high), (w_low_ref, low), (w_high_ref, low)]
+    weights += [(w_after_ref, low), (w_after_ref, high)]
+    weights += [(w_opposite_ref, low), (w_opposite_ref, high)]
     made = jnp.zeros((tokens, w_own_ref.shape[1]), jnp.float32)
     for k, (ref, at) in enumerate(weights):
         block = place_ref[1 + k]
@@ -201,7 +202,7 @@
     tokens = 2 * own.shape[1]
     return pl.pallas_call(
         project_kernel,
-        in_specs=[VMEM] * 7 + [SMEM, VMEM, VMEM, SMEM],
+        in_specs=[VMEM] * 6 + [SMEM, VMEM, VMEM, SMEM],
         out_shape=[
             jax.ShapeDtypeStruct((count, tokens + DH, DV), jnp.bfloat16),
             jax.ShapeDtypeStruct((tokens, 2 * DH), jnp.bfloat16),
@@ -468,7 +469,7 @@
     w_own, inputs, small = lax.optimization_barrier((w_own, inputs, small))
     features, norm_gain, att_lambda, att_gain, ret_gain = inputs
     even, ys, zs, chip, z, y, c, x = small
-    weights = (w_own, *around(w_own, 2 * ny * rows))
+    weights = (w_own, *around(w_own))
     blocks = [high * nl + (z + k) % nl for k in (0, nl - 1, 1, 2) for high in range(2)]
 
     gathered = lax.all_to_all(features, "tp", 0, 0, tiled=True)
@@ -482,6 +483,18 @@
     cosine, sine = jnp.cos(angles), jnp.sin(angles)
     span = log_decay * tokens
     to_end = jnp.exp(span * (ny - 1 - ys).astype(jnp.float32))
+    place = jnp.stack([c, *blocks]).astype(jnp.int32)
+    tables = (cosine, sine, log_decay, to_end, place)
+    normed, across, weights, tables = lax.optimization_barrier((normed, across, weights, tables))
+    cosine, sine, log_decay, to_end, place = tables
+
+    send, att, query, within = project(
+        normed, across, weights, place, cosine, sine, log_decay, ny
+    )
+    spread = lax.all_to_all(send, "y", 0, 0, tiled=True)
+    small = (ys, zs, span, z, y, c, att_lambda, att_gain, ret_gain)
+    spread, small = lax.optimization_barrier((spread, small))
+    ys, zs, span, z, y, c, att_lambda, att_gain, ret_gain = small
     y_steps = jnp.maximum(y - 1 - ys, 0).astype(jnp.float32)
     z_steps = jnp.maximum(ny * (z - 1 - zs) + y, 0).astype(jnp.float32)
     before = jnp.concatenate(
@@ -491,21 +504,14 @@
         ]
     )
     where = jnp.stack([z, y, c]).astype(jnp.int32)
-    place = jnp.stack([c, *blocks]).astype(jnp.int32)
     mixing = lax.dynamic_index_in_dim(att_lambda, c, 0, keepdims=False)
     gains = jnp.stack([att_gain, ret_gain])
-
-    tables = (cosine, sine, log_decay, to_end, before, where, place, mixing, gains)
-    normed, across, weights, tables = lax.optimization_barrier((normed, across, weights, tables))
-    cosine, sine, log_decay, to_end, before, where, place, mixing, gains = tables
-
-    send, att, query, within = project(
-        normed, across, weights, place, cosine, sine, log_decay, ny
-    )
-    spread = lax.all_to_all(send, "y", 0, 0, tiled=True)
     send = pass_on(spread, att, to_end, nz)
     along = lax.all_to_all(send, Z, 0, 0, tiled=True)
     other = swapped(spread)
+    tables = (before, where, mixing, gains)
+    along, tables = lax.optimization_barrier((along, tables))
+    before, where, mixing, gains = tables
     parts = attend(where, along, spread, other, tokens)
     parts = lax.all_to_all(parts, Z, 0, 0, tiled=True)
 

time: 196 us -> 197 us (level)
  the two profiles are of different devices: /device:TPU:48 before, /device:TPU:1 now
where the time goes in v7:
time: 197 us; the launch traced here: 196 us
  blocking collectives  107 us (54%)
  starting transfers between devices  30.5 us (15%)
  Pallas kernels  27.5 us (14%)
  waiting for transfers between devices  27.4 us (14%)
  other arithmetic  2.17 us (1%)
    all_to_all x1, blocking collectives, layer(): w_own = lax.all_to_all(sent, ('zh', 'y', 'c'), 0, 0, tiled=True)  37.5 us
    all_to_all x1, blocking collectives, layer(): parts = lax.all_to_all(parts, Z, 0, 0, tiled=True)  32.2 us
    all_to_all x1, blocking collectives, layer(): spread = lax.all_to_all(send, 'y', 0, 0, tiled=True)  19.9 us
    pallas_call x1, Pallas kernels, attend(): pl.pallas_call(attend_kernel, in_specs=[SMEM, VMEM, VMEM, HBM], scratch_s...  18.3 us
    all_to_all x1, waiting for transfers between devices, layer(): along = lax.all_to_all(send, Z, 0, 0, tiled=True)  16.7 us
    all_to_all x1, blocking collectives, layer(): lax.all_to_all(partial.reshape(groups, -1, partial.shape[1]), 'tp', 0, 0,...  12.6 us
    all_to_all x1, starting transfers between devices, layer(): along = lax.all_to_all(send, Z, 0, 0, tiled=True)  9.61 us
    ppermute x2, starting transfers between devices, swapped(): return lax.ppermute(value, 'c', [(0, 1), (1, 0)])  9.23 us
  transfers between devices with their start and end apart: 7, of which 3 were waited for; matrix products, arithmetic and copies ran while one was open for 1% of the time, Pallas kernels for 1%

profile of v7, /device:TPU:1, one launch (start us, length us, event | category | flops | bytes accessed | tf_op | source)
XLA Modules:
  0.0 196.4 jit_solution(12688763688684736569)
XLA Ops:
  0.0 2.1 %pack.1 = (bf16[16,2,16,512]{3,2,1,0:T(8,128)(2,1)S(1)}, bf16[4,128,512]{2,1,0:T(8,128)(2,1)}) custom-call(bf16[16,256]{1,0:T(8,128)(2,1)} %refs_0_.1, bf16[16,128]{1,0:T(8,128)(2,1)} %refs_1_.1, bf16[16,128]{1,0:T(8,128)(2,1)} %refs_2_.1, bf16[16,128]{1,0:T(8,128)(2,1)} %refs_3_.1, bf16[16,128]{1,0:T(8,128)(2,1)} %refs_4_.1, bf16[16,256]{1,0:T(8,128)(2,1)} %refs_5_.1, ...), custom_call_target="tpu_custom_call" | custom-call | tf_op jit(solution)/shard_map/pack/pallas_call | solution.py:77
  2.1 37.5 %all_to_all.35 = bf16[32,16,512]{2,1,0:T(8,128)(2,1)S(1)} all-to-all(bf16[32,16,512]{2,1,0:T(8,128)(2,1)S(1)} %bitcast.36), channel_id=1, replica_groups=mesh['zh'=2,'zl'=4,'y'=8,'c'=2,'tp'=4] {'zh','y','c'}, dimensions={0} | all-to-all | bytes 1048576 | tf_op jit(solution)/shard_map/all_to_all | solution.py:466
  39.6 4.1 %all-to-all-start.1 = ((bf16[4,128,512]{2,1,0:T(8,128)(2,1)}), bf16[4,128,512]{2,1,0:T(8,128)(2,1)}, u32[]{:S(2)}, u32[]{:S(2)}) async-start(bf16[4,128,512]{2,1,0:T(8,128)(2,1)} %get-tuple-element.71), calls=%async_computation.1 | async-start | bytes 1048576 | tf_op jit(solution)/shard_map/all_to_all | solution.py:475
  43.8 2.3 %collective-permute-start.3 = (bf16[512,512]{1,0:T(8,128)(2,1)S(1)}, bf16[512,512]{1,0:T(8,128)(2,1)S(1)}, u32[]{:S(2)}, u32[]{:S(2)}) collective-permute-start(bf16[512,512]{1,0:T(8,128)(2,1)S(1)} %bitcast.32), channel_id=1, source_target_pairs={{0,128},{4,388},{64,192},{68,452},{128,256},{132,4},{192,320},{196... | collective-permute-start | bytes 1572872 | tf_op jit(solution)/shard_map/ppermute | solution.py:42
  46.1 2.2 %collective-permute-start.2 = (bf16[512,512]{1,0:T(8,128)(2,1)S(1)}, bf16[512,512]{1,0:T(8,128)(2,1)}, u32[]{:S(2)}, u32[]{:S(2)}) collective-permute-start(bf16[512,512]{1,0:T(8,128)(2,1)S(1)} %bitcast.33), channel_id=1, source_target_pairs={{0,448},{64,0},{128,64},{192,128},{256,192},{320,256},{384,320},{4... | collective-permute-start | bytes 1572872 | tf_op jit(solution)/shard_map/ppermute | solution.py:34
  48.2 3.1 %collective-permute-start.1 = (bf16[512,512]{1,0:T(8,128)(2,1)S(1)}, bf16[512,512]{1,0:T(8,128)(2,1)}, u32[]{:S(2)}, u32[]{:S(2)}) collective-permute-start(bf16[512,512]{1,0:T(8,128)(2,1)S(1)} %bitcast.34), channel_id=1, source_target_pairs={{0,64},{64,128},{128,192},{192,256},{256,320},{320,384},{384,448},... | collective-permute-start | bytes 1572872 | tf_op jit(solution)/shard_map/ppermute | solution.py:34
  51.7 1.4 norm.1.own_ref
  53.1 6.7 %collective-permute-start = (bf16[8,128,256]{2,1,0:T(8,128)(2,1)S(1)}, bf16[8,128,256]{2,1,0:T(8,128)(2,1)S(1)}, u32[]{:S(2)}, u32[]{:S(2)}) collective-permute-start(bf16[8,128,256]{2,1,0:T(8,128)(2,1)S(1)} %norm.1.own_ref), channel_id=1, source_target_pairs={{0,4},{4,0},{1,5},{5,1},{2,6},{6,2},{3,7},{7,3},{8,12},{12,8},{9,1... | collective-permute-start | bytes 1572872 | tf_op jit(solution)/shard_map/ppermute | solution.py:29
  60.4 1.8 collective-permute-done.3.w_opposite_ref
  62.1 8.9 %collective-permute-done.2.w_after_ref = bf16[512,512]{1,0:T(8,128)(2,1)} collective-permute-done((bf16[512,512]{1,0:T(8,128)(2,1)S(1)}, bf16[512,512]{1,0:T(8,128)(2,1)}, u32[]{:S(2)}, u32[]{:S(2)}) %collective-permute-start.2) | collective-permute-done | bytes 524320 | tf_op jit(solution)/shard_map/ppermute | solution.py:34
  71.1 2.4 %project.1 = (bf16[8,320,128]{2,1,0:T(8,128)(2,1)S(1)}, bf16[256,128]{1,0:T(8,128)(2,1)S(1)}, f32[256,64]{1,0:T(8,128)S(1)}, f32[256,128]{1,0:T(8,128)S(1)}) custom-call(bf16[8,128,256]{2,1,0:T(8,128)(2,1)S(1)} %norm.1.own_ref, bf16[8,128,256]{2,1,0:T(8,128)(2,1)S(1)} %collective-permute-done.across_ref, bf16[512,512]{1,0:T(8,128)(2,1)S(1)} %bitcast.35, ...), custom_call_target="tpu_custom_call" | custom-call | tf_op jit(solution)/shard_map/project/pallas_call | solution.py:203
  73.5 19.9 %all_to_all.36.spread_ref.mine_ref = bf16[8,320,128]{2,1,0:T(8,128)(2,1)S(1)} all-to-all(bf16[8,320,128]{2,1,0:T(8,128)(2,1)S(1)} %get-tuple-element.90), channel_id=1, replica_groups=mesh['zh'=2,'zl'=4,'y'=8,'c'=2,'tp'=4] {'y'}, dimensions={0} | all-to-all | bytes 1310720 | tf_op jit(solution)/shard_map/all_to_all | solution.py:494
  93.5 1.5 pass_on.1
  94.9 9.6 %all-to-all-start.3 = ((bf16[8,320,128]{2,1,0:T(8,128)(2,1)}), bf16[8,320,128]{2,1,0:T(8,128)(2,1)S(1)}, u32[]{:S(2)}, u32[]{:S(2)}) async-start(bf16[8,320,128]{2,1,0:T(8,128)(2,1)} %pass_on.1), calls=%async_computation.3 | async-start | bytes 1310720 | tf_op jit(solution)/shard_map/all_to_all | solution.py:510
  104.5 2.6 %collective-permute-start.4 = (bf16[8,320,128]{2,1,0:T(8,128)(2,1)S(1)}, bf16[8,320,128]{2,1,0:T(8,128)(2,1)}, u32[]{:S(2)}, u32[]{:S(2)}) collective-permute-start(bf16[8,320,128]{2,1,0:T(8,128)(2,1)S(1)} %all_to_all.36.spread_ref.mine_ref), channel_id=1, source_target_pairs={{0,4},{4,0},{1,5},{5,1},{2,6},{6,2},{3,7},{7,3},{8,12},{12,8},{9,1... | collective-permute-start | bytes 1966088 | tf_op jit(solution)/shard_map/ppermute | solution.py:29
  107.1 0.6 dynamic_slice.4
  107.9 0.7 pad_maximum_fusion.gain_ref
  108.6 16.7 %all-to-all-done.3.q_ref.along_ref = bf16[8,320,128]{2,1,0:T(8,128)(2,1)S(1)} async-done(((bf16[8,320,128]{2,1,0:T(8,128)(2,1)}), bf16[8,320,128]{2,1,0:T(8,128)(2,1)S(1)}, u32[]{:S(2)}, u32[]{:S(2)}) %all-to-all-start.3) | async-done | bytes 655392 | tf_op jit(solution)/shard_map/all_to_all | solution.py:510
  125.3 18.3 %attend.1 = bf16[8,136,512]{2,1,0:T(8,128)(2,1)S(1)} custom-call(s32[3]{0:T(128)S(1)} %pad_add_fusion.where_ref, bf16[8,320,128]{2,1,0:T(8,128)(2,1)S(1)} %all-to-all-done.3.q_ref.along_ref, bf16[8,320,128]{2,1,0:T(8,128)(2,1)S(1)} %all_to_all.36.spread_ref.mine_ref, bf16[8,320,128]{2,1,0:T(8,128)(2,1)} %collective-permute-done.4.far_ref), custom_call_target="tpu_custom_call" | custom-call | flops 4294967296 | bytes 3145728 | tf_op jit(solution)/shard_map/attend/pallas_call | solution.py:357
  143.6 32.2 %all_to_all.37.parts_ref = bf16[8,136,512]{2,1,0:T(8,128)(2,1)S(1)} all-to-all(bf16[8,136,512]{2,1,0:T(8,128)(2,1)S(1)} %attend.1), channel_id=1, replica_groups=mesh['zh'=2,'zl'=4,'y'=8,'c'=2,'tp'=4] {'zh','zl'}, dimensions={0} | all-to-all | bytes 2228224 | tf_op jit(solution)/shard_map/all_to_all | solution.py:516
  175.8 1.8 finish.1
  177.6 4.9 %all_to_all.38 = bf16[2,128,256]{2,1,0:T(8,128)(2,1)S(1)} all-to-all(bf16[2,128,256]{2,1,0:T(8,128)(2,1)S(1)} %finish.1), channel_id=1, replica_groups=mesh['zh'=2,'zl'=4,'y'=8,'c'=2,'tp'=4] {'c'}, dimensions={0} | all-to-all | bytes 262144 | tf_op jit(solution)/shard_map/all_to_all | solution.py:519
  183.0 12.6 %all_to_all.39 = bf16[4,32,2048]{2,1,0:T(8,128)(2,1)S(1)} all-to-all(bf16[4,32,2048]{2,1,0:T(8,128)(2,1)S(1)} %bitcast.38), channel_id=1, replica_groups=mesh['zh'=2,'zl'=4,'y'=8,'c'=2,'tp'=4] {'tp'}, dimensions={0} | all-to-all | bytes 1048576 | tf_op jit(solution)/shard_map/all_to_all | solution.py:526
  195.6 0.8 convert_reduce_fusion
  (28 shorter events, 1.3 us)
Async XLA Ops:
  0.0 182.6 %copy-start = (bf16[2,256,2048]{2,1,0:T(8,128)(2,1)S(1)}, bf16[2,256,2048]{2,1,0:T(8,128)(2,1)}, u32[]{:S(2)}) copy-start(bf16[2,256,2048]{2,1,0:T(8,128)(2,1)} %param.23) | copy-start | bytes 6291460
  0.0 51.7 %copy-start.3 = (f32[2048]{0:T(1024)S(1)}, f32[2048]{0:T(1024)}, u32[]{:S(2)}) copy-start(f32[2048]{0:T(1024)} %param.13) | copy-start | bytes 24580
  39.6 12.1 %all-to-all-start.1 = ((bf16[4,128,512]{2,1,0:T(8,128)(2,1)}), bf16[4,128,512]{2,1,0:T(8,128)(2,1)}, u32[]{:S(2)}, u32[]{:S(2)}) async-start(bf16[4,128,512]{2,1,0:T(8,128)(2,1)} %get-tuple-element.71), calls=%async_computation.1 | async-start | bytes 1048576 | tf_op jit(solution)/shard_map/all_to_all | solution.py:475
  43.8 18.3 %collective-permute-start.3 = (bf16[512,512]{1,0:T(8,128)(2,1)S(1)}, bf16[512,512]{1,0:T(8,128)(2,1)S(1)}, u32[]{:S(2)}, u32[]{:S(2)}) collective-permute-start(bf16[512,512]{1,0:T(8,128)(2,1)S(1)} %bitcast.32), channel_id=1, source_target_pairs={{0,128},{4,388},{64,192},{68,452},{128,256},{132,4},{192,320},{196... | collective-permute-start | bytes 1572872 | tf_op jit(solution)/shard_map/ppermute | solution.py:42
  46.1 25.0 %collective-permute-start.2 = (bf16[512,512]{1,0:T(8,128)(2,1)S(1)}, bf16[512,512]{1,0:T(8,128)(2,1)}, u32[]{:S(2)}, u32[]{:S(2)}) collective-permute-start(bf16[512,512]{1,0:T(8,128)(2,1)S(1)} %bitcast.33), channel_id=1, source_target_pairs={{0,448},{64,0},{128,64},{192,128},{256,192},{320,256},{384,320},{4... | collective-permute-start | bytes 1572872 | tf_op jit(solution)/shard_map/ppermute | solution.py:34
  48.2 22.8 %collective-permute-start.1 = (bf16[512,512]{1,0:T(8,128)(2,1)S(1)}, bf16[512,512]{1,0:T(8,128)(2,1)}, u32[]{:S(2)}, u32[]{:S(2)}) collective-permute-start(bf16[512,512]{1,0:T(8,128)(2,1)S(1)} %bitcast.34), channel_id=1, source_target_pairs={{0,64},{64,128},{128,192},{192,256},{256,320},{320,384},{384,448},... | collective-permute-start | bytes 1572872 | tf_op jit(solution)/shard_map/ppermute | solution.py:34
  53.1 17.9 %collective-permute-start = (bf16[8,128,256]{2,1,0:T(8,128)(2,1)S(1)}, bf16[8,128,256]{2,1,0:T(8,128)(2,1)S(1)}, u32[]{:S(2)}, u32[]{:S(2)}) collective-permute-start(bf16[8,128,256]{2,1,0:T(8,128)(2,1)S(1)} %norm.1.own_ref), channel_id=1, source_target_pairs={{0,4},{4,0},{1,5},{5,1},{2,6},{6,2},{3,7},{7,3},{8,12},{12,8},{9,1... | collective-permute-start | bytes 1572872 | tf_op jit(solution)/shard_map/ppermute | solution.py:29
  73.5 21.4 %copy-start.1 = (f32[256,128]{1,0:T(8,128)}, f32[256,128]{1,0:T(8,128)S(1)}, u32[]{:S(2)}) copy-start(f32[256,128]{1,0:T(8,128)S(1)} %get-tuple-element.114.within_ref) | copy-start | bytes 393220
  73.5 33.6 %copy-start.5 = (f32[2]{0:T(128)S(1)}, f32[2]{0:T(128)}, u32[]{:S(2)}) copy-start(f32[2]{0:T(128)} %param.17) | copy-start | bytes 28
  73.5 34.4 %copy-start.4 = (f32[128]{0:T(128)S(1)}, f32[128]{0:T(128)}, u32[]{:S(2)}) copy-start(f32[128]{0:T(128)} %param.22) | copy-start | bytes 1540
  94.9 30.4 %all-to-all-start.3 = ((bf16[8,320,128]{2,1,0:T(8,128)(2,1)}), bf16[8,320,128]{2,1,0:T(8,128)(2,1)S(1)}, u32[]{:S(2)}, u32[]{:S(2)}) async-start(bf16[8,320,128]{2,1,0:T(8,128)(2,1)} %pass_on.1), calls=%async_computation.3 | async-start | bytes 1310720 | tf_op jit(solution)/shard_map/all_to_all | solution.py:510
  104.5 20.8 %collective-permute-start.4 = (bf16[8,320,128]{2,1,0:T(8,128)(2,1)S(1)}, bf16[8,320,128]{2,1,0:T(8,128)(2,1)}, u32[]{:S(2)}, u32[]{:S(2)}) collective-permute-start(bf16[8,320,128]{2,1,0:T(8,128)(2,1)S(1)} %all_to_all.36.spread_ref.mine_ref), channel_id=1, source_target_pairs={{0,4},{4,0},{1,5},{5,1},{2,6},{6,2},{3,7},{7,3},{8,12},{12,8},{9,1... | collective-permute-start | bytes 1966088 | tf_op jit(solution)/shard_map/ppermute | solution.py:29
  143.6 32.2 %copy-start.2 = (f32[256,128]{1,0:T(8,128)S(1)}, f32[256,128]{1,0:T(8,128)}, u32[]{:S(2)}) copy-start(f32[256,128]{1,0:T(8,128)} %copy-done.1) | copy-start | bytes 393220

commit v8 on v7

--- a/solution.py
+++ b/solution.py
@@ -59,7 +59,13 @@
         copy.start()
     for copy in copies:
         copy.wait()
-    query, key, value, rq, rk, rv, features = (buffer[...] for buffer in scratch)
+    wide = [
+        pltpu.make_async_copy(scratch[-1], wide_ref.at[i], sems.at[count - 1 + i])
+        for i in range(wide_ref.shape[0])
+    ]
+    for copy in wide:
+        copy.start()
+    query, key, value, rq, rk, rv = (buffer[...] for buffer in scratch[:-1])
     for h, whole in enumerate((key, value)):
         parts = [query, whole, rq, rk, rv]
         for k in (0, 2, 3, 4):
@@ -68,8 +74,8 @@
         row = jnp.concatenate(parts, axis=1)
         for i in range(out_ref.shape[0]):
             out_ref[i, h] = row
-    for i in range(wide_ref.shape[0]):
-        wide_ref[i] = features
+    for copy in wide:
+        copy.wait()
 
 
 def pack(count, groups, *arrays):
@@ -77,12 +83,13 @@
     return pl.pallas_call(
         pack_kernel,
         in_specs=[HBM] * len(arrays),
+        out_specs=[VMEM, HBM],
         out_shape=[
             jax.ShapeDtypeStruct((count, 2, rows, 512), jnp.bfloat16),
             jax.ShapeDtypeStruct((groups, *arrays[-1].shape), jnp.bfloat16),
         ],
         scratch_shapes=[pltpu.VMEM(a.shape, a.dtype) for a in arrays]
-        + [pltpu.SemaphoreType.DMA((len(arrays),))],
+        + [pltpu.SemaphoreType.DMA((len(arrays) + groups,))],
         compiler_params=pltpu.CompilerParams(vmem_limit_bytes=4 * MIB),
         name="pack",
         interpret=INTERPRET,
@@ -149,8 +156,8 @@
     decay_ref,
     send_ref,
     att_ref,
-    query_ref,
-    within_ref,
+    turned_ref,
+    value_ref,
 ):
     half, wide = own_ref.shape[1:]
     tokens = 2 * half
@@ -179,7 +186,6 @@
     cosine = jnp.concatenate([cosine_ref[...]] * 4, axis=1)
     sine = jnp.concatenate([sine_ref[...]] * 4, axis=1)
     turned = pair * cosine + crossed * sine
-    query = turned[:, :DH]
     key = turned[:, DH:] * DH ** (-0.5)
     value = made[:, 384:512]
     log_decay = decay_ref[0]
@@ -189,6 +195,17 @@
     for k in range(send_ref.shape[0]):
         send_ref[k, :tokens] = made[:, 128:256]
         send_ref[k, tokens:] = state
+    turned_ref[...] = turned
+    value_ref[...] = value
+
+
+def local_kernel(turned_ref, value_ref, decay_ref, query_ref, within_ref):
+    tokens = turned_ref.shape[0]
+    query = turned_ref[:, :DH]
+    key = turned_ref[:, DH:] * DH ** (-0.5)
+    value = value_ref[...]
+    log_decay = decay_ref[0]
+    offset = lax.broadcasted_iota(jnp.int32, (tokens, 1), 0).astype(jnp.float32)
     i = lax.broadcasted_iota(jnp.int32, (tokens, tokens), 0)
     j = lax.broadcasted_iota(jnp.int32, (tokens, tokens), 1)
     distance = (i - j).astype(jnp.float32)
@@ -198,6 +215,21 @@
     query_ref[...] = query * jnp.exp(log_decay * (offset + 1.0))
 
 
+def local(turned, value, log_decay):
+    tokens = turned.shape[0]
+    return pl.pallas_call(
+        local_kernel,
+        in_specs=[VMEM, VMEM, SMEM],
+        out_shape=[
+            jax.ShapeDtypeStruct((tokens, DH), jnp.float32),
+            jax.ShapeDtypeStruct((tokens, DV), jnp.float32),
+        ],
+        compiler_params=pltpu.CompilerParams(vmem_limit_bytes=6 * MIB),
+        name="local",
+        interpret=INTERPRET,
+    )(turned, value, log_decay.reshape(1))
+
+
 def project(own, across, weights, place, cosine, sine, log_decay, count):
     tokens = 2 * own.shape[1]
     return pl.pallas_call(
@@ -206,8 +238,8 @@
         out_shape=[
             jax.ShapeDtypeStruct((count, tokens + DH, DV), jnp.bfloat16),
             jax.ShapeDtypeStruct((tokens, 2 * DH), jnp.bfloat16),
-            jax.ShapeDtypeStruct((tokens, DH), jnp.float32),
-            jax.ShapeDtypeStruct((tokens, DV), jnp.float32),
+            jax.ShapeDtypeStruct((tokens, 2 * DH), jnp.float32),
+            jax.ShapeDtypeStruct((tokens, DV), jnp.bfloat16),
         ],
         compiler_params=pltpu.CompilerParams(vmem_limit_bytes=12 * MIB),
         name="project",
@@ -488,13 +520,14 @@
     normed, across, weights, tables = lax.optimization_barrier((normed, across, weights, tables))
     cosine, sine, log_decay, to_end, place = tables
 
-    send, att, query, within = project(
+    send, att, turned, value = project(
         normed, across, weights, place, cosine, sine, log_decay, ny
     )
     spread = lax.all_to_all(send, "y", 0, 0, tiled=True)
-    small = (ys, zs, span, z, y, c, att_lambda, att_gain, ret_gain)
+    small = (ys, zs, span, z, y, c, att_lambda, att_gain, ret_gain, turned, value, log_decay)
     spread, small = lax.optimization_barrier((spread, small))
-    ys, zs, span, z, y, c, att_lambda, att_gain, ret_gain = small
+    ys, zs, span, z, y, c, att_lambda, att_gain, ret_gain, turned, value, log_decay = small
+    query, within = local(turned, value, log_decay)
     y_steps = jnp.maximum(y - 1 - ys, 0).astype(jnp.float32)
     z_steps = jnp.maximum(ny * (z - 1 - zs) + y, 0).astype(jnp.float32)
     before = jnp.concatenate(
@@ -509,9 +542,9 @@
     send = pass_on(spread, att, to_end, nz)
     along = lax.all_to_all(send, Z, 0, 0, tiled=True)
     other = swapped(spread)
-    tables = (before, where, mixing, gains)
+    tables = (before, where, mixing, gains, query, within)
     along, tables = lax.optimization_barrier((along, tables))
-    before, where, mixing, gains = tables
+    before, where, mixing, gains, query, within = tables
     parts = attend(where, along, spread, other, tokens)
     parts = lax.all_to_all(parts, Z, 0, 0, tiled=True)
 

time: 197 us -> 197 us (level)
  waiting for transfers between devices: 27.4 us -> 24.6 us
  local copies, waits for them, and re-layouts: 0.76 us -> 3.1 us
    all_to_all x1, waiting for transfers between devices: 16.7 us -> 14 us  [layer(): along = lax.all_to_all(send, Z, 0, 0, tiled=True)]
    unnamed x12 -> x20, local copies, waits for them, and re-layouts: 0.03 us -> 2.43 us
where the time goes in v8:
time: 197 us; the launch traced here: 196 us
  blocking collectives  107 us (54%)
  starting transfers between devices  30.5 us (15%)
  Pallas kernels  27.7 us (14%)
  waiting for transfers between devices  24.6 us (12%)
  local copies, waits for them, and re-layouts  3.1 us (2%)
  other arithmetic  2.17 us (1%)
    all_to_all x1, blocking collectives, layer(): w_own = lax.all_to_all(sent, ('zh', 'y', 'c'), 0, 0, tiled=True)  37.5 us
    all_to_all x1, blocking collectives, layer(): parts = lax.all_to_all(parts, Z, 0, 0, tiled=True)  32.2 us
    all_to_all x1, blocking collectives, layer(): spread = lax.all_to_all(send, 'y', 0, 0, tiled=True)  19.9 us
    pallas_call x1, Pallas kernels, attend(): pl.pallas_call(attend_kernel, in_specs=[SMEM, VMEM, VMEM, HBM], scratch_s...  18.3 us
    all_to_all x1, waiting for transfers between devices, layer(): along = lax.all_to_all(send, Z, 0, 0, tiled=True)  14 us
    all_to_all x1, blocking collectives, layer(): lax.all_to_all(partial.reshape(groups, -1, partial.shape[1]), 'tp', 0, 0,...  12.6 us
    all_to_all x1, starting transfers between devices, layer(): along = lax.all_to_all(send, Z, 0, 0, tiled=True)  9.61 us
    ppermute x2, starting transfers between devices, swapped(): return lax.ppermute(value, 'c', [(0, 1), (1, 0)])  9.24 us
  transfers between devices with their start and end apart: 7, of which 3 were waited for; matrix products, arithmetic and copies ran while one was open for 1% of the time, Pallas kernels for 1%

profile of v8, /device:TPU:1, one launch (start us, length us, event | category | flops | bytes accessed | tf_op | source)
XLA Modules:
  0.0 196.2 jit_solution(16427037215173978008)
XLA Ops:
  0.0 2.0 %pack.1 = (bf16[16,2,16,512]{3,2,1,0:T(8,128)(2,1)S(1)}, bf16[4,128,512]{2,1,0:T(8,128)(2,1)}) custom-call(bf16[16,256]{1,0:T(8,128)(2,1)} %refs_0_.1, bf16[16,128]{1,0:T(8,128)(2,1)} %refs_1_.1, bf16[16,128]{1,0:T(8,128)(2,1)} %refs_2_.1, bf16[16,128]{1,0:T(8,128)(2,1)} %refs_3_.1, bf16[16,128]{1,0:T(8,128)(2,1)} %refs_4_.1, bf16[16,256]{1,0:T(8,128)(2,1)} %refs_5_.1, ...), custom_call_target="tpu_custom_call" | custom-call | tf_op jit(solution)/shard_map/pack/pallas_call | solution.py:83
  2.1 37.5 %all_to_all.35 = bf16[32,16,512]{2,1,0:T(8,128)(2,1)S(1)} all-to-all(bf16[32,16,512]{2,1,0:T(8,128)(2,1)S(1)} %bitcast.37), channel_id=1, replica_groups=mesh['zh'=2,'zl'=4,'y'=8,'c'=2,'tp'=4] {'zh','y','c'}, dimensions={0} | all-to-all | bytes 1048576 | tf_op jit(solution)/shard_map/all_to_all | solution.py:498
  39.6 4.1 %all-to-all-start.1 = ((bf16[4,128,512]{2,1,0:T(8,128)(2,1)}), bf16[4,128,512]{2,1,0:T(8,128)(2,1)}, u32[]{:S(2)}, u32[]{:S(2)}) async-start(bf16[4,128,512]{2,1,0:T(8,128)(2,1)} %get-tuple-element.78), calls=%async_computation.1 | async-start | bytes 1048576 | tf_op jit(solution)/shard_map/all_to_all | solution.py:507
  43.8 2.3 %collective-permute-start.3 = (bf16[512,512]{1,0:T(8,128)(2,1)S(1)}, bf16[512,512]{1,0:T(8,128)(2,1)S(1)}, u32[]{:S(2)}, u32[]{:S(2)}) collective-permute-start(bf16[512,512]{1,0:T(8,128)(2,1)S(1)} %bitcast.33), channel_id=1, source_target_pairs={{0,128},{4,388},{64,192},{68,452},{128,256},{132,4},{192,320},{196... | collective-permute-start | bytes 1572872 | tf_op jit(solution)/shard_map/ppermute | solution.py:42
  46.0 2.2 %collective-permute-start.2 = (bf16[512,512]{1,0:T(8,128)(2,1)S(1)}, bf16[512,512]{1,0:T(8,128)(2,1)}, u32[]{:S(2)}, u32[]{:S(2)}) collective-permute-start(bf16[512,512]{1,0:T(8,128)(2,1)S(1)} %bitcast.34), channel_id=1, source_target_pairs={{0,448},{64,0},{128,64},{192,128},{256,192},{320,256},{384,320},{4... | collective-permute-start | bytes 1572872 | tf_op jit(solution)/shard_map/ppermute | solution.py:34
  48.2 3.1 %collective-permute-start.1 = (bf16[512,512]{1,0:T(8,128)(2,1)S(1)}, bf16[512,512]{1,0:T(8,128)(2,1)}, u32[]{:S(2)}, u32[]{:S(2)}) collective-permute-start(bf16[512,512]{1,0:T(8,128)(2,1)S(1)} %bitcast.35), channel_id=1, source_target_pairs={{0,64},{64,128},{128,192},{192,256},{256,320},{320,384},{384,448},... | collective-permute-start | bytes 1572872 | tf_op jit(solution)/shard_map/ppermute | solution.py:34
  51.7 1.4 norm.1.own_ref
  53.1 6.7 %collective-permute-start = (bf16[8,128,256]{2,1,0:T(8,128)(2,1)S(1)}, bf16[8,128,256]{2,1,0:T(8,128)(2,1)S(1)}, u32[]{:S(2)}, u32[]{:S(2)}) collective-permute-start(bf16[8,128,256]{2,1,0:T(8,128)(2,1)S(1)} %norm.1.own_ref), channel_id=1, source_target_pairs={{0,4},{4,0},{1,5},{5,1},{2,6},{6,2},{3,7},{7,3},{8,12},{12,8},{9,1... | collective-permute-start | bytes 1572872 | tf_op jit(solution)/shard_map/ppermute | solution.py:29
  60.4 1.7 collective-permute-done.3.w_opposite_ref
  62.1 8.9 %collective-permute-done.2.w_after_ref = bf16[512,512]{1,0:T(8,128)(2,1)} collective-permute-done((bf16[512,512]{1,0:T(8,128)(2,1)S(1)}, bf16[512,512]{1,0:T(8,128)(2,1)}, u32[]{:S(2)}, u32[]{:S(2)}) %collective-permute-start.2) | collective-permute-done | bytes 524320 | tf_op jit(solution)/shard_map/ppermute | solution.py:34
  71.0 2.3 %project.1 = (bf16[8,320,128]{2,1,0:T(8,128)(2,1)S(1)}, bf16[256,128]{1,0:T(8,128)(2,1)S(1)}, f32[256,128]{1,0:T(8,128)S(1)}, bf16[256,128]{1,0:T(8,128)(2,1)S(1)}) custom-call(bf16[8,128,256]{2,1,0:T(8,128)(2,1)S(1)} %norm.1.own_ref, bf16[8,128,256]{2,1,0:T(8,128)(2,1)S(1)} %collective-permute-done.across_ref, bf16[512,512]{1,0:T(8,128)(2,1)S(1)} %bitcast.36, ...), custom_call_target="tpu_custom_call" | custom-call | tf_op jit(solution)/shard_map/project/pallas_call | solution.py:235
  73.4 19.9 %all_to_all.36.spread_ref.mine_ref = bf16[8,320,128]{2,1,0:T(8,128)(2,1)S(1)} all-to-all(bf16[8,320,128]{2,1,0:T(8,128)(2,1)S(1)} %get-tuple-element.97), channel_id=1, replica_groups=mesh['zh'=2,'zl'=4,'y'=8,'c'=2,'tp'=4] {'y'}, dimensions={0} | all-to-all | bytes 1310720 | tf_op jit(solution)/shard_map/all_to_all | solution.py:526
  93.3 1.5 pass_on.1
  94.8 9.6 %all-to-all-start.3 = ((bf16[8,320,128]{2,1,0:T(8,128)(2,1)}), bf16[8,320,128]{2,1,0:T(8,128)(2,1)S(1)}, u32[]{:S(2)}, u32[]{:S(2)}) async-start(bf16[8,320,128]{2,1,0:T(8,128)(2,1)} %pass_on.1), calls=%async_computation.3 | async-start | bytes 1310720 | tf_op jit(solution)/shard_map/all_to_all | solution.py:543
  104.4 2.6 %collective-permute-start.4 = (bf16[8,320,128]{2,1,0:T(8,128)(2,1)S(1)}, bf16[8,320,128]{2,1,0:T(8,128)(2,1)}, u32[]{:S(2)}, u32[]{:S(2)}) collective-permute-start(bf16[8,320,128]{2,1,0:T(8,128)(2,1)S(1)} %all_to_all.36.spread_ref.mine_ref), channel_id=1, source_target_pairs={{0,4},{4,0},{1,5},{5,1},{2,6},{6,2},{3,7},{7,3},{8,12},{12,8},{9,1... | collective-permute-start | bytes 1966088 | tf_op jit(solution)/shard_map/ppermute | solution.py:29
  107.6 0.9 copy-done.4
  108.5 0.8 copy-done.6
  111.2 14.0 %all-to-all-done.3.q_ref.along_ref = bf16[8,320,128]{2,1,0:T(8,128)(2,1)S(1)} async-done(((bf16[8,320,128]{2,1,0:T(8,128)(2,1)}), bf16[8,320,128]{2,1,0:T(8,128)(2,1)S(1)}, u32[]{:S(2)}, u32[]{:S(2)}) %all-to-all-start.3) | async-done | bytes 655392 | tf_op jit(solution)/shard_map/all_to_all | solution.py:543
  125.2 18.3 %attend.1 = bf16[8,136,512]{2,1,0:T(8,128)(2,1)S(1)} custom-call(s32[3]{0:T(128)S(1)} %pad_add_fusion.where_ref, bf16[8,320,128]{2,1,0:T(8,128)(2,1)S(1)} %all-to-all-done.3.q_ref.along_ref, bf16[8,320,128]{2,1,0:T(8,128)(2,1)S(1)} %all_to_all.36.spread_ref.mine_ref, bf16[8,320,128]{2,1,0:T(8,128)(2,1)} %collective-permute-done.4.far_ref), custom_call_target="tpu_custom_call" | custom-call | flops 4294967296 | bytes 3145728 | tf_op jit(solution)/shard_map/attend/pallas_call | solution.py:389
  143.5 32.2 %all_to_all.37.parts_ref = bf16[8,136,512]{2,1,0:T(8,128)(2,1)S(1)} all-to-all(bf16[8,136,512]{2,1,0:T(8,128)(2,1)S(1)} %attend.1), channel_id=1, replica_groups=mesh['zh'=2,'zl'=4,'y'=8,'c'=2,'tp'=4] {'zh','zl'}, dimensions={0} | all-to-all | bytes 2228224 | tf_op jit(solution)/shard_map/all_to_all | solution.py:549
  175.7 1.7 finish.1
  177.4 4.9 %all_to_all.38 = bf16[2,128,256]{2,1,0:T(8,128)(2,1)S(1)} all-to-all(bf16[2,128,256]{2,1,0:T(8,128)(2,1)S(1)} %finish.1), channel_id=1, replica_groups=mesh['zh'=2,'zl'=4,'y'=8,'c'=2,'tp'=4] {'c'}, dimensions={0} | all-to-all | bytes 262144 | tf_op jit(solution)/shard_map/all_to_all | solution.py:552
  182.8 12.6 %all_to_all.39 = bf16[4,32,2048]{2,1,0:T(8,128)(2,1)S(1)} all-to-all(bf16[4,32,2048]{2,1,0:T(8,128)(2,1)S(1)} %bitcast.39), channel_id=1, replica_groups=mesh['zh'=2,'zl'=4,'y'=8,'c'=2,'tp'=4] {'tp'}, dimensions={0} | all-to-all | bytes 1048576 | tf_op jit(solution)/shard_map/all_to_all | solution.py:559
  195.4 0.8 convert_reduce_fusion
  (37 shorter events, 3.6 us)
Async XLA Ops:
  0.0 182.4 %copy-start = (bf16[2,256,2048]{2,1,0:T(8,128)(2,1)S(1)}, bf16[2,256,2048]{2,1,0:T(8,128)(2,1)}, u32[]{:S(2)}) copy-start(bf16[2,256,2048]{2,1,0:T(8,128)(2,1)} %param.23) | copy-start | bytes 6291460
  0.0 51.7 %copy-start.7 = (f32[2048]{0:T(1024)S(1)}, f32[2048]{0:T(1024)}, u32[]{:S(2)}) copy-start(f32[2048]{0:T(1024)} %param.13) | copy-start | bytes 24580
  39.6 12.1 %all-to-all-start.1 = ((bf16[4,128,512]{2,1,0:T(8,128)(2,1)}), bf16[4,128,512]{2,1,0:T(8,128)(2,1)}, u32[]{:S(2)}, u32[]{:S(2)}) async-start(bf16[4,128,512]{2,1,0:T(8,128)(2,1)} %get-tuple-element.78), calls=%async_computation.1 | async-start | bytes 1048576 | tf_op jit(solution)/shard_map/all_to_all | solution.py:507
  43.8 18.3 %collective-permute-start.3 = (bf16[512,512]{1,0:T(8,128)(2,1)S(1)}, bf16[512,512]{1,0:T(8,128)(2,1)S(1)}, u32[]{:S(2)}, u32[]{:S(2)}) collective-permute-start(bf16[512,512]{1,0:T(8,128)(2,1)S(1)} %bitcast.33), channel_id=1, source_target_pairs={{0,128},{4,388},{64,192},{68,452},{128,256},{132,4},{192,320},{196... | collective-permute-start | bytes 1572872 | tf_op jit(solution)/shard_map/ppermute | solution.py:42
  46.0 25.0 %collective-permute-start.2 = (bf16[512,512]{1,0:T(8,128)(2,1)S(1)}, bf16[512,512]{1,0:T(8,128)(2,1)}, u32[]{:S(2)}, u32[]{:S(2)}) collective-permute-start(bf16[512,512]{1,0:T(8,128)(2,1)S(1)} %bitcast.34), channel_id=1, source_target_pairs={{0,448},{64,0},{128,64},{192,128},{256,192},{320,256},{384,320},{4... | collective-permute-start | bytes 1572872 | tf_op jit(solution)/shard_map/ppermute | solution.py:34
  48.2 22.8 %collective-permute-start.1 = (bf16[512,512]{1,0:T(8,128)(2,1)S(1)}, bf16[512,512]{1,0:T(8,128)(2,1)}, u32[]{:S(2)}, u32[]{:S(2)}) collective-permute-start(bf16[512,512]{1,0:T(8,128)(2,1)S(1)} %bitcast.35), channel_id=1, source_target_pairs={{0,64},{64,128},{128,192},{192,256},{256,320},{320,384},{384,448},... | collective-permute-start | bytes 1572872 | tf_op jit(solution)/shard_map/ppermute | solution.py:34
  53.1 17.9 %collective-permute-start = (bf16[8,128,256]{2,1,0:T(8,128)(2,1)S(1)}, bf16[8,128,256]{2,1,0:T(8,128)(2,1)S(1)}, u32[]{:S(2)}, u32[]{:S(2)}) collective-permute-start(bf16[8,128,256]{2,1,0:T(8,128)(2,1)S(1)} %norm.1.own_ref), channel_id=1, source_target_pairs={{0,4},{4,0},{1,5},{5,1},{2,6},{6,2},{3,7},{7,3},{8,12},{12,8},{9,1... | collective-permute-start | bytes 1572872 | tf_op jit(solution)/shard_map/ppermute | solution.py:29
  73.3 20.0 %copy-start.3 = (f32[256,128]{1,0:T(8,128)}, f32[256,128]{1,0:T(8,128)S(1)}, u32[]{:S(2)}) copy-start(f32[256,128]{1,0:T(8,128)S(1)} %get-tuple-element.117.turned_ref) | copy-start | bytes 393220
  73.4 20.0 %copy-start.5 = (bf16[256,128]{1,0:T(8,128)(2,1)}, bf16[256,128]{1,0:T(8,128)(2,1)S(1)}, u32[]{:S(2)}) copy-start(bf16[256,128]{1,0:T(8,128)(2,1)S(1)} %get-tuple-element.118.value_ref) | copy-start | bytes 196612
  73.4 33.7 %copy-start.9 = (f32[2]{0:T(128)S(1)}, f32[2]{0:T(128)}, u32[]{:S(2)}) copy-start(f32[2]{0:T(128)} %param.17) | copy-start | bytes 28
  73.4 37.2 %copy-start.8 = (f32[128]{0:T(128)S(1)}, f32[128]{0:T(128)}, u32[]{:S(2)}) copy-start(f32[128]{0:T(128)} %param.22) | copy-start | bytes 1540
  94.8 30.4 %all-to-all-start.3 = ((bf16[8,320,128]{2,1,0:T(8,128)(2,1)}), bf16[8,320,128]{2,1,0:T(8,128)(2,1)S(1)}, u32[]{:S(2)}, u32[]{:S(2)}) async-start(bf16[8,320,128]{2,1,0:T(8,128)(2,1)} %pass_on.1), calls=%async_computation.3 | async-start | bytes 1310720 | tf_op jit(solution)/shard_map/all_to_all | solution.py:543
  104.4 20.8 %collective-permute-start.4 = (bf16[8,320,128]{2,1,0:T(8,128)(2,1)S(1)}, bf16[8,320,128]{2,1,0:T(8,128)(2,1)}, u32[]{:S(2)}, u32[]{:S(2)}) collective-permute-start(bf16[8,320,128]{2,1,0:T(8,128)(2,1)S(1)} %all_to_all.36.spread_ref.mine_ref), channel_id=1, source_target_pairs={{0,4},{4,0},{1,5},{5,1},{2,6},{6,2},{3,7},{7,3},{8,12},{12,8},{9,1... | collective-permute-start | bytes 1966088 | tf_op jit(solution)/shard_map/ppermute | solution.py:29
  107.6 0.9 copy-start.4
  108.5 0.8 copy-start.6
  109.7 0.7 copy-start.1
  143.5 32.2 %copy-start.2 = (f32[256,128]{1,0:T(8,128)S(1)}, f32[256,128]{1,0:T(8,128)}, u32[]{:S(2)}) copy-start(f32[256,128]{1,0:T(8,128)} %copy-done.1) | copy-start | bytes 393220
